TPU v7x, 256 devices: a whole 4x4x8 slice. The times are simulated.
256 devices in a mesh: kv: 32 (over z, y), tp: 8 (over x, core).
Axes of the slice: x: 4, y: 4, z: 8, core: 2. Of those that a mesh axis runs over, the one named last changes fastest.
Arguments:
- residual: bfloat16 [1024, 2048], P('kv', 'tp'), may hold values from -12 to 12
- first_gain: bfloat16 [2048], P('tp'), may hold values from 0.099609375 to 1.8984375
- first_gate: bfloat16 [2048, 5632], P('tp', 'kv'), may hold values from -0.125 to 0.125
- first_lift: bfloat16 [2048, 5632], P('tp', 'kv'), may hold values from -0.125 to 0.125
- first_down: bfloat16 [5632, 2048], P('kv', 'tp'), may hold values from -0.078125 to 0.078125
- mixer_gain: bfloat16 [2048], replicated, may hold values from 0.099609375 to 1.8984375
- proj_gate: bfloat16 [2048, 2048], P(None, 'tp'), may hold values from -0.125 to 0.125
- proj_input: bfloat16 [2048, 2048], P(None, 'tp'), may hold values from -0.125 to 0.125
- proj_write: bfloat16 [2048, 1024], P(None, 'tp'), may hold values from -0.125 to 0.125
- proj_read: bfloat16 [2048, 1024], P(None, 'tp'), may hold values from -0.125 to 0.125
- proj_step: bfloat16 [2048, 32], P(None, 'tp'), may hold values from -0.125 to 0.125
- step_bias: float32 [32], P('tp'), may hold values from -5 to -2
- rate_log: float32 [32], P('tp'), may hold values from -0.7 to 2.1
- skip_gain: float32 [32], P('tp'), may hold values from 0.5 to 2
- taps_input: bfloat16 [4, 2048], P(None, 'tp'), may hold values from -3 to 3
- taps_write: bfloat16 [4, 1024], P(None, 'tp'), may hold values from -3 to 3
- taps_read: bfloat16 [4, 1024], P(None, 'tp'), may hold values from -3 to 3
- buffer_input: bfloat16 [1024, 3, 2048], P('kv', None, 'tp'), may hold values from -6 to 6
- buffer_write: bfloat16 [1024, 3, 1024], P('kv', None, 'tp'), may hold values from -6 to 6
- buffer_read: bfloat16 [1024, 3, 1024], P('kv', None, 'tp'), may hold values from -6 to 6
- scan_state: float32 [1024, 32, 64, 128], P('kv', 'tp'), may hold values from -1.5 to 1.5
- group_gain: bfloat16 [2048], P('tp'), may hold values from 0.099609375 to 1.8984375
- proj_output: bfloat16 [2048, 2048], P('tp'), may hold values from -0.125 to 0.125
- second_gain: bfloat16 [2048], P('tp'), may hold values from 0.099609375 to 1.8984375
- second_gate: bfloat16 [2048, 5632], P('tp', 'kv'), may hold values from -0.125 to 0.125
- second_lift: bfloat16 [2048, 5632], P('tp', 'kv'), may hold values from -0.125 to 0.125
- second_down: bfloat16 [5632, 2048], P('kv', 'tp'), may hold values from -0.078125 to 0.078125
Outputs:
- residual_out: bfloat16 [1024, 2048], P('kv', 'tp')
- state_out: float32 [1024, 32, 64, 128], P('kv', 'tp')
All inputs are finite; a program needn't handle non-finite values.
Results may differ from a plain program's by a relative error of at most 0.023.
Values may be sent and summed in bfloat16 or wider, within the bound.
No kernel may reach another device: no remote copies, remote signals or barrier semaphores. Data moves between devices by JAX's collectives and lax.ppermute only.
A program may use at most 64 MiB of HBM per device.

v0:
```python
import jax
import jax.numpy as jnp
from jax import lax
from jax.sharding import PartitionSpec as P

D = 2048
HEAD_DIM = 64
STATE = 128


norm_eps = 1e-06


def sent_to_all(array, axis):
    length = lax.axis_size(axis)
    return lax.all_to_all(
        jnp.broadcast_to(array[None], (length, *array.shape)), axis, 0, 0, tiled=True
    )


def over_copies(array, axis):
    everything = sent_to_all(array, axis)
    return jnp.sum(everything, axis=0)


def joined_along(tiles, dim):
    tiles = jnp.moveaxis(tiles, 0, dim)
    shape = tiles.shape
    return tiles.reshape(*shape[:dim], shape[dim] * shape[dim + 1], *shape[dim + 2 :])


def gathered_copies(array, axis, dim):
    return joined_along(sent_to_all(array, axis), dim)


def in_blocks(array, dim, length):
    before, after = (array.shape[:dim], array.shape[dim + 1 :])
    return jnp.moveaxis(array.reshape(*before, length, -1, *after), dim, 0)


def sum_at_owner(array, axis, dim):
    length = lax.axis_size(axis)
    tiles = lax.all_to_all(in_blocks(array, dim, length), axis, 0, 0, tiled=True)
    return jnp.sum(tiles.astype(jnp.float32), axis=0)


def inverse_rms(values):
    return lax.rsqrt(jnp.mean(values * values, axis=-1, keepdims=True) + norm_eps)


def half_step(residual, gain, gate_weight, lift_weight, down_weight):
    widened = residual.astype(jnp.float32)
    row_total = over_copies(jnp.sum(widened * widened, axis=1), "tp")
    factor = lax.rsqrt(row_total / D + norm_eps)
    normed = (widened * factor[:, None] * gain.astype(jnp.float32)[None, :]).astype(jnp.bfloat16)
    hidden_cols = gate_weight.shape[1]
    row_piece = gathered_copies(normed, "kv", 0)
    gate_part = jnp.dot(row_piece, gate_weight, preferred_element_type=jnp.float32).astype(
        jnp.bfloat16
    )
    lift_part = jnp.dot(row_piece, lift_weight, preferred_element_type=jnp.float32).astype(
        jnp.bfloat16
    )
    joined = lax.optimization_barrier(jnp.concatenate([gate_part, lift_part], axis=1))
    partial_value = joined.astype(jnp.float32)
    share = sum_at_owner(partial_value.astype(jnp.bfloat16), "tp", 0)
    active = (jax.nn.silu(share[:, :hidden_cols]) * share[:, hidden_cols:]).astype(jnp.bfloat16)
    hidden = gathered_copies(active, "tp", 0)
    branch = sum_at_owner(
        jnp.dot(hidden, down_weight, preferred_element_type=jnp.float32).astype(jnp.bfloat16),
        "kv",
        0,
    )
    return (widened + 0.5 * branch).astype(jnp.bfloat16)


def short_conv(tap_weights, buffer, newest):
    taps_f = tap_weights.astype(jnp.float32)
    summed = jnp.sum(buffer.astype(jnp.float32) * taps_f[None, :-1, :], axis=1)
    summed = summed + newest.astype(jnp.float32) * taps_f[-1][None, :]
    return jax.nn.silu(summed)


def state_mixer(
    residual,
    mixer_gain,
    proj_gate,
    proj_input,
    proj_write,
    proj_read,
    proj_step,
    step_bias,
    rate_log,
    skip_gain,
    taps_input,
    taps_write,
    taps_read,
    buffer_input,
    buffer_write,
    buffer_read,
    scan_state,
    group_gain,
    proj_output,
):
    seq_rows = residual.shape[0]
    full_rows = gathered_copies(residual, "tp", 1)
    widened = full_rows.astype(jnp.float32)
    normed = (widened * inverse_rms(widened) * mixer_gain.astype(jnp.float32)[None, :]).astype(
        jnp.bfloat16
    )

    def state_project(weight):
        return jnp.dot(normed, weight, preferred_element_type=jnp.float32).astype(jnp.bfloat16)

    gate_z = state_project(proj_gate)
    input_new = state_project(proj_input)
    write_new = state_project(proj_write)
    read_new = state_project(proj_read)
    step_raw = state_project(proj_step)
    input_conv = short_conv(taps_input, buffer_input, input_new)
    write_conv = short_conv(taps_write, buffer_write, write_new)
    read_conv = short_conv(taps_read, buffer_read, read_new)
    head_count = proj_step.shape[1]
    group_count = proj_write.shape[1] // STATE
    per_group = head_count // group_count
    step = jax.nn.softplus(step_raw.astype(jnp.float32) + step_bias[None, :])
    retain = jnp.exp(-step * jnp.exp(rate_log)[None, :])
    input_heads = input_conv.reshape(seq_rows, group_count, per_group, HEAD_DIM)
    write_groups = write_conv.reshape(seq_rows, group_count, STATE)
    read_groups = read_conv.reshape(seq_rows, group_count, STATE)
    old_state = scan_state.reshape(seq_rows, group_count, per_group, HEAD_DIM, STATE)
    retain_g = retain.reshape(seq_rows, group_count, per_group)
    step_g = step.reshape(seq_rows, group_count, per_group)
    updated = (
        retain_g[..., None, None] * old_state
        + (step_g[..., None] * input_heads)[..., None] * write_groups[:, :, None, None, :]
    )
    head_out = jnp.einsum("bgrpn,bgn->bgrp", updated, read_groups)
    head_out = head_out + skip_gain.reshape(group_count, per_group)[None, :, :, None] * input_heads
    head_short = lax.optimization_barrier(head_out.astype(jnp.bfloat16))
    gated = head_short.astype(jnp.float32).reshape(seq_rows, group_count, per_group * HEAD_DIM)
    gated = gated * jax.nn.silu(
        gate_z.astype(jnp.float32).reshape(seq_rows, group_count, per_group * HEAD_DIM)
    )
    gated = (
        gated
        * inverse_rms(gated)
        * group_gain.astype(jnp.float32).reshape(group_count, per_group * HEAD_DIM)[None]
    )
    gated = gated.reshape(seq_rows, head_count * HEAD_DIM).astype(jnp.bfloat16)
    partial_out = jnp.dot(gated, proj_output, preferred_element_type=jnp.float32).astype(
        jnp.bfloat16
    )
    partial_out = lax.optimization_barrier(partial_out).astype(jnp.float32)
    mixed = sum_at_owner(partial_out.astype(jnp.bfloat16), "tp", 1)
    mixed_rows = (residual.astype(jnp.float32) + mixed).astype(jnp.bfloat16)
    return (mixed_rows, updated.reshape(seq_rows, head_count, HEAD_DIM, STATE))


def per_device(
    residual,
    first_gain,
    first_gate,
    first_lift,
    first_down,
    mixer_gain,
    proj_gate,
    proj_input,
    proj_write,
    proj_read,
    proj_step,
    step_bias,
    rate_log,
    skip_gain,
    taps_input,
    taps_write,
    taps_read,
    buffer_input,
    buffer_write,
    buffer_read,
    scan_state,
    group_gain,
    proj_output,
    second_gain,
    second_gate,
    second_lift,
    second_down,
):
    first = half_step(residual, first_gain, first_gate, first_lift, first_down)
    mixed, state_out = state_mixer(
        first,
        mixer_gain,
        proj_gate,
        proj_input,
        proj_write,
        proj_read,
        proj_step,
        step_bias,
        rate_log,
        skip_gain,
        taps_input,
        taps_write,
        taps_read,
        buffer_input,
        buffer_write,
        buffer_read,
        scan_state,
        group_gain,
        proj_output,
    )
    residual_out = half_step(mixed, second_gain, second_gate, second_lift, second_down)
    return (residual_out, state_out)


def solution(mesh):
    placed = (
        P("kv", "tp"),
        P("tp"),
        P("tp", "kv"),
        P("tp", "kv"),
        P("kv", "tp"),
        P(),
        P(None, "tp"),
        P(None, "tp"),
        P(None, "tp"),
        P(None, "tp"),
        P(None, "tp"),
        P("tp"),
        P("tp"),
        P("tp"),
        P(None, "tp"),
        P(None, "tp"),
        P(None, "tp"),
        P("kv", None, "tp"),
        P("kv", None, "tp"),
        P("kv", None, "tp"),
        P("kv", "tp", None, None),
        P("tp"),
        P("tp", None),
        P("tp"),
        P("tp", "kv"),
        P("tp", "kv"),
        P("kv", "tp"),
    )
    return jax.shard_map(
        per_device,
        mesh=mesh,
        in_specs=placed,
        out_specs=(P("kv", "tp"), P("kv", "tp", None, None)),
        check_vma=False,
    )
```

profile of v0, /device:TPU:1, one launch (start us, length us, event | category | flops | bytes accessed | tf_op | source)
XLA Modules:
  0.0 203.2 jit_solution(12820025739309025349)
XLA Ops:
  0.6 0.0 copy-start
  0.6 0.9 fusion.19
  1.6 0.6 broadcast_in_dim.14
  2.2 6.4 %all-to-all-start = ((f32[8,1,32]{2,1,0:T(1,128)}), f32[8,1,32]{2,1,0:T(1,128)S(1)}, u32[]{:S(2)}, u32[]{:S(2)}) async-start(f32[8,1,32]{2,1,0:T(1,128)} %broadcast_in_dim.14), calls=%async_computation | async-start | bytes 8192 | tf_op jit(solution)/shard_map/all_to_all | solution.py:16
  8.6 0.7 convert_element_type.159
  9.2 3.9 %all-to-all-done = f32[8,1,32]{2,1,0:T(1,128)S(1)} async-done(((f32[8,1,32]{2,1,0:T(1,128)}), f32[8,1,32]{2,1,0:T(1,128)S(1)}, u32[]{:S(2)}, u32[]{:S(2)}) %all-to-all-start) | async-done | bytes 1056 | tf_op jit(solution)/shard_map/all_to_all | solution.py:16
  13.2 0.8 fusion.21
  13.9 0.1 broadcast_in_dim.15
  14.0 26.7 %all_to_all.62 = bf16[32,32,256]{2,1,0:T(8,128)(2,1)S(1)} all-to-all(bf16[32,32,256]{2,1,0:T(8,128)(2,1)S(1)} %broadcast_in_dim.15), channel_id=1, replica_groups=mesh['kv'=32,'tp'=8] {'kv'}, dimensions={0} | all-to-all | bytes 1048576 | tf_op jit(solution)/shard_map/all_to_all | solution.py:16
  40.7 1.2 convolution_convert_fusion.5
  41.9 1.2 convolution_convert_fusion.6
  43.1 0.0 copy-start.12
  43.1 0.0 copy-start.13
  43.2 0.0 copy-start.20
  43.2 0.0 copy-start.14
  43.3 0.0 copy-start.5
  43.3 0.1 copy_bitcast_fusion.1
  43.5 0.0 copy-start.21
  43.5 0.0 copy-start.2
  43.5 16.5 %all_to_all.63 = bf16[8,128,352]{1,2,0:T(8,128)(2,1)S(1)} all-to-all(bf16[8,128,352]{1,2,0:T(8,128)(2,1)S(1)} %copy_bitcast_fusion.1), channel_id=1, replica_groups=mesh['kv'=32,'tp'=8] {'tp'}, dimensions={0} | all-to-all | bytes 1441792 | tf_op jit(solution)/shard_map/all_to_all | solution.py:43
  59.9 0.1 convert_reduce_fusion.1
  60.1 11.2 %all_to_all.64 = bf16[8,128,176]{1,2,0:T(8,128)(2,1)S(1)} all-to-all(bf16[8,128,176]{1,2,0:T(8,128)(2,1)S(1)} %broadcast_in_dim.16), channel_id=1, replica_groups=mesh['kv'=32,'tp'=8] {'tp'}, dimensions={0} | all-to-all | bytes 720896 | tf_op jit(solution)/shard_map/all_to_all | solution.py:16
  71.4 1.1 convolution_convert_fusion.2
  72.5 4.4 %all-to-all-start.4 = ((bf16[32,32,256]{2,1,0:T(8,128)(2,1)}), bf16[32,32,256]{2,1,0:T(8,128)(2,1)S(1)}, u32[]{:S(2)}, u32[]{:S(2)}) async-start(bf16[32,32,256]{2,1,0:T(8,128)(2,1)} %bitcast.84), calls=%async_computation.4 | async-start | bytes 1048576 | tf_op jit(solution)/shard_map/all_to_all | solution.py:43
  77.1 15.3 %all-to-all-done.4 = bf16[32,32,256]{2,1,0:T(8,128)(2,1)S(1)} async-done(((bf16[32,32,256]{2,1,0:T(8,128)(2,1)}), bf16[32,32,256]{2,1,0:T(8,128)(2,1)S(1)}, u32[]{:S(2)}, u32[]{:S(2)}) %all-to-all-start.4) | async-done | bytes 524320 | tf_op jit(solution)/shard_map/all_to_all | solution.py:43
  92.4 0.1 convert_reduce_fusion.3
  92.5 0.7 broadcast_in_dim.17
  93.2 6.4 %all-to-all-start.5 = ((bf16[8,32,256]{2,1,0:T(8,128)(2,1)}), bf16[8,32,256]{2,1,0:T(8,128)(2,1)S(1)}, u32[]{:S(2)}, u32[]{:S(2)}) async-start(bf16[8,32,256]{2,1,0:T(8,128)(2,1)} %broadcast_in_dim.17), calls=%async_computation.5 | async-start | bytes 262144 | tf_op jit(solution)/shard_map/all_to_all | solution.py:16
  99.6 5.2 %all-to-all-done.5 = bf16[8,32,256]{2,1,0:T(8,128)(2,1)S(1)} async-done(((bf16[8,32,256]{2,1,0:T(8,128)(2,1)}), bf16[8,32,256]{2,1,0:T(8,128)(2,1)S(1)}, u32[]{:S(2)}, u32[]{:S(2)}) %all-to-all-start.5) | async-done | bytes 131104 | tf_op jit(solution)/shard_map/all_to_all | solution.py:16
  104.9 0.1 fusion.16
  105.1 0.1 multiply_convert_fusion
  105.2 0.2 multiply_exponential_fusion
  105.4 0.1 copy.66
  105.4 0.1 copy.67
  105.5 0.3 divide_multiply_fusion
  105.9 0.1 reshape.157
  106.0 0.1 broadcast_multiply_fusion
  106.1 0.2 divide_multiply_fusion.1
  106.3 1.3 divide_multiply_fusion.2
  107.6 3.1 %multiply_add_fusion = f32[32,4,64,128]{3,2,1,0:T(8,128)S(1)} fusion(f32[32,4,64,128]{3,2,1,0:T(8,128)} %param.47, f32[32,128]{1,0:T(8,128)S(1)} %divide_multiply_fusion.2, f32[32,4,64]{2,1,0:T(4,128)S(1)} %broadcast_multiply_fusion, f32[32,4]{1,0:T(8,128)S(1)} %copy.66), kind=kLoop, calls=%fused_computation | loop fusion | flops 3145728 | bytes 8438272 | tf_op jit(solution)/shard_map/add | solution.py:135
  110.7 2.0 copy-done.1
  112.7 1.7 fusion.30
  114.4 0.1 fusion.27
  114.5 0.1 reshape.167
  114.6 0.4 multiply_reduce_fusion.3
  115.0 0.3 convolution_convert_fusion
  115.4 8.5 %all_to_all.65 = bf16[8,32,256]{2,1,0:T(8,128)(2,1)S(1)} all-to-all(bf16[8,32,256]{2,1,0:T(8,128)(2,1)S(1)} %bitcast.86), channel_id=1, replica_groups=mesh['kv'=32,'tp'=8] {'tp'}, dimensions={0} | all-to-all | bytes 262144 | tf_op jit(solution)/shard_map/all_to_all | solution.py:43
  123.9 0.1 fusion.23
  124.0 0.6 broadcast_in_dim.18
  124.6 4.1 %all-to-all-start.7 = ((f32[8,1,32]{2,1,0:T(1,128)}), f32[8,1,32]{2,1,0:T(1,128)S(1)}, u32[]{:S(2)}, u32[]{:S(2)}) async-start(f32[8,1,32]{2,1,0:T(1,128)} %broadcast_in_dim.18), calls=%async_computation.7 | async-start | bytes 8192 | tf_op jit(solution)/shard_map/all_to_all | solution.py:16
  128.7 4.5 %all-to-all-done.7 = f32[8,1,32]{2,1,0:T(1,128)S(1)} async-done(((f32[8,1,32]{2,1,0:T(1,128)}), f32[8,1,32]{2,1,0:T(1,128)S(1)}, u32[]{:S(2)}, u32[]{:S(2)}) %all-to-all-start.7) | async-done | bytes 1056 | tf_op jit(solution)/shard_map/all_to_all | solution.py:16
  133.3 0.1 fusion.25
  133.3 0.1 broadcast_in_dim.19
  133.4 20.5 %all_to_all.66 = bf16[32,32,256]{2,1,0:T(8,128)(2,1)S(1)} all-to-all(bf16[32,32,256]{2,1,0:T(8,128)(2,1)S(1)} %broadcast_in_dim.19), channel_id=1, replica_groups=mesh['kv'=32,'tp'=8] {'kv'}, dimensions={0} | all-to-all | bytes 1048576 | tf_op jit(solution)/shard_map/all_to_all | solution.py:16
  153.9 0.3 convolution_convert_fusion.3
  154.2 0.3 convolution_convert_fusion.4
  154.6 0.1 copy_bitcast_fusion
  154.8 16.3 %all_to_all.67 = bf16[8,128,352]{1,2,0:T(8,128)(2,1)S(1)} all-to-all(bf16[8,128,352]{1,2,0:T(8,128)(2,1)S(1)} %copy_bitcast_fusion), channel_id=1, replica_groups=mesh['kv'=32,'tp'=8] {'tp'}, dimensions={0} | all-to-all | bytes 1441792 | tf_op jit(solution)/shard_map/all_to_all | solution.py:43
  171.1 0.1 convert_reduce_fusion
  171.3 11.1 %all_to_all.68 = bf16[8,128,176]{1,2,0:T(8,128)(2,1)S(1)} all-to-all(bf16[8,128,176]{1,2,0:T(8,128)(2,1)S(1)} %broadcast_in_dim.20), channel_id=1, replica_groups=mesh['kv'=32,'tp'=8] {'tp'}, dimensions={0} | all-to-all | bytes 720896 | tf_op jit(solution)/shard_map/all_to_all | solution.py:16
  182.3 0.3 convolution_convert_fusion.1
  182.7 19.7 %all_to_all.69 = bf16[32,32,256]{2,1,0:T(8,128)(2,1)S(1)} all-to-all(bf16[32,32,256]{2,1,0:T(8,128)(2,1)S(1)} %bitcast.85), channel_id=1, replica_groups=mesh['kv'=32,'tp'=8] {'kv'}, dimensions={0} | all-to-all | bytes 1048576 | tf_op jit(solution)/shard_map/all_to_all | solution.py:43
  202.5 0.1 convert_reduce_fusion.2
  202.5 0.6 fusion.26
  (69 shorter events, 0.6 us)
Async XLA Ops:
  0.6 114.4 %copy-start = (bf16[256,2048]{1,0:T(8,128)(2,1)S(1)}, bf16[256,2048]{1,0:T(8,128)(2,1)}, u32[]{:S(2)}) copy-start(bf16[256,2048]{1,0:T(8,128)(2,1)} %param.49) | copy-start | bytes 3145732
  2.2 11.0 %all-to-all-start = ((f32[8,1,32]{2,1,0:T(1,128)}), f32[8,1,32]{2,1,0:T(1,128)S(1)}, u32[]{:S(2)}, u32[]{:S(2)}) async-start(f32[8,1,32]{2,1,0:T(1,128)} %broadcast_in_dim.14), calls=%async_computation | async-start | bytes 8192 | tf_op jit(solution)/shard_map/all_to_all | solution.py:16
  40.7 30.7 %copy-start.16 = (bf16[176,256]{1,0:T(8,128)(2,1)S(1)}, bf16[176,256]{1,0:T(8,128)(2,1)}, u32[]{:S(2)}) copy-start(bf16[176,256]{1,0:T(8,128)(2,1)} %param.31) | copy-start | bytes 270340
  43.1 33.7 %copy-start.12 = (bf16[4,128]{1,0:T(4,128)(2,1)S(1)}, bf16[4,128]{1,0:T(4,128)(2,1)}, u32[]{:S(2)}) copy-start(bf16[4,128]{1,0:T(4,128)(2,1)} %param.42) | copy-start | bytes 3076
  43.1 33.8 %copy-start.13 = (bf16[4,128]{1,0:T(4,128)(2,1)S(1)}, bf16[4,128]{1,0:T(4,128)(2,1)}, u32[]{:S(2)}) copy-start(bf16[4,128]{1,0:T(4,128)(2,1)} %param.43) | copy-start | bytes 3076
  43.2 33.8 %copy-start.11 = (bf16[4,256]{1,0:T(4,128)(2,1)S(1)}, bf16[4,256]{1,0:T(4,128)(2,1)}, u32[]{:S(2)}) copy-start(bf16[4,256]{1,0:T(4,128)(2,1)} %param.41) | copy-start | bytes 6148
  43.2 33.8 %copy-start.19 = (f32[4]{0:T(128)S(1)}, f32[4]{0:T(128)}, u32[]{:S(2)}) copy-start(f32[4]{0:T(128)} %param.39) | copy-start | bytes 52
  43.2 33.8 %copy-start.20 = (bf16[256]{0:T(256)(128)(2,1)S(1)}, bf16[256]{0:T(256)(128)(2,1)}, u32[]{:S(2)}) copy-start(bf16[256]{0:T(256)(128)(2,1)} %param.48) | copy-start | bytes 1540
  43.2 33.8 %copy-start.14 = (bf16[2048]{0:T(1024)(128)(2,1)S(1)}, bf16[2048]{0:T(1024)(128)(2,1)}, u32[]{:S(2)}) copy-start(bf16[2048]{0:T(1024)(128)(2,1)} %param.32) | copy-start | bytes 12292
  43.2 33.8 %copy-start.9 = (bf16[32,3,128]{2,0,1:T(8,128)(2,1)S(1)}, bf16[32,3,128]{2,0,1:T(8,128)(2,1)}, u32[]{:S(2)}) copy-start(bf16[32,3,128]{2,0,1:T(8,128)(2,1)} %param.46) | copy-start | bytes 73732
  43.2 33.9 %copy-start.10 = (bf16[32,3,128]{2,0,1:T(8,128)(2,1)S(1)}, bf16[32,3,128]{2,0,1:T(8,128)(2,1)}, u32[]{:S(2)}) copy-start(bf16[32,3,128]{2,0,1:T(8,128)(2,1)} %param.45) | copy-start | bytes 73732
  43.3 49.2 %copy-start.5 = (bf16[32,256]{1,0:T(8,128)(2,1)S(1)}, bf16[32,256]{1,0:T(8,128)(2,1)}, u32[]{:S(2)}) copy-start(bf16[32,256]{1,0:T(8,128)(2,1)} %param.27) | copy-start | bytes 49156
  43.3 56.3 %copy-start.8 = (bf16[32,3,256]{2,0,1:T(8,128)(2,1)S(1)}, bf16[32,3,256]{2,0,1:T(8,128)(2,1)}, u32[]{:S(2)}) copy-start(bf16[32,3,256]{2,0,1:T(8,128)(2,1)} %param.44) | copy-start | bytes 147460
  43.4 61.7 %copy-start.18 = (bf16[2048,4]{0,1:T(4,128)(2,1)S(1)}, bf16[2048,4]{0,1:T(4,128)(2,1)}, u32[]{:S(2)}) copy-start(bf16[2048,4]{0,1:T(4,128)(2,1)} %param.37) | copy-start | bytes 49156
  43.5 61.7 %copy-start.21 = (f32[4]{0:T(128)S(1)}, f32[4]{0:T(128)}, u32[]{:S(2)}) copy-start(f32[4]{0:T(128)} %param.38) | copy-start | bytes 52
  43.5 62.1 %copy-start.2 = (bf16[2048,256]{1,0:T(8,128)(2,1)S(1)}, bf16[2048,256]{1,0:T(8,128)(2,1)}, u32[]{:S(2)}) copy-start(bf16[2048,256]{1,0:T(8,128)(2,1)} %param.34) | copy-start | bytes 3145732
  60.0 46.0 %copy-start.4 = (bf16[2048,128]{1,0:T(8,128)(2,1)S(1)}, bf16[2048,128]{1,0:T(8,128)(2,1)}, u32[]{:S(2)}) copy-start(bf16[2048,128]{1,0:T(8,128)(2,1)} %param.36) | copy-start | bytes 1572868
  72.5 19.9 %all-to-all-start.4 = ((bf16[32,32,256]{2,1,0:T(8,128)(2,1)}), bf16[32,32,256]{2,1,0:T(8,128)(2,1)S(1)}, u32[]{:S(2)}, u32[]{:S(2)}) async-start(bf16[32,32,256]{2,1,0:T(8,128)(2,1)} %bitcast.84), calls=%async_computation.4 | async-start | bytes 1048576 | tf_op jit(solution)/shard_map/all_to_all | solution.py:43
  93.2 11.6 %all-to-all-start.5 = ((bf16[8,32,256]{2,1,0:T(8,128)(2,1)}), bf16[8,32,256]{2,1,0:T(8,128)(2,1)S(1)}, u32[]{:S(2)}, u32[]{:S(2)}) async-start(bf16[8,32,256]{2,1,0:T(8,128)(2,1)} %broadcast_in_dim.17), calls=%async_computation.5 | async-start | bytes 262144 | tf_op jit(solution)/shard_map/all_to_all | solution.py:16
  110.6 2.0 copy-start.1
  110.7 3.7 %copy-start.15 = (f32[4]{0:T(128)S(1)}, f32[4]{0:T(128)}, u32[]{:S(2)}) copy-start(f32[4]{0:T(128)} %param.40) | copy-start | bytes 52
  110.7 3.9 %copy-start.3 = (bf16[2048,256]{1,0:T(8,128)(2,1)S(1)}, bf16[2048,256]{1,0:T(8,128)(2,1)}, u32[]{:S(2)}) copy-start(bf16[2048,256]{1,0:T(8,128)(2,1)} %param.33) | copy-start | bytes 3145732
  110.7 18.0 %copy-start.22 = (bf16[256]{0:T(256)(128)(2,1)S(1)}, bf16[256]{0:T(256)(128)(2,1)}, u32[]{:S(2)}) copy-start(bf16[256]{0:T(256)(128)(2,1)} %param.50) | copy-start | bytes 1540
  112.7 41.2 %copy-start.6 = (bf16[256,176]{0,1:T(8,128)(2,1)S(1)}, bf16[256,176]{0,1:T(8,128)(2,1)}, u32[]{:S(2)}) copy-start(bf16[256,176]{0,1:T(8,128)(2,1)} %param.52) | copy-start | bytes 270340
  112.7 41.6 %copy-start.7 = (bf16[256,176]{0,1:T(8,128)(2,1)S(1)}, bf16[256,176]{0,1:T(8,128)(2,1)}, u32[]{:S(2)}) copy-start(bf16[256,176]{0,1:T(8,128)(2,1)} %param.51) | copy-start | bytes 270340
  124.6 8.6 %all-to-all-start.7 = ((f32[8,1,32]{2,1,0:T(1,128)}), f32[8,1,32]{2,1,0:T(1,128)S(1)}, u32[]{:S(2)}, u32[]{:S(2)}) async-start(f32[8,1,32]{2,1,0:T(1,128)} %broadcast_in_dim.18), calls=%async_computation.7 | async-start | bytes 8192 | tf_op jit(solution)/shard_map/all_to_all | solution.py:16
  153.9 28.5 %copy-start.17 = (bf16[176,256]{1,0:T(8,128)(2,1)S(1)}, bf16[176,256]{1,0:T(8,128)(2,1)}, u32[]{:S(2)}) copy-start(bf16[176,256]{1,0:T(8,128)(2,1)} %param.53) | copy-start | bytes 270340
where the time goes:
time: 205 us; the launch traced here: 203 us
  blocking collectives  130 us (63%)
  waiting for transfers between devices  29 us (14%)
  starting transfers between devices  21.2 us (10%)
  matrix products  8.98 us (4%)
  other arithmetic  7.38 us (4%)
  local copies, waits for them, and re-layouts  4.87 us (2%)
    all_to_all x4, blocking collectives, sent_to_all(): lax.all_to_all(jnp.broadcast_to(array[None], (length, *array.shape)), axi...  69.4 us
    all_to_all x4, blocking collectives, sum_at_owner(): lax.all_to_all(in_blocks(array, dim, length), axis, 0, 0, tiled=True)  61 us
    all_to_all x3, starting transfers between devices, sent_to_all(): lax.all_to_all(jnp.broadcast_to(array[None], (length, *array.shape)), axi...  16.9 us
    all_to_all x1, waiting for transfers between devices, sum_at_owner(): lax.all_to_all(in_blocks(array, dim, length), axis, 0, 0, tiled=True)  15.3 us
    all_to_all x3, waiting for transfers between devices, sent_to_all(): lax.all_to_all(jnp.broadcast_to(array[None], (length, *array.shape)), axi...  13.7 us
    all_to_all x1, starting transfers between devices, sum_at_owner(): lax.all_to_all(in_blocks(array, dim, length), axis, 0, 0, tiled=True)  4.37 us
  transfers between devices with their start and end apart: 4, of which 4 were waited for; matrix products, arithmetic and copies ran while one was open for 0% of the time, Pallas kernels for 0%

commit v1 on v0

--- a/solution.py
+++ b/solution.py
@@ -1,12 +1,16 @@
 import jax
 import jax.numpy as jnp
 from jax import lax
+from jax.experimental import pallas as pl
+from jax.experimental.pallas import tpu as pltpu
 from jax.sharding import PartitionSpec as P
 
 D = 2048
 HEAD_DIM = 64
 STATE = 128
-
+FEATS = 256
+HIDDEN = 176
+ROWS = 4
 
 norm_eps = 1e-06
 
@@ -18,60 +22,63 @@
     )
 
 
-def over_copies(array, axis):
-    everything = sent_to_all(array, axis)
-    return jnp.sum(everything, axis=0)
-
-
-def joined_along(tiles, dim):
-    tiles = jnp.moveaxis(tiles, 0, dim)
-    shape = tiles.shape
-    return tiles.reshape(*shape[:dim], shape[dim] * shape[dim + 1], *shape[dim + 2 :])
-
-
-def gathered_copies(array, axis, dim):
-    return joined_along(sent_to_all(array, axis), dim)
-
-
-def in_blocks(array, dim, length):
-    before, after = (array.shape[:dim], array.shape[dim + 1 :])
-    return jnp.moveaxis(array.reshape(*before, length, -1, *after), dim, 0)
-
-
-def sum_at_owner(array, axis, dim):
-    length = lax.axis_size(axis)
-    tiles = lax.all_to_all(in_blocks(array, dim, length), axis, 0, 0, tiled=True)
-    return jnp.sum(tiles.astype(jnp.float32), axis=0)
-
-
 def inverse_rms(values):
     return lax.rsqrt(jnp.mean(values * values, axis=-1, keepdims=True) + norm_eps)
 
 
-def half_step(residual, gain, gate_weight, lift_weight, down_weight):
-    widened = residual.astype(jnp.float32)
-    row_total = over_copies(jnp.sum(widened * widened, axis=1), "tp")
-    factor = lax.rsqrt(row_total / D + norm_eps)
-    normed = (widened * factor[:, None] * gain.astype(jnp.float32)[None, :]).astype(jnp.bfloat16)
-    hidden_cols = gate_weight.shape[1]
-    row_piece = gathered_copies(normed, "kv", 0)
-    gate_part = jnp.dot(row_piece, gate_weight, preferred_element_type=jnp.float32).astype(
-        jnp.bfloat16
-    )
-    lift_part = jnp.dot(row_piece, lift_weight, preferred_element_type=jnp.float32).astype(
-        jnp.bfloat16
-    )
-    joined = lax.optimization_barrier(jnp.concatenate([gate_part, lift_part], axis=1))
-    partial_value = joined.astype(jnp.float32)
-    share = sum_at_owner(partial_value.astype(jnp.bfloat16), "tp", 0)
-    active = (jax.nn.silu(share[:, :hidden_cols]) * share[:, hidden_cols:]).astype(jnp.bfloat16)
-    hidden = gathered_copies(active, "tp", 0)
-    branch = sum_at_owner(
-        jnp.dot(hidden, down_weight, preferred_element_type=jnp.float32).astype(jnp.bfloat16),
-        "kv",
-        0,
-    )
-    return (widened + 0.5 * branch).astype(jnp.bfloat16)
+def shift_perm(shift):
+    return [(i, (i + shift) % 8) for i in range(8)]
+
+
+def gathered_weights(gain, gate_weight, lift_weight, down_weight):
+    gain_f = gain.astype(jnp.float32)[None, :]
+    gate_t = (gate_weight.T.astype(jnp.float32) * gain_f).astype(jnp.bfloat16)
+    lift_t = (lift_weight.T.astype(jnp.float32) * gain_f).astype(jnp.bfloat16)
+    own = jnp.concatenate([gate_t, lift_t, down_weight], axis=0)
+    pieces = [own] + [lax.ppermute(own, "tp", shift_perm(s)) for s in (2, 4, 6)]
+    swap = [(i, i ^ 1) for i in range(8)]
+    return pieces + [lax.ppermute(piece, "tp", swap) for piece in pieces]
+
+
+def ffn_kernel(tp_ref, rows_ref, *refs):
+    weights, out_ref, normed_ref = refs[:8], refs[8], refs[9]
+    tp = tp_ref[0]
+    values = rows_ref[...].astype(jnp.float32)
+    factor = lax.rsqrt(jnp.sum(values * values, axis=-1, keepdims=True) * (1.0 / D) + norm_eps)
+    for u in range(8):
+        normed_ref[u] = (values[:, u * FEATS : (u + 1) * FEATS] * factor).astype(jnp.bfloat16)
+    chip, core = tp // 2, tp % 2
+    owners = [((chip + 4 - j) % 4) * 2 + core for j in range(4)]
+    owners = owners + [((chip + 4 - j) % 4) * 2 + 1 - core for j in range(4)]
+    contract = (((1,), (1,)), ((), ()))
+    gate = jnp.zeros((values.shape[0], HIDDEN), jnp.float32)
+    lift = jnp.zeros((values.shape[0], HIDDEN), jnp.float32)
+    for j in range(8):
+        block = normed_ref[owners[j]]
+        gate += lax.dot_general(
+            block, weights[j][:HIDDEN], contract, preferred_element_type=jnp.float32
+        )
+        lift += lax.dot_general(
+            block, weights[j][HIDDEN : 2 * HIDDEN], contract, preferred_element_type=jnp.float32
+        )
+    hidden = (gate * jax.nn.sigmoid(gate) * lift).astype(jnp.bfloat16)
+    for j in range(8):
+        down = jnp.dot(hidden, weights[j][2 * HIDDEN :], preferred_element_type=jnp.float32)
+        out_ref[owners[j]] = down.astype(jnp.bfloat16)
+
+
+def ffn_partial(rows, weights):
+    tp = lax.axis_index("tp").astype(jnp.int32).reshape(1)
+    count = rows.shape[0]
+    return pl.pallas_call(
+        ffn_kernel,
+        out_shape=jax.ShapeDtypeStruct((8, count, FEATS), jnp.bfloat16),
+        in_specs=[pl.BlockSpec(memory_space=pltpu.SMEM)]
+        + [pl.BlockSpec(memory_space=pltpu.VMEM)] * 9,
+        out_specs=pl.BlockSpec(memory_space=pltpu.VMEM),
+        scratch_shapes=[pltpu.VMEM((8, count, FEATS), jnp.bfloat16)],
+        name="ffn",
+    )(tp, rows, *weights)
 
 
 def short_conv(tap_weights, buffer, newest):
@@ -102,8 +109,8 @@
     group_gain,
     proj_output,
 ):
-    seq_rows = residual.shape[0]
-    full_rows = gathered_copies(residual, "tp", 1)
+    full_rows = sent_to_all(residual, "tp").reshape(8 * ROWS, D)
+    seq_rows = full_rows.shape[0]
     widened = full_rows.astype(jnp.float32)
     normed = (widened * inverse_rms(widened) * mixer_gain.astype(jnp.float32)[None, :]).astype(
         jnp.bfloat16
@@ -151,8 +158,8 @@
     partial_out = jnp.dot(gated, proj_output, preferred_element_type=jnp.float32).astype(
         jnp.bfloat16
     )
-    partial_out = lax.optimization_barrier(partial_out).astype(jnp.float32)
-    mixed = sum_at_owner(partial_out.astype(jnp.bfloat16), "tp", 1)
+    tiles = lax.all_to_all(partial_out.reshape(8, ROWS, D), "tp", 0, 0, tiled=True)
+    mixed = jnp.sum(tiles.astype(jnp.float32), axis=0)
     mixed_rows = (residual.astype(jnp.float32) + mixed).astype(jnp.bfloat16)
     return (mixed_rows, updated.reshape(seq_rows, head_count, HEAD_DIM, STATE))
 
@@ -186,7 +193,28 @@
     second_lift,
     second_down,
 ):
-    first = half_step(residual, first_gain, first_gate, first_lift, first_down)
+    weights_one = gathered_weights(first_gain, first_gate, first_lift, first_down)
+    weights_two = gathered_weights(second_gain, second_gate, second_lift, second_down)
+    kv = lax.axis_index("kv")
+    kv_size = lax.axis_size("kv")
+    both = ("kv", "tp")
+
+    split = residual.reshape(8, ROWS, FEATS)
+    tiles = lax.all_to_all(
+        jnp.broadcast_to(split[None], (kv_size, 8, ROWS, FEATS)).reshape(-1, ROWS, FEATS),
+        both,
+        0,
+        0,
+        tiled=True,
+    ).reshape(kv_size, 8, ROWS, FEATS)
+    rows = tiles.transpose(0, 2, 1, 3).reshape(kv_size * ROWS, D)
+    own_rows = lax.dynamic_slice_in_dim(rows, kv * ROWS, ROWS, 0)
+    share = ffn_partial(rows, weights_one)
+    share = share.reshape(8, kv_size, ROWS, FEATS).transpose(1, 2, 0, 3)
+    share = lax.all_to_all(share.reshape(kv_size, ROWS, D), "kv", 0, 0, tiled=True)
+    branch = jnp.sum(share.astype(jnp.float32), axis=0)
+    first = (own_rows.astype(jnp.float32) + 0.5 * branch).astype(jnp.bfloat16)
+
     mixed, state_out = state_mixer(
         first,
         mixer_gain,
@@ -208,7 +236,16 @@
         group_gain,
         proj_output,
     )
-    residual_out = half_step(mixed, second_gain, second_gate, second_lift, second_down)
+
+    rows = sent_to_all(mixed, "kv").reshape(kv_size * ROWS, D)
+    share = ffn_partial(rows, weights_two)
+    share = share.reshape(8, kv_size, ROWS, FEATS).transpose(1, 0, 2, 3)
+    mine = (jnp.arange(kv_size) == kv)[:, None, None, None]
+    own = 2.0 * mixed.astype(jnp.float32).reshape(ROWS, 8, FEATS).transpose(1, 0, 2)
+    share = jnp.where(mine, share.astype(jnp.float32) + own[None], share.astype(jnp.float32))
+    share = share.astype(jnp.bfloat16).reshape(-1, ROWS, FEATS)
+    share = lax.all_to_all(share, both, 0, 0, tiled=True).reshape(kv_size, 8 * ROWS, FEATS)
+    residual_out = (0.5 * jnp.sum(share.astype(jnp.float32), axis=0)).astype(jnp.bfloat16)
     return (residual_out, state_out)
 
 

time: 205 us -> 170 us (0.83)
  blocking collectives: 130 us -> 39.9 us
  starting transfers between devices: 21.2 us -> 56.7 us
  waiting for transfers between devices: 29 us -> 37.9 us
  local copies, waits for them, and re-layouts: 4.87 us -> 13.7 us
  Pallas kernels: 0 us -> 7 us
  matrix products: 8.98 us -> 4.38 us
    all_to_all x8 -> x2, blocking collectives: 130 us -> 39.9 us  [the longest x1 31.4 us: per_device(): lax.all_to_all(share, both, 0, 0, tiled=True)]
    ppermute x0 -> x14, starting transfers between devices: none -> 22.5 us  [the longest x8 14.6 us: gathered_weights(): return pieces + [lax.ppermute(piece, 'tp', swap) for piece in pieces]]
    all_to_all x1 -> x2, starting transfers between devices: 4.37 us -> 24.4 us  [the longest x1 15.6 us: per_device(): lax.all_to_all(jnp.broadcast_to(split[None], (kv_size, 8, ROWS, FEATS)).r...]
    ppermute x0 -> x14, waiting for transfers between devices: none -> 16.2 us  [the longest x6 15.3 us: gathered_weights(): pieces = [own] + [lax.ppermute(own, 'tp', shift_perm(s)) for s in (2, 4, 6)]]
    all_to_all x3 -> x2, waiting for transfers between devices: 13.7 us -> 5.25 us  [sent_to_all(): lax.all_to_all(jnp.broadcast_to(array[None], (length, *array.shape)), axi...]
    all_to_all x3 -> x2, starting transfers between devices: 16.9 us -> 9.73 us  [sent_to_all(): lax.all_to_all(jnp.broadcast_to(array[None], (length, *array.shape)), axi...]
    pallas_call x0 -> x2, Pallas kernels: none -> 7 us  [ffn_partial(): pl.pallas_call(ffn_kernel, out_shape=jax.ShapeDtypeStruct((8, count, FEAT...]
    dot_general x6 -> x0, matrix products: 4.59 us -> none  [the longest x2 1.56 us: half_step(): jnp.dot(row_piece, lift_weight, preferred_element_type=jnp.float32)]
  transfers between devices with their start and end apart: 4 -> 18, of which waited for: 4 -> 7; matrix products, arithmetic and copies ran while one was open for 0% -> 3% of each run, Pallas kernels for 0% -> 0%
where the time goes in v1:
time: 170 us; the launch traced here: 169 us
  starting transfers between devices  56.7 us (33%)
  blocking collectives  39.9 us (23%)
  waiting for transfers between devices  37.9 us (22%)
  local copies, waits for them, and re-layouts  13.7 us (8%)
  other arithmetic  8.59 us (5%)
  Pallas kernels  7 us (4%)
  matrix products  4.38 us (3%)
    all_to_all x1, blocking collectives, per_device(): lax.all_to_all(share, both, 0, 0, tiled=True)  31.4 us
    all_to_all x1, waiting for transfers between devices, per_device(): lax.all_to_all(share.reshape(kv_size, ROWS, D), 'kv', 0, 0, tiled=True)  16.4 us
    all_to_all x1, starting transfers between devices, per_device(): lax.all_to_all(jnp.broadcast_to(split[None], (kv_size, 8, ROWS, FEATS)).r...  15.6 us
    ppermute x6, waiting for transfers between devices, gathered_weights(): pieces = [own] + [lax.ppermute(own, 'tp', shift_perm(s)) for s in (2, 4, 6)]  15.3 us
    ppermute x8, starting transfers between devices, gathered_weights(): return pieces + [lax.ppermute(piece, 'tp', swap) for piece in pieces]  14.6 us
    all_to_all x2, starting transfers between devices, sent_to_all(): lax.all_to_all(jnp.broadcast_to(array[None], (length, *array.shape)), axi...  9.73 us
    all_to_all x1, starting transfers between devices, per_device(): lax.all_to_all(share.reshape(kv_size, ROWS, D), 'kv', 0, 0, tiled=True)  8.78 us
    all_to_all x1, blocking collectives, state_mixer(): lax.all_to_all(partial_out.reshape(8, ROWS, D), 'tp', 0, 0, tiled=True)  8.49 us
  transfers between devices with their start and end apart: 18, of which 7 were waited for; matrix products, arithmetic and copies ran while one was open for 3% of the time, Pallas kernels for 0%

profile of v1, /device:TPU:1, one launch (start us, length us, event | category | flops | bytes accessed | tf_op | source)
XLA Modules:
  0.0 169.4 jit_solution(9826098348864546498)
XLA Ops:
  0.6 0.8 broadcast_in_dim.14
  1.5 1.0 broadcast_in_dim.15
  2.5 15.6 %all-to-all-start = ((bf16[256,4,256]{2,1,0:T(4,128)(2,1)}), bf16[256,4,256]{2,1,0:T(4,128)(2,1)S(1)}, u32[]{:S(2)}, u32[]{:S(2)}) async-start(bf16[256,4,256]{2,1,0:T(4,128)(2,1)} %bitcast.1), calls=%async_computation | async-start | bytes 1048576 | tf_op jit(solution)/shard_map/all_to_all | solution.py:203
  18.1 0.7 convert_element_type.170
  18.8 1.0 fusion.14
  19.8 0.9 pad_maximum_fusion.refs_0_
  20.7 1.4 collective-permute-start
  22.1 2.4 %collective-permute-start.1 = (bf16[528,256]{1,0:T(8,128)(2,1)S(1)}, bf16[528,256]{1,0:T(8,128)(2,1)S(1)}, u32[]{:S(2)}, u32[]{:S(2)}) collective-permute-start(bf16[528,256]{1,0:T(8,128)(2,1)S(1)} %pad_maximum_fusion.refs_0_), channel_id=1, source_target_pairs={{0,4},{1,5},{2,6},{3,7},{4,0},{5,1},{6,2},{7,3},{8,12},{9,13},{10,... | collective-permute-start | bytes 811016 | tf_op jit(solution)/shard_map/ppermute | solution.py:38
  24.5 1.2 collective-permute-start.2
  25.7 1.2 collective-permute-start.3
  26.9 5.0 %collective-permute-done.refs_1_ = bf16[528,256]{1,0:T(8,128)(2,1)S(1)} collective-permute-done((bf16[528,256]{1,0:T(8,128)(2,1)S(1)}, bf16[528,256]{1,0:T(8,128)(2,1)S(1)}, u32[]{:S(2)}, u32[]{:S(2)}) %collective-permute-start) | collective-permute-done | bytes 270368 | tf_op jit(solution)/shard_map/ppermute | solution.py:38
  31.9 2.8 %collective-permute-start.4 = (bf16[528,256]{1,0:T(8,128)(2,1)S(1)}, bf16[528,256]{1,0:T(8,128)(2,1)S(1)}, u32[]{:S(2)}, u32[]{:S(2)}) collective-permute-start(bf16[528,256]{1,0:T(8,128)(2,1)S(1)} %collective-permute-done.refs_1_), channel_id=1, source_target_pairs={{0,1},{1,0},{2,3},{3,2},{4,5},{5,4},{6,7},{7,6},{8,9},{9,8},{10,11... | collective-permute-start | bytes 811016 | tf_op jit(solution)/shard_map/ppermute | solution.py:40
  34.7 6.2 %collective-permute-done.1.refs_2_ = bf16[528,256]{1,0:T(8,128)(2,1)S(1)} collective-permute-done((bf16[528,256]{1,0:T(8,128)(2,1)S(1)}, bf16[528,256]{1,0:T(8,128)(2,1)S(1)}, u32[]{:S(2)}, u32[]{:S(2)}) %collective-permute-start.1) | collective-permute-done | bytes 270368 | tf_op jit(solution)/shard_map/ppermute | solution.py:38
  40.9 0.9 collective-permute-start.5
  41.8 0.1 collective-permute-start.6
  42.1 0.9 copy.75
  43.0 0.5 collective-permute-done.6.refs_7_
  43.5 0.2 copy-done.12
  43.7 0.1 copy-done.15
  43.9 3.5 %ffn.2 = bf16[8,128,256]{2,1,0:T(8,128)(2,1)} custom-call(s32[1]{0:T(128)} %bitcast.tp_ref, bf16[128,2048]{1,0:T(8,128)(2,1)} %bitcast.65, bf16[528,256]{1,0:T(8,128)(2,1)} %copy-done.2, bf16[528,256]{1,0:T(8,128)(2,1)} %copy-done.7, bf16[528,256]{1,0:T(8,128)(2,1)} %copy-done.8, bf16[528,256]{1,0:T(8,128)(2,1)} %copy-done.10, bf16[528,256]{1,0:T(8,128)(2,1)} %copy-done.12, ...), custom_call_target="tpu_custom_call" | custom-call | tf_op jit(solution)/shard_map/ffn/pallas_call | solution.py:73
  47.5 1.3 reshape.157
  48.7 0.3 copy.84
  49.0 0.2 reshape.158
  49.3 1.2 copy.65
  50.5 8.8 %all-to-all-start.1 = ((bf16[32,4,2048]{2,1,0:T(4,128)(2,1)}), bf16[32,4,2048]{2,1,0:T(4,128)(2,1)S(1)}, u32[]{:S(2)}, u32[]{:S(2)}) async-start(bf16[32,4,2048]{2,1,0:T(4,128)(2,1)} %copy.65), calls=%async_computation.1 | async-start | bytes 1048576 | tf_op jit(solution)/shard_map/all_to_all | solution.py:214
  59.5 16.4 %all-to-all-done.1 = bf16[32,4,2048]{2,1,0:T(4,128)(2,1)S(1)} async-done(((bf16[32,4,2048]{2,1,0:T(4,128)(2,1)}), bf16[32,4,2048]{2,1,0:T(4,128)(2,1)S(1)}, u32[]{:S(2)}, u32[]{:S(2)}) %all-to-all-start.1) | async-done | bytes 524320 | tf_op jit(solution)/shard_map/all_to_all | solution.py:214
  75.9 0.2 convert_reduce_fusion
  76.1 0.8 add_convert_fusion.2
  76.9 0.7 broadcast_in_dim.16
  77.6 5.4 %all-to-all-start.2 = ((bf16[8,4,2048]{2,1,0:T(4,128)(2,1)}), bf16[8,4,2048]{2,1,0:T(4,128)(2,1)S(1)}, u32[]{:S(2)}, u32[]{:S(2)}) async-start(bf16[8,4,2048]{2,1,0:T(4,128)(2,1)} %broadcast_in_dim.16), calls=%async_computation.2 | async-start | bytes 262144 | tf_op jit(solution)/shard_map/all_to_all | solution.py:20
  83.0 5.2 %all-to-all-done.2 = bf16[8,4,2048]{2,1,0:T(4,128)(2,1)S(1)} async-done(((bf16[8,4,2048]{2,1,0:T(4,128)(2,1)}), bf16[8,4,2048]{2,1,0:T(4,128)(2,1)S(1)}, u32[]{:S(2)}, u32[]{:S(2)}) %all-to-all-start.2) | async-done | bytes 131104 | tf_op jit(solution)/shard_map/all_to_all | solution.py:20
  88.3 0.2 multiply_reduce_fusion
  88.6 0.3 divide_multiply_fusion
  89.1 0.2 multiply_exponential_fusion
  89.4 0.1 broadcast_multiply_fusion
  89.5 0.2 divide_multiply_fusion.2
  89.8 1.3 divide_multiply_fusion.1
  91.0 3.1 %multiply_add_fusion = f32[32,4,64,128]{3,2,1,0:T(8,128)S(1)} fusion(f32[32,4,64,128]{3,2,1,0:T(8,128)} %param.47, f32[32,128]{1,0:T(8,128)S(1)} %divide_multiply_fusion.2, f32[32,4,64]{2,1,0:T(4,128)S(1)} %broadcast_multiply_fusion, f32[32,4]{1,0:T(8,128)S(1)} %copy.68), kind=kLoop, calls=%fused_computation | loop fusion | flops 3145728 | bytes 8438272 | tf_op jit(solution)/shard_map/add | solution.py:142
  94.2 2.0 %copy-done.1 = f32[32,4,64,128]{3,2,1,0:T(8,128)} copy-done((f32[32,4,64,128]{3,2,1,0:T(8,128)}, f32[32,4,64,128]{3,2,1,0:T(8,128)S(1)}, u32[]{:S(2)}) %copy-start.1) | copy-done | bytes 4194328
  96.1 1.7 %fusion.21 = f32[32,1,4,64]{3,1,2,0:T(1,128)S(1)} fusion(f32[32,4,64,128]{3,2,1,0:T(8,128)S(1)} %multiply_add_fusion, f32[32,128,1,1]{1,2,3,0:T(1,128)S(1)} %bitcast.73), kind=kOutput, calls=%fused_computation.64 | convolution fusion | flops 2097152 | bytes 4243456 | tf_op jit(solution)/shard_map/bgrpn,bgn->bgrp/dot_general | solution.py:145
  97.9 0.1 fusion.18
  98.1 0.4 multiply_reduce_fusion.4
  98.5 0.3 convolution_convert_fusion
  98.9 8.5 %all_to_all.30 = bf16[8,4,2048]{2,1,0:T(4,128)(2,1)S(1)} all-to-all(bf16[8,4,2048]{2,1,0:T(4,128)(2,1)S(1)} %reshape.162), channel_id=1, replica_groups=mesh['kv'=32,'tp'=8] {'tp'}, dimensions={0} | all-to-all | bytes 262144 | tf_op jit(solution)/shard_map/all_to_all | solution.py:161
  107.5 1.0 broadcast_in_dim.17
  108.5 4.3 %all-to-all-start.4 = ((bf16[32,4,2048]{2,1,0:T(4,128)(2,1)}), bf16[32,4,2048]{2,1,0:T(4,128)(2,1)S(1)}, u32[]{:S(2)}, u32[]{:S(2)}) async-start(bf16[32,4,2048]{2,1,0:T(4,128)(2,1)} %broadcast_in_dim.17), calls=%async_computation.4 | async-start | bytes 1048576 | tf_op jit(solution)/shard_map/all_to_all | solution.py:20
  113.0 0.4 collective-permute-start.7
  113.3 1.8 %collective-permute-start.8 = (bf16[528,256]{1,0:T(8,128)(2,1)S(1)}, bf16[528,256]{1,0:T(8,128)(2,1)S(1)}, u32[]{:S(2)}, u32[]{:S(2)}) collective-permute-start(bf16[528,256]{1,0:T(8,128)(2,1)S(1)} %pad_maximum_fusion.1.refs_0_), channel_id=1, source_target_pairs={{0,4},{1,5},{2,6},{3,7},{4,0},{5,1},{6,2},{7,3},{8,12},{9,13},{10,... | collective-permute-start | bytes 811016 | tf_op jit(solution)/shard_map/ppermute | solution.py:38
  115.1 0.8 collective-permute-start.9
  115.9 1.8 %collective-permute-start.10 = (bf16[528,256]{1,0:T(8,128)(2,1)S(1)}, bf16[528,256]{1,0:T(8,128)(2,1)S(1)}, u32[]{:S(2)}, u32[]{:S(2)}) collective-permute-start(bf16[528,256]{1,0:T(8,128)(2,1)S(1)} %pad_maximum_fusion.1.refs_0_), channel_id=1, source_target_pairs={{0,1},{1,0},{2,3},{3,2},{4,5},{5,4},{6,7},{7,6},{8,9},{9,8},{10,11... | collective-permute-start | bytes 811016 | tf_op jit(solution)/shard_map/ppermute | solution.py:40
  117.7 4.1 %collective-permute-done.7.refs_1_ = bf16[528,256]{1,0:T(8,128)(2,1)S(1)} collective-permute-done((bf16[528,256]{1,0:T(8,128)(2,1)S(1)}, bf16[528,256]{1,0:T(8,128)(2,1)S(1)}, u32[]{:S(2)}, u32[]{:S(2)}) %collective-permute-start.7) | collective-permute-done | bytes 270368 | tf_op jit(solution)/shard_map/ppermute | solution.py:38
  121.8 7.2 %collective-permute-start.11 = (bf16[528,256]{1,0:T(8,128)(2,1)S(1)}, bf16[528,256]{1,0:T(8,128)(2,1)S(1)}, u32[]{:S(2)}, u32[]{:S(2)}) collective-permute-start(bf16[528,256]{1,0:T(8,128)(2,1)S(1)} %collective-permute-done.7.refs_1_), channel_id=1, source_target_pairs={{0,1},{1,0},{2,3},{3,2},{4,5},{5,4},{6,7},{7,6},{8,9},{9,8},{10,11... | collective-permute-start | bytes 811016 | tf_op jit(solution)/shard_map/ppermute | solution.py:40
  129.0 0.1 collective-permute-start.12
  129.1 0.5 collective-permute-start.13
  129.6 0.9 reshape.163.rows_ref
  130.6 0.5 collective-permute-done.13.refs_7_
  131.1 0.2 copy-done.14
  131.3 0.1 copy-done.18
  131.4 3.5 %ffn.3 = bf16[8,128,256]{2,1,0:T(8,128)(2,1)} custom-call(s32[1]{0:T(128)} %bitcast.tp_ref, bf16[128,2048]{1,0:T(8,128)(2,1)} %reshape.163.rows_ref, bf16[528,256]{1,0:T(8,128)(2,1)} %copy-done.3, bf16[528,256]{1,0:T(8,128)(2,1)} %copy-done.9, bf16[528,256]{1,0:T(8,128)(2,1)} %copy-done.11, bf16[528,256]{1,0:T(8,128)(2,1)} %copy-done.13, ...), custom_call_target="tpu_custom_call" | custom-call | tf_op jit(solution)/shard_map/ffn/pallas_call | solution.py:73
  134.9 1.3 reshape.169
  136.2 0.6 fusion.13
  136.8 0.4 copy.71
  137.2 31.4 %all_to_all.31 = bf16[256,4,256]{2,1,0:T(4,128)(2,1)S(1)} all-to-all(bf16[256,4,256]{2,1,0:T(4,128)(2,1)S(1)} %copy.71), channel_id=1, replica_groups=mesh['kv'=32,'tp'=8] {'kv','tp'}, dimensions={0} | all-to-all | bytes 1048576 | tf_op jit(solution)/shard_map/all_to_all | solution.py:247
  168.8 0.6 multiply_convert_fusion.5
  (111 shorter events, 1.5 us)
Async XLA Ops:
  0.6 97.9 %copy-start = (bf16[256,2048]{1,0:T(8,128)(2,1)S(1)}, bf16[256,2048]{1,0:T(8,128)(2,1)}, u32[]{:S(2)}) copy-start(bf16[256,2048]{1,0:T(8,128)(2,1)} %param.49) | copy-start | bytes 3145732
  2.5 39.4 %all-to-all-start = ((bf16[256,4,256]{2,1,0:T(4,128)(2,1)}), bf16[256,4,256]{2,1,0:T(4,128)(2,1)S(1)}, u32[]{:S(2)}, u32[]{:S(2)}) async-start(bf16[256,4,256]{2,1,0:T(4,128)(2,1)} %bitcast.1), calls=%async_computation | async-start | bytes 1048576 | tf_op jit(solution)/shard_map/all_to_all | solution.py:203
  20.7 22.8 %copy-start.2 = (bf16[528,256]{1,0:T(8,128)(2,1)}, bf16[528,256]{1,0:T(8,128)(2,1)S(1)}, u32[]{:S(2)}) copy-start(bf16[528,256]{1,0:T(8,128)(2,1)S(1)} %pad_maximum_fusion.refs_0_) | copy-start | bytes 811012
  20.7 11.2 %collective-permute-start = (bf16[528,256]{1,0:T(8,128)(2,1)S(1)}, bf16[528,256]{1,0:T(8,128)(2,1)S(1)}, u32[]{:S(2)}, u32[]{:S(2)}) collective-permute-start(bf16[528,256]{1,0:T(8,128)(2,1)S(1)} %pad_maximum_fusion.refs_0_), channel_id=1, source_target_pairs={{0,2},{1,3},{2,4},{3,5},{4,6},{5,7},{6,0},{7,1},{8,10},{9,11},{10,... | collective-permute-start | bytes 811016 | tf_op jit(solution)/shard_map/ppermute | solution.py:38
  22.1 18.7 %collective-permute-start.1 = (bf16[528,256]{1,0:T(8,128)(2,1)S(1)}, bf16[528,256]{1,0:T(8,128)(2,1)S(1)}, u32[]{:S(2)}, u32[]{:S(2)}) collective-permute-start(bf16[528,256]{1,0:T(8,128)(2,1)S(1)} %pad_maximum_fusion.refs_0_), channel_id=1, source_target_pairs={{0,4},{1,5},{2,6},{3,7},{4,0},{5,1},{6,2},{7,3},{8,12},{9,13},{10,... | collective-permute-start | bytes 811016 | tf_op jit(solution)/shard_map/ppermute | solution.py:38
  24.5 17.3 %collective-permute-start.2 = (bf16[528,256]{1,0:T(8,128)(2,1)S(1)}, bf16[528,256]{1,0:T(8,128)(2,1)S(1)}, u32[]{:S(2)}, u32[]{:S(2)}) collective-permute-start(bf16[528,256]{1,0:T(8,128)(2,1)S(1)} %pad_maximum_fusion.refs_0_), channel_id=1, source_target_pairs={{0,6},{1,7},{2,0},{3,1},{4,2},{5,3},{6,4},{7,5},{8,14},{9,15},{10,... | collective-permute-start | bytes 811016 | tf_op jit(solution)/shard_map/ppermute | solution.py:38
  25.7 17.3 %collective-permute-start.3 = (bf16[528,256]{1,0:T(8,128)(2,1)S(1)}, bf16[528,256]{1,0:T(8,128)(2,1)S(1)}, u32[]{:S(2)}, u32[]{:S(2)}) collective-permute-start(bf16[528,256]{1,0:T(8,128)(2,1)S(1)} %pad_maximum_fusion.refs_0_), channel_id=1, source_target_pairs={{0,1},{1,0},{2,3},{3,2},{4,5},{5,4},{6,7},{7,6},{8,9},{9,8},{10,11... | collective-permute-start | bytes 811016 | tf_op jit(solution)/shard_map/ppermute | solution.py:40
  31.9 11.6 %copy-start.7 = (bf16[528,256]{1,0:T(8,128)(2,1)}, bf16[528,256]{1,0:T(8,128)(2,1)S(1)}, u32[]{:S(2)}) copy-start(bf16[528,256]{1,0:T(8,128)(2,1)S(1)} %collective-permute-done.refs_1_) | copy-start | bytes 811012
  31.9 11.1 %collective-permute-start.4 = (bf16[528,256]{1,0:T(8,128)(2,1)S(1)}, bf16[528,256]{1,0:T(8,128)(2,1)S(1)}, u32[]{:S(2)}, u32[]{:S(2)}) collective-permute-start(bf16[528,256]{1,0:T(8,128)(2,1)S(1)} %collective-permute-done.refs_1_), channel_id=1, source_target_pairs={{0,1},{1,0},{2,3},{3,2},{4,5},{5,4},{6,7},{7,6},{8,9},{9,8},{10,11... | collective-permute-start | bytes 811016 | tf_op jit(solution)/shard_map/ppermute | solution.py:40
  40.9 2.6 %copy-start.8 = (bf16[528,256]{1,0:T(8,128)(2,1)}, bf16[528,256]{1,0:T(8,128)(2,1)S(1)}, u32[]{:S(2)}) copy-start(bf16[528,256]{1,0:T(8,128)(2,1)S(1)} %collective-permute-done.1.refs_2_) | copy-start | bytes 811012
  40.9 2.1 %collective-permute-start.5 = (bf16[528,256]{1,0:T(8,128)(2,1)S(1)}, bf16[528,256]{1,0:T(8,128)(2,1)S(1)}, u32[]{:S(2)}, u32[]{:S(2)}) collective-permute-start(bf16[528,256]{1,0:T(8,128)(2,1)S(1)} %collective-permute-done.1.refs_2_), channel_id=1, source_target_pairs={{0,1},{1,0},{2,3},{3,2},{4,5},{5,4},{6,7},{7,6},{8,9},{9,8},{10,11... | collective-permute-start | bytes 811016 | tf_op jit(solution)/shard_map/ppermute | solution.py:40
  41.8 1.7 %copy-start.10 = (bf16[528,256]{1,0:T(8,128)(2,1)}, bf16[528,256]{1,0:T(8,128)(2,1)S(1)}, u32[]{:S(2)}) copy-start(bf16[528,256]{1,0:T(8,128)(2,1)S(1)} %collective-permute-done.2.refs_3_) | copy-start | bytes 811012
  41.8 1.7 collective-permute-start.6
  43.0 0.7 copy-start.12
  43.0 0.8 copy-start.15
  43.0 0.9 copy-start.17
  43.9 15.4 %copy-start.25 = (bf16[4,256]{1,0:T(4,128)(2,1)S(1)}, bf16[4,256]{1,0:T(4,128)(2,1)}, u32[]{:S(2)}) copy-start(bf16[4,256]{1,0:T(4,128)(2,1)} %param.41) | copy-start | bytes 6148
  43.9 15.4 %copy-start.26 = (bf16[4,128]{1,0:T(4,128)(2,1)S(1)}, bf16[4,128]{1,0:T(4,128)(2,1)}, u32[]{:S(2)}) copy-start(bf16[4,128]{1,0:T(4,128)(2,1)} %param.42) | copy-start | bytes 3076
  43.9 15.5 %copy-start.27 = (bf16[4,128]{1,0:T(4,128)(2,1)S(1)}, bf16[4,128]{1,0:T(4,128)(2,1)}, u32[]{:S(2)}) copy-start(bf16[4,128]{1,0:T(4,128)(2,1)} %param.43) | copy-start | bytes 3076
  43.9 15.5 %copy-start.28 = (bf16[2048]{0:T(1024)(128)(2,1)S(1)}, bf16[2048]{0:T(1024)(128)(2,1)}, u32[]{:S(2)}) copy-start(bf16[2048]{0:T(1024)(128)(2,1)} %param.32) | copy-start | bytes 12292
  43.9 15.6 %copy-start.23 = (bf16[32,3,128]{2,0,1:T(8,128)(2,1)S(1)}, bf16[32,3,128]{2,0,1:T(8,128)(2,1)}, u32[]{:S(2)}) copy-start(bf16[32,3,128]{2,0,1:T(8,128)(2,1)} %param.45) | copy-start | bytes 73732
  43.9 39.1 %copy-start.22 = (bf16[32,3,256]{2,0,1:T(8,128)(2,1)S(1)}, bf16[32,3,256]{2,0,1:T(8,128)(2,1)}, u32[]{:S(2)}) copy-start(bf16[32,3,256]{2,0,1:T(8,128)(2,1)} %param.44) | copy-start | bytes 147460
  47.4 12.0 %copy-start.31 = (f32[4]{0:T(128)S(1)}, f32[4]{0:T(128)}, u32[]{:S(2)}) copy-start(f32[4]{0:T(128)} %param.39) | copy-start | bytes 52
  47.4 12.0 %copy-start.32 = (bf16[256]{0:T(256)(128)(2,1)S(1)}, bf16[256]{0:T(256)(128)(2,1)}, u32[]{:S(2)}) copy-start(bf16[256]{0:T(256)(128)(2,1)} %param.48) | copy-start | bytes 1540
  47.4 12.0 %copy-start.24 = (bf16[32,3,128]{2,0,1:T(8,128)(2,1)S(1)}, bf16[32,3,128]{2,0,1:T(8,128)(2,1)}, u32[]{:S(2)}) copy-start(bf16[32,3,128]{2,0,1:T(8,128)(2,1)} %param.46) | copy-start | bytes 73732
  47.4 41.2 %copy-start.4 = (bf16[2048,256]{1,0:T(8,128)(2,1)S(1)}, bf16[2048,256]{1,0:T(8,128)(2,1)}, u32[]{:S(2)}) copy-start(bf16[2048,256]{1,0:T(8,128)(2,1)} %param.34) | copy-start | bytes 3145732
  47.5 41.6 %copy-start.30 = (bf16[2048,4]{0,1:T(4,128)(2,1)S(1)}, bf16[2048,4]{0,1:T(4,128)(2,1)}, u32[]{:S(2)}) copy-start(bf16[2048,4]{0,1:T(4,128)(2,1)} %param.37) | copy-start | bytes 49156
  47.5 41.6 %copy-start.33 = (f32[4]{0:T(128)S(1)}, f32[4]{0:T(128)}, u32[]{:S(2)}) copy-start(f32[4]{0:T(128)} %param.38) | copy-start | bytes 52
  50.5 39.0 %copy-start.6 = (bf16[2048,128]{1,0:T(8,128)(2,1)S(1)}, bf16[2048,128]{1,0:T(8,128)(2,1)}, u32[]{:S(2)}) copy-start(bf16[2048,128]{1,0:T(8,128)(2,1)} %param.35) | copy-start | bytes 1572868
  50.5 25.4 %all-to-all-start.1 = ((bf16[32,4,2048]{2,1,0:T(4,128)(2,1)}), bf16[32,4,2048]{2,1,0:T(4,128)(2,1)S(1)}, u32[]{:S(2)}, u32[]{:S(2)}) async-start(bf16[32,4,2048]{2,1,0:T(4,128)(2,1)} %copy.65), calls=%async_computation.1 | async-start | bytes 1048576 | tf_op jit(solution)/shard_map/all_to_all | solution.py:214
  77.6 10.7 %all-to-all-start.2 = ((bf16[8,4,2048]{2,1,0:T(4,128)(2,1)}), bf16[8,4,2048]{2,1,0:T(4,128)(2,1)S(1)}, u32[]{:S(2)}, u32[]{:S(2)}) async-start(bf16[8,4,2048]{2,1,0:T(4,128)(2,1)} %broadcast_in_dim.16), calls=%async_computation.2 | async-start | bytes 262144 | tf_op jit(solution)/shard_map/all_to_all | solution.py:20
  94.1 2.0 %copy-start.1 = (f32[32,4,64,128]{3,2,1,0:T(8,128)}, f32[32,4,64,128]{3,2,1,0:T(8,128)S(1)}, u32[]{:S(2)}) copy-start(f32[32,4,64,128]{3,2,1,0:T(8,128)S(1)} %multiply_add_fusion) | copy-start | bytes 12582916
  94.1 3.7 %copy-start.29 = (f32[4]{0:T(128)S(1)}, f32[4]{0:T(128)}, u32[]{:S(2)}) copy-start(f32[4]{0:T(128)} %param.40) | copy-start | bytes 52
  94.1 3.9 %copy-start.5 = (bf16[2048,256]{1,0:T(8,128)(2,1)S(1)}, bf16[2048,256]{1,0:T(8,128)(2,1)}, u32[]{:S(2)}) copy-start(bf16[2048,256]{1,0:T(8,128)(2,1)} %param.33) | copy-start | bytes 3145732
  96.1 16.7 %copy-start.34 = (bf16[256]{0:T(256)(128)(2,1)S(1)}, bf16[256]{0:T(256)(128)(2,1)}, u32[]{:S(2)}) copy-start(bf16[256]{0:T(256)(128)(2,1)} %param.50) | copy-start | bytes 1540
  96.1 16.7 %copy-start.19 = (bf16[256,176]{0,1:T(8,128)(2,1)S(1)}, bf16[256,176]{0,1:T(8,128)(2,1)}, u32[]{:S(2)}) copy-start(bf16[256,176]{0,1:T(8,128)(2,1)} %param.51) | copy-start | bytes 270340
  96.1 16.7 %copy-start.20 = (bf16[256,176]{0,1:T(8,128)(2,1)S(1)}, bf16[256,176]{0,1:T(8,128)(2,1)}, u32[]{:S(2)}) copy-start(bf16[256,176]{0,1:T(8,128)(2,1)} %param.52) | copy-start | bytes 270340
  96.1 16.8 %copy-start.21 = (bf16[176,256]{1,0:T(8,128)(2,1)S(1)}, bf16[176,256]{1,0:T(8,128)(2,1)}, u32[]{:S(2)}) copy-start(bf16[176,256]{1,0:T(8,128)(2,1)} %param.53) | copy-start | bytes 270340
  108.5 21.1 %all-to-all-start.4 = ((bf16[32,4,2048]{2,1,0:T(4,128)(2,1)}), bf16[32,4,2048]{2,1,0:T(4,128)(2,1)S(1)}, u32[]{:S(2)}, u32[]{:S(2)}) async-start(bf16[32,4,2048]{2,1,0:T(4,128)(2,1)} %broadcast_in_dim.17), calls=%async_computation.4 | async-start | bytes 1048576 | tf_op jit(solution)/shard_map/all_to_all | solution.py:20
  113.0 18.1 %copy-start.3 = (bf16[528,256]{1,0:T(8,128)(2,1)}, bf16[528,256]{1,0:T(8,128)(2,1)S(1)}, u32[]{:S(2)}) copy-start(bf16[528,256]{1,0:T(8,128)(2,1)S(1)} %pad_maximum_fusion.1.refs_0_) | copy-start | bytes 811012
  113.0 8.8 %collective-permute-start.7 = (bf16[528,256]{1,0:T(8,128)(2,1)S(1)}, bf16[528,256]{1,0:T(8,128)(2,1)S(1)}, u32[]{:S(2)}, u32[]{:S(2)}) collective-permute-start(bf16[528,256]{1,0:T(8,128)(2,1)S(1)} %pad_maximum_fusion.1.refs_0_), channel_id=1, source_target_pairs={{0,2},{1,3},{2,4},{3,5},{4,6},{5,7},{6,0},{7,1},{8,10},{9,11},{10,... | collective-permute-start | bytes 811016 | tf_op jit(solution)/shard_map/ppermute | solution.py:38
  113.3 15.6 %collective-permute-start.8 = (bf16[528,256]{1,0:T(8,128)(2,1)S(1)}, bf16[528,256]{1,0:T(8,128)(2,1)S(1)}, u32[]{:S(2)}, u32[]{:S(2)}) collective-permute-start(bf16[528,256]{1,0:T(8,128)(2,1)S(1)} %pad_maximum_fusion.1.refs_0_), channel_id=1, source_target_pairs={{0,4},{1,5},{2,6},{3,7},{4,0},{5,1},{6,2},{7,3},{8,12},{9,13},{10,... | collective-permute-start | bytes 811016 | tf_op jit(solution)/shard_map/ppermute | solution.py:38
  115.1 13.9 %collective-permute-start.9 = (bf16[528,256]{1,0:T(8,128)(2,1)S(1)}, bf16[528,256]{1,0:T(8,128)(2,1)S(1)}, u32[]{:S(2)}, u32[]{:S(2)}) collective-permute-start(bf16[528,256]{1,0:T(8,128)(2,1)S(1)} %pad_maximum_fusion.1.refs_0_), channel_id=1, source_target_pairs={{0,6},{1,7},{2,0},{3,1},{4,2},{5,3},{6,4},{7,5},{8,14},{9,15},{10,... | collective-permute-start | bytes 811016 | tf_op jit(solution)/shard_map/ppermute | solution.py:38
  115.9 14.7 %collective-permute-start.10 = (bf16[528,256]{1,0:T(8,128)(2,1)S(1)}, bf16[528,256]{1,0:T(8,128)(2,1)S(1)}, u32[]{:S(2)}, u32[]{:S(2)}) collective-permute-start(bf16[528,256]{1,0:T(8,128)(2,1)S(1)} %pad_maximum_fusion.1.refs_0_), channel_id=1, source_target_pairs={{0,1},{1,0},{2,3},{3,2},{4,5},{5,4},{6,7},{7,6},{8,9},{9,8},{10,11... | collective-permute-start | bytes 811016 | tf_op jit(solution)/shard_map/ppermute | solution.py:40
  121.8 9.3 %copy-start.9 = (bf16[528,256]{1,0:T(8,128)(2,1)}, bf16[528,256]{1,0:T(8,128)(2,1)S(1)}, u32[]{:S(2)}) copy-start(bf16[528,256]{1,0:T(8,128)(2,1)S(1)} %collective-permute-done.7.refs_1_) | copy-start | bytes 811012
  121.8 8.8 %collective-permute-start.11 = (bf16[528,256]{1,0:T(8,128)(2,1)S(1)}, bf16[528,256]{1,0:T(8,128)(2,1)S(1)}, u32[]{:S(2)}, u32[]{:S(2)}) collective-permute-start(bf16[528,256]{1,0:T(8,128)(2,1)S(1)} %collective-permute-done.7.refs_1_), channel_id=1, source_target_pairs={{0,1},{1,0},{2,3},{3,2},{4,5},{5,4},{6,7},{7,6},{8,9},{9,8},{10,11... | collective-permute-start | bytes 811016 | tf_op jit(solution)/shard_map/ppermute | solution.py:40
  129.0 2.1 %copy-start.11 = (bf16[528,256]{1,0:T(8,128)(2,1)}, bf16[528,256]{1,0:T(8,128)(2,1)S(1)}, u32[]{:S(2)}) copy-start(bf16[528,256]{1,0:T(8,128)(2,1)S(1)} %collective-permute-done.8.refs_2_) | copy-start | bytes 811012
  129.0 1.6 collective-permute-start.12
  129.1 2.0 %copy-start.13 = (bf16[528,256]{1,0:T(8,128)(2,1)}, bf16[528,256]{1,0:T(8,128)(2,1)S(1)}, u32[]{:S(2)}) copy-start(bf16[528,256]{1,0:T(8,128)(2,1)S(1)} %collective-permute-done.9.refs_3_) | copy-start | bytes 811012
  129.1 2.0 %collective-permute-start.13 = (bf16[528,256]{1,0:T(8,128)(2,1)S(1)}, bf16[528,256]{1,0:T(8,128)(2,1)}, u32[]{:S(2)}, u32[]{:S(2)}) collective-permute-start(bf16[528,256]{1,0:T(8,128)(2,1)S(1)} %collective-permute-done.9.refs_3_), channel_id=1, source_target_pairs={{0,1},{1,0},{2,3},{3,2},{4,5},{5,4},{6,7},{7,6},{8,9},{9,8},{10,11... | collective-permute-start | bytes 811016 | tf_op jit(solution)/shard_map/ppermute | solution.py:40
  130.5 0.7 copy-start.14
  130.5 0.8 copy-start.16
  130.6 0.9 copy-start.18

commit v2 on v1

v2 whole, which is shorter than its diff:
```python
import jax
import jax.numpy as jnp
from jax import lax
from jax.experimental import pallas as pl
from jax.experimental.pallas import tpu as pltpu
from jax.sharding import Mesh
from jax.sharding import PartitionSpec as P

D = 2048
HEAD_DIM = 64
STATE = 128
FEATS = 256
HIDDEN = 176
ROWS = 4
Z, Y, TP = 8, 4, 8

KV_AXES = ("z", "y")
TP_AXES = ("x", "core")

norm_eps = 1e-06

by_rows = (((1,), (1,)), ((), ()))


def sent_to_all(array, axis):
    length = lax.axis_size(axis)
    return lax.all_to_all(
        jnp.broadcast_to(array[None], (length, *array.shape)), axis, 0, 0, tiled=True
    )


def inverse_rms(values):
    return lax.rsqrt(jnp.mean(values * values, axis=-1, keepdims=True) + norm_eps)


def weight_share(gain, gate_weight, lift_weight, down_weight):
    gain_f = gain.astype(jnp.float32)[None, :]
    gate_t = (gate_weight.T.astype(jnp.float32) * gain_f).astype(jnp.bfloat16)
    lift_t = (lift_weight.T.astype(jnp.float32) * gain_f).astype(jnp.bfloat16)
    return jnp.concatenate([gate_t, lift_t, down_weight], axis=0)


def hidden_units(normed_ref, weights, rows):
    gate = jnp.zeros((rows, HIDDEN), jnp.float32)
    lift = jnp.zeros((rows, HIDDEN), jnp.float32)
    for u in range(TP):
        block = normed_ref[u]
        gate += lax.dot_general(
            block, weights[u, :HIDDEN], by_rows, preferred_element_type=jnp.float32
        )
        lift += lax.dot_general(
            block, weights[u, HIDDEN : 2 * HIDDEN], by_rows, preferred_element_type=jnp.float32
        )
    return (gate * jax.nn.sigmoid(gate) * lift).astype(jnp.bfloat16)


def first_kernel(rows_ref, weights_ref, out_ref, normed_ref):
    blocks = Z * Y
    total = jnp.zeros((blocks, ROWS, 1), jnp.float32)
    for u in range(TP):
        values = rows_ref[:, u].astype(jnp.float32)
        total += jnp.sum(values * values, axis=-1, keepdims=True)
    factor = lax.rsqrt(total * (1.0 / D) + norm_eps)
    for u in range(TP):
        values = rows_ref[:, u].astype(jnp.float32) * factor
        normed_ref[u] = values.reshape(blocks * ROWS, FEATS).astype(jnp.bfloat16)
    hidden = hidden_units(normed_ref, weights_ref, blocks * ROWS)
    for u in range(TP):
        down = jnp.dot(hidden, weights_ref[u, 2 * HIDDEN :], preferred_element_type=jnp.float32)
        out_ref[:, u] = down.reshape(blocks, ROWS, FEATS).astype(jnp.bfloat16)


def first_partial(rows, weights):
    return pl.pallas_call(
        first_kernel,
        out_shape=jax.ShapeDtypeStruct(rows.shape, jnp.bfloat16),
        scratch_shapes=[pltpu.VMEM((TP, Z * Y * ROWS, FEATS), jnp.bfloat16)],
        name="first_ffn",
    )(rows, weights)


def second_kernel(place_ref, rows_ref, weights_ref, out_ref, normed_ref, sum_ref):
    step = pl.program_id(0)
    rows = Z * ROWS

    @pl.when(step == 0)
    def _():
        values = rows_ref[...].astype(jnp.float32)
        factor = lax.rsqrt(jnp.sum(values * values, axis=-1, keepdims=True) * (1.0 / D) + norm_eps)
        row = lax.broadcasted_iota(jnp.int32, (rows, 1), 0)
        own = jnp.where(row // ROWS == place_ref[0], 2.0, 0.0)
        for u in range(TP):
            block = values[:, u * FEATS : (u + 1) * FEATS]
            normed_ref[u] = (block * factor).astype(jnp.bfloat16)
            sum_ref[u] = block * own

    hidden = hidden_units(normed_ref, weights_ref.at[0], rows)
    for u in range(TP):
        down = jnp.dot(hidden, weights_ref[0, u, 2 * HIDDEN :], preferred_element_type=jnp.float32)
        sum_ref[u] = sum_ref[u] + down

    @pl.when(step == pl.num_programs(0) - 1)
    def _():
        out_ref[...] = sum_ref[...].reshape(TP, Z, ROWS, FEATS).astype(jnp.bfloat16)


def second_partial(rows, weights):
    place = lax.axis_index("z").astype(jnp.int32).reshape(1)
    return pl.pallas_call(
        second_kernel,
        grid=(Y,),
        out_shape=jax.ShapeDtypeStruct((TP, Z, ROWS, FEATS), jnp.bfloat16),
        in_specs=[
            pl.BlockSpec(memory_space=pltpu.SMEM),
            pl.BlockSpec(rows.shape, lambda i: (0, 0)),
            pl.BlockSpec((1, TP, 3 * HIDDEN, FEATS), lambda i: (i, 0, 0, 0)),
        ],
        out_specs=pl.BlockSpec((TP, Z, ROWS, FEATS), lambda i: (0, 0, 0, 0)),
        scratch_shapes=[
            pltpu.VMEM((TP, Z * ROWS, FEATS), jnp.bfloat16),
            pltpu.VMEM((TP, Z * ROWS, FEATS), jnp.float32),
        ],
        name="second_ffn",
    )(place, rows, weights)


def short_conv(tap_weights, buffer, newest):
    taps_f = tap_weights.astype(jnp.float32)
    summed = jnp.sum(buffer.astype(jnp.float32) * taps_f[None, :-1, :], axis=1)
    summed = summed + newest.astype(jnp.float32) * taps_f[-1][None, :]
    return jax.nn.silu(summed)


def state_mixer(
    residual,
    mixer_gain,
    proj_gate,
    proj_input,
    proj_write,
    proj_read,
    proj_step,
    step_bias,
    rate_log,
    skip_gain,
    taps_input,
    taps_write,
    taps_read,
    buffer_input,
    buffer_write,
    buffer_read,
    scan_state,
    group_gain,
    proj_output,
):
    full_rows = sent_to_all(residual, TP_AXES).transpose(0, 2, 1, 3).reshape(TP * ROWS, D)
    seq_rows = full_rows.shape[0]
    widened = full_rows.astype(jnp.float32)
    normed = (widened * inverse_rms(widened) * mixer_gain.astype(jnp.float32)[None, :]).astype(
        jnp.bfloat16
    )

    def state_project(weight):
        return jnp.dot(normed, weight, preferred_element_type=jnp.float32).astype(jnp.bfloat16)

    gate_z = state_project(proj_gate)
    input_new = state_project(proj_input)
    write_new = state_project(proj_write)
    read_new = state_project(proj_read)
    step_raw = state_project(proj_step)
    input_conv = short_conv(taps_input, buffer_input, input_new)
    write_conv = short_conv(taps_write, buffer_write, write_new)
    read_conv = short_conv(taps_read, buffer_read, read_new)
    head_count = proj_step.shape[1]
    group_count = proj_write.shape[1] // STATE
    per_group = head_count // group_count
    step = jax.nn.softplus(step_raw.astype(jnp.float32) + step_bias[None, :])
    retain = jnp.exp(-step * jnp.exp(rate_log)[None, :])
    input_heads = input_conv.reshape(seq_rows, group_count, per_group, HEAD_DIM)
    write_groups = write_conv.reshape(seq_rows, group_count, STATE)
    read_groups = read_conv.reshape(seq_rows, group_count, STATE)
    old_state = scan_state.reshape(seq_rows, group_count, per_group, HEAD_DIM, STATE)
    retain_g = retain.reshape(seq_rows, group_count, per_group)
    step_g = step.reshape(seq_rows, group_count, per_group)
    updated = (
        retain_g[..., None, None] * old_state
        + (step_g[..., None] * input_heads)[..., None] * write_groups[:, :, None, None, :]
    )
    head_out = jnp.einsum("bgrpn,bgn->bgrp", updated, read_groups)
    head_out = head_out + skip_gain.reshape(group_count, per_group)[None, :, :, None] * input_heads
    head_short = lax.optimization_barrier(head_out.astype(jnp.bfloat16))
    gated = head_short.astype(jnp.float32).reshape(seq_rows, group_count, per_group * HEAD_DIM)
    gated = gated * jax.nn.silu(
        gate_z.astype(jnp.float32).reshape(seq_rows, group_count, per_group * HEAD_DIM)
    )
    gated = (
        gated
        * inverse_rms(gated)
        * group_gain.astype(jnp.float32).reshape(group_count, per_group * HEAD_DIM)[None]
    )
    gated = gated.reshape(seq_rows, head_count * HEAD_DIM).astype(jnp.bfloat16)
    partial_out = jnp.dot(gated, proj_output, preferred_element_type=jnp.float32).astype(
        jnp.bfloat16
    )
    tiles = lax.all_to_all(partial_out.reshape(TP, ROWS, D), TP_AXES, 0, 0, tiled=True)
    mixed = jnp.sum(tiles.astype(jnp.float32), axis=0)
    own = residual.astype(jnp.float32).transpose(1, 0, 2).reshape(ROWS, D)
    mixed_rows = (own + mixed).astype(jnp.bfloat16)
    return (mixed_rows, updated.reshape(seq_rows, head_count, HEAD_DIM, STATE))


def per_device(
    residual,
    first_gain,
    first_gate,
    first_lift,
    first_down,
    mixer_gain,
    proj_gate,
    proj_input,
    proj_write,
    proj_read,
    proj_step,
    step_bias,
    rate_log,
    skip_gain,
    taps_input,
    taps_write,
    taps_read,
    buffer_input,
    buffer_write,
    buffer_read,
    scan_state,
    group_gain,
    proj_output,
    second_gain,
    second_gate,
    second_lift,
    second_down,
):
    weights_one = lax.all_gather(
        weight_share(first_gain, first_gate, first_lift, first_down), TP_AXES
    )
    weights_two = lax.all_gather(
        weight_share(second_gain, second_gate, second_lift, second_down), ("y", *TP_AXES)
    ).reshape(Y, TP, 3 * HIDDEN, FEATS)
    everyone = (*KV_AXES, *TP_AXES)

    split = residual.reshape(TP, ROWS, FEATS)
    tiles = lax.all_to_all(
        jnp.broadcast_to(split[None], (Z * Y, TP, ROWS, FEATS)).reshape(-1, ROWS, FEATS),
        everyone,
        0,
        0,
        tiled=True,
    ).reshape(Z * Y, TP, ROWS, FEATS)
    own_rows = lax.dynamic_index_in_dim(tiles, lax.axis_index(KV_AXES), 0, keepdims=False)
    share = first_partial(tiles, weights_one)
    share = lax.all_to_all(share, KV_AXES, 0, 0, tiled=True)
    branch = jnp.sum(share.astype(jnp.float32), axis=0)
    first = (own_rows.astype(jnp.float32) + 0.5 * branch).astype(jnp.bfloat16)

    mixed, state_out = state_mixer(
        first,
        mixer_gain,
        proj_gate,
        proj_input,
        proj_write,
        proj_read,
        proj_step,
        step_bias,
        rate_log,
        skip_gain,
        taps_input,
        taps_write,
        taps_read,
        buffer_input,
        buffer_write,
        buffer_read,
        scan_state,
        group_gain,
        proj_output,
    )

    rows = sent_to_all(mixed, "z").reshape(Z * ROWS, D)
    share = second_partial(rows, weights_two).transpose(1, 0, 2, 3)
    share = lax.all_to_all(
        share.reshape(-1, ROWS, FEATS), ("z", *TP_AXES), 0, 0, tiled=True
    ).reshape(Z, TP * ROWS, FEATS)
    residual_out = (0.5 * jnp.sum(share.astype(jnp.float32), axis=0)).astype(jnp.bfloat16)
    return (residual_out, state_out)


def solution(mesh):
    mesh = Mesh(mesh.devices.reshape(Z, Y, TP // 2, 2), (*KV_AXES, *TP_AXES))
    placed = (
        P(KV_AXES, TP_AXES),
        P(TP_AXES),
        P(TP_AXES, KV_AXES),
        P(TP_AXES, KV_AXES),
        P(KV_AXES, TP_AXES),
        P(),
        P(None, TP_AXES),
        P(None, TP_AXES),
        P(None, TP_AXES),
        P(None, TP_AXES),
        P(None, TP_AXES),
        P(TP_AXES),
        P(TP_AXES),
        P(TP_AXES),
        P(None, TP_AXES),
        P(None, TP_AXES),
        P(None, TP_AXES),
        P(KV_AXES, None, TP_AXES),
        P(KV_AXES, None, TP_AXES),
        P(KV_AXES, None, TP_AXES),
        P(KV_AXES, TP_AXES, None, None),
        P(TP_AXES),
        P(TP_AXES, None),
        P(TP_AXES),
        P(TP_AXES, KV_AXES),
        P(TP_AXES, KV_AXES),
        P(KV_AXES, TP_AXES),
    )
    return jax.shard_map(
        per_device,
        mesh=mesh,
        in_specs=placed,
        out_specs=(P(KV_AXES, TP_AXES), P(KV_AXES, TP_AXES, None, None)),
        check_vma=False,
    )
```

time: 170 us -> 155 us (0.912)
  starting transfers between devices: 56.7 us -> 15.5 us
  blocking collectives: 39.9 us -> 64.5 us
  between operations: 1.27 us -> 14.5 us
  waiting for transfers between devices: 37.9 us -> 26.1 us
  local copies, waits for them, and re-layouts: 13.7 us -> 6.82 us
  other arithmetic: 8.59 us -> 12.8 us
  Pallas kernels: 7 us -> 10.2 us
    all_to_all x2 -> x3, blocking collectives: 39.9 us -> 64.5 us  [the longest x1 35.4 us: per_device(): lax.all_to_all(jnp.broadcast_to(split[None], (Z * Y, TP, ROWS, FEATS)).re...]
    ppermute x14 -> x0, starting transfers between devices: 22.5 us -> none  [the longest x8 14.6 us: gathered_weights(): return pieces + [lax.ppermute(piece, 'tp', swap) for piece in pieces]]
    ppermute x14 -> x0, waiting for transfers between devices: 16.2 us -> none  [the longest x6 15.3 us: gathered_weights(): pieces = [own] + [lax.ppermute(own, 'tp', shift_perm(s)) for s in (2, 4, 6)]]
    all_to_all x2, starting transfers between devices: 24.4 us -> 9.97 us  [the longest x1 5.9 us: per_device(): share = lax.all_to_all(share, KV_AXES, 0, 0, tiled=True)]
    all_to_all x2, waiting for transfers between devices: 16.4 us -> 20.9 us  [the longest x1 16.3 us: per_device(): share = lax.all_to_all(share, KV_AXES, 0, 0, tiled=True)]
    all_to_all x2 -> x1, starting transfers between devices: 9.73 us -> 5.48 us  [sent_to_all(): lax.all_to_all(jnp.broadcast_to(array[None], (length, *array.shape)), axi...]
    pallas_call x2, Pallas kernels: 7 us -> 10.2 us  [the longest x1 6.48 us: second_partial(): pl.pallas_call(second_kernel, grid=(Y,), out_shape=jax.ShapeDtypeStruct((...]
    reshape x7 -> x3, local copies, waits for them, and re-layouts: 4.4 us -> 1.53 us  [the longest x1 0.73 us: state_mixer(): partial_out.reshape(TP, ROWS, D)]
  transfers between devices with their start and end apart: 18 -> 5, of which waited for: 7 -> 3; matrix products, arithmetic and copies ran while one was open for 3% -> 10% of each run, Pallas kernels for 0% -> 2%
where the time goes in v2:
time: 155 us; the launch traced here: 154 us
  blocking collectives  64.5 us (42%)
  waiting for transfers between devices  26.1 us (17%)
  starting transfers between devices  15.5 us (10%)
  between operations  14.5 us (9%)
  other arithmetic  12.8 us (8%)
  Pallas kernels  10.2 us (7%)
  local copies, waits for them, and re-layouts  6.82 us (4%)
  matrix products  3.35 us (2%)
    all_to_all x1, blocking collectives, per_device(): lax.all_to_all(jnp.broadcast_to(split[None], (Z * Y, TP, ROWS, FEATS)).re...  35.4 us
    all_to_all x1, blocking collectives, per_device(): lax.all_to_all(share.reshape(-1, ROWS, FEATS), ('z', *TP_AXES), 0, 0, til...  17 us
    all_to_all x1, waiting for transfers between devices, per_device(): share = lax.all_to_all(share, KV_AXES, 0, 0, tiled=True)  16.3 us
    all_to_all x1, blocking collectives, sent_to_all(): lax.all_to_all(jnp.broadcast_to(array[None], (length, *array.shape)), axi...  12 us
    pallas_call x1, Pallas kernels, second_partial(): pl.pallas_call(second_kernel, grid=(Y,), out_shape=jax.ShapeDtypeStruct((...  6.48 us
    all_to_all x1, starting transfers between devices, per_device(): share = lax.all_to_all(share, KV_AXES, 0, 0, tiled=True)  5.9 us
    all_to_all x1, starting transfers between devices, sent_to_all(): lax.all_to_all(jnp.broadcast_to(array[None], (length, *array.shape)), axi...  5.48 us
    all_to_all x1, waiting for transfers between devices, sent_to_all(): lax.all_to_all(jnp.broadcast_to(array[None], (length, *array.shape)), axi...  5.25 us
  transfers between devices with their start and end apart: 5, of which 3 were waited for; matrix products, arithmetic and copies ran while one was open for 10% of the time, Pallas kernels for 2%

profile of v2, /device:TPU:1, one launch (start us, length us, event | category | flops | bytes accessed | tf_op | source)
XLA Modules:
  0.0 153.8 jit_solution(12205739559151506700)
XLA Ops:
  7.2 0.0 copy-start
  7.2 0.0 copy-start.10
  7.2 0.0 copy-start.11
  7.2 0.0 copy-start.9
  7.2 0.0 copy-start.15
  7.2 0.0 copy-start.16
  7.3 0.0 all-gather.5.cloned.1.call-start
  7.3 0.7 convert_element_type.170
  8.0 1.0 fusion.12
  9.0 1.6 %pad_maximum_fusion = bf16[528,256]{1,0:T(8,128)(2,1)} fusion(bf16[176,256]{1,0:T(8,128)(2,1)} %param.31, bf16[176,256]{1,0:T(8,128)(2,1)S(1)} %get-tuple-element.5, bf16[176,256]{1,0:T(8,128)(2,1)S(1)} %get-tuple-element.4), kind=kLoop, calls=%fused_computation.20 | loop fusion | flops 811008 | bytes 540672 | tf_op jit(solution)/shard_map/concatenate | solution.py:40
  10.6 0.0 all-gather.5.cloned.1.call-update
  10.7 0.0 copy-start.6
  10.7 0.0 all-gather.7.cloned.1.call-start
  10.7 0.7 convert_element_type.210
  11.4 1.0 fusion.14
  12.3 1.6 %pad_maximum_fusion.1 = bf16[528,256]{1,0:T(8,128)(2,1)} fusion(bf16[176,256]{1,0:T(8,128)(2,1)} %param.53, bf16[176,256]{1,0:T(8,128)(2,1)S(1)} %get-tuple-element.3, bf16[176,256]{1,0:T(8,128)(2,1)S(1)} %get-tuple-element.2), kind=kLoop, calls=%fused_computation.21 | loop fusion | flops 811008 | bytes 540672 | tf_op jit(solution)/shard_map/concatenate | solution.py:40
  14.0 0.0 all-gather.7.cloned.1.call-update
  14.0 0.7 broadcast_in_dim.10
  14.7 0.0 copy-start.17
  14.7 0.2 broadcast_in_dim.11
  15.0 0.0 copy-start.2
  15.0 35.4 %all_to_all.30 = bf16[256,4,256]{2,1,0:T(4,128)(2,1)} all-to-all(bf16[256,4,256]{2,1,0:T(4,128)(2,1)S(1)} %bitcast.70), channel_id=1, replica_groups=mesh['z'=8,'y'=4,'x'=4,'core'=2] {'z','y','x','core'}, dimensions={0} | all-to-all | bytes 1048576 | tf_op jit(solution)/shard_map/all_to_all | solution.py:249
  50.4 3.7 %first_ffn.1 = bf16[32,8,4,256]{3,2,1,0:T(4,128)(2,1)} custom-call(bf16[32,8,4,256]{3,2,1,0:T(4,128)(2,1)} %bitcast.66, bf16[8,528,256]{2,1,0:T(8,128)(2,1)} %bitcast.69), custom_call_target="tpu_custom_call" | custom-call | tf_op jit(solution)/shard_map/first_ffn/pallas_call | solution.py:74
  54.2 5.9 %all-to-all-start.1 = ((bf16[32,8,4,256]{3,2,1,0:T(4,128)(2,1)}), bf16[32,8,4,256]{3,2,1,0:T(4,128)(2,1)S(1)}, u32[]{:S(2)}, u32[]{:S(2)}) async-start(bf16[32,8,4,256]{3,2,1,0:T(4,128)(2,1)} %first_ffn.1), calls=%async_computation.1 | async-start | bytes 1048576 | tf_op jit(solution)/shard_map/all_to_all | solution.py:258
  60.3 16.3 %all-to-all-done.1 = bf16[32,8,4,256]{3,2,1,0:T(4,128)(2,1)S(1)} async-done(((bf16[32,8,4,256]{3,2,1,0:T(4,128)(2,1)}), bf16[32,8,4,256]{3,2,1,0:T(4,128)(2,1)S(1)}, u32[]{:S(2)}, u32[]{:S(2)}) %all-to-all-start.1) | async-done | bytes 524320 | tf_op jit(solution)/shard_map/all_to_all | solution.py:258
  76.6 0.2 convert_reduce_fusion
  76.9 0.8 fusion.20
  77.7 0.7 broadcast_in_dim.13
  78.4 5.5 %all-to-all-start.2 = ((bf16[8,8,4,256]{3,1,2,0:T(8,128)(2,1)}), bf16[8,8,4,256]{3,1,2,0:T(8,128)(2,1)S(1)}, u32[]{:S(2)}, u32[]{:S(2)}) async-start(bf16[8,8,4,256]{3,1,2,0:T(8,128)(2,1)} %broadcast_in_dim.13), calls=%async_computation.2 | async-start | bytes 262144 | tf_op jit(solution)/shard_map/all_to_all | solution.py:27
  83.9 5.2 %all-to-all-done.2 = bf16[8,8,4,256]{3,1,2,0:T(8,128)(2,1)S(1)} async-done(((bf16[8,8,4,256]{3,1,2,0:T(8,128)(2,1)}), bf16[8,8,4,256]{3,1,2,0:T(8,128)(2,1)S(1)}, u32[]{:S(2)}, u32[]{:S(2)}) %all-to-all-start.2) | async-done | bytes 131104 | tf_op jit(solution)/shard_map/all_to_all | solution.py:27
  89.1 0.1 multiply_reduce_fusion
  89.3 0.1 rsqrt.20
  89.4 0.1 copy.47
  89.5 0.1 multiply_convert_fusion
  89.6 0.2 multiply_exponential_fusion
  89.7 0.1 copy.41
  89.8 0.1 copy.42
  89.9 0.3 divide_multiply_fusion
  90.3 0.1 reshape.163
  90.3 0.1 broadcast_multiply_fusion
  90.5 0.2 divide_multiply_fusion.1
  90.7 0.2 divide_multiply_fusion.2
  90.9 3.2 %multiply_add_fusion = f32[32,4,64,128]{3,2,1,0:T(8,128)S(1)} fusion(f32[32,4,64,128]{3,2,1,0:T(8,128)} %param.47, f32[32,128]{1,0:T(8,128)S(1)} %divide_multiply_fusion.2, f32[32,4,64]{2,1,0:T(4,128)S(1)} %broadcast_multiply_fusion, f32[32,4]{1,0:T(8,128)S(1)} %copy.41), kind=kLoop, calls=%fused_computation | loop fusion | flops 3145728 | bytes 8438272 | tf_op jit(solution)/shard_map/add | solution.py:185
  94.2 0.0 copy-start.1
  94.2 0.0 copy-start.13
  94.2 0.0 copy-start.3
  94.2 2.0 %copy-done.1 = f32[32,4,64,128]{3,2,1,0:T(8,128)} copy-done((f32[32,4,64,128]{3,2,1,0:T(8,128)}, f32[32,4,64,128]{3,2,1,0:T(8,128)S(1)}, u32[]{:S(2)}) %copy-start.1) | copy-done | bytes 4194328
  96.2 1.7 %fusion.24 = f32[32,1,4,64]{3,1,2,0:T(1,128)S(1)} fusion(f32[32,4,64,128]{3,2,1,0:T(8,128)S(1)} %multiply_add_fusion, f32[32,128,1,1]{1,2,3,0:T(1,128)S(1)} %bitcast.77), kind=kOutput, calls=%fused_computation.63 | convolution fusion | flops 2097152 | bytes 4243456 | tf_op jit(solution)/shard_map/bgrpn,bgn->bgrp/dot_general | solution.py:188
  97.9 0.1 fusion.19
  98.0 0.1 reshape.175
  98.1 0.4 multiply_reduce_fusion.4
  98.5 0.3 convolution_convert_fusion
  98.8 0.7 reshape.166
  99.6 4.1 %all-to-all-start.3 = ((bf16[8,4,2048]{2,1,0:T(4,128)(2,1)}), bf16[8,4,2048]{2,1,0:T(4,128)(2,1)S(1)}, u32[]{:S(2)}, u32[]{:S(2)}) async-start(bf16[8,4,2048]{2,1,0:T(4,128)(2,1)} %reshape.166), calls=%async_computation.3 | async-start | bytes 262144 | tf_op jit(solution)/shard_map/all_to_all | solution.py:204
  103.6 0.7 fusion.21
  104.4 4.5 %all-to-all-done.3 = bf16[8,4,2048]{2,1,0:T(4,128)(2,1)S(1)} async-done(((bf16[8,4,2048]{2,1,0:T(4,128)(2,1)}), bf16[8,4,2048]{2,1,0:T(4,128)(2,1)S(1)}, u32[]{:S(2)}, u32[]{:S(2)}) %all-to-all-start.3) | async-done | bytes 131104 | tf_op jit(solution)/shard_map/all_to_all | solution.py:204
  108.9 0.1 convert_reduce_fusion.1
  109.0 12.0 %all_to_all.31 = bf16[8,4,2048]{2,1,0:T(4,128)(2,1)S(1)} all-to-all(bf16[8,4,2048]{2,1,0:T(4,128)(2,1)S(1)} %broadcast_in_dim.14), channel_id=1, replica_groups=mesh['z'=8,'y'=4,'x'=4,'core'=2] {'z'}, dimensions={0} | all-to-all | bytes 262144 | tf_op jit(solution)/shard_map/all_to_all | solution.py:27
  121.1 0.7 reshape.167.rows_ref
  121.8 6.5 %second_ffn.1 = bf16[8,8,4,256]{3,2,1,0:T(4,128)(2,1)} custom-call(s32[1]{0:T(128)} %bitcast.place_ref, bf16[32,2048]{1,0:T(8,128)(2,1)} %reshape.167.rows_ref, bf16[4,8,528,256]{3,2,1,0:T(8,128)(2,1)} %bitcast.65), custom_call_target="tpu_custom_call" | custom-call | tf_op jit(solution)/shard_map/second_ffn/pallas_call | solution.py:109
  128.2 1.0 copy.49
  129.2 0.1 copy.44
  129.3 17.0 %all_to_all.32 = bf16[64,4,256]{2,1,0:T(4,128)(2,1)S(1)} all-to-all(bf16[64,4,256]{2,1,0:T(4,128)(2,1)S(1)} %copy.44), channel_id=1, replica_groups=mesh['z'=8,'y'=4,'x'=4,'core'=2] {'z','x','core'}, dimensions={0} | all-to-all | bytes 262144 | tf_op jit(solution)/shard_map/all_to_all | solution.py:286
  146.4 0.6 multiply_convert_fusion.5
  (47 shorter events, 0.3 us)
Async XLA Ops:
  7.2 91.3 %copy-start = (bf16[256,2048]{1,0:T(8,128)(2,1)S(1)}, bf16[256,2048]{1,0:T(8,128)(2,1)}, u32[]{:S(2)}) copy-start(bf16[256,2048]{1,0:T(8,128)(2,1)} %param.49) | copy-start | bytes 3145732
  7.2 52.9 %copy-start.10 = (bf16[4,128]{1,0:T(4,128)(2,1)S(1)}, bf16[4,128]{1,0:T(4,128)(2,1)}, u32[]{:S(2)}) copy-start(bf16[4,128]{1,0:T(4,128)(2,1)} %param.42) | copy-start | bytes 3076
  7.2 52.9 %copy-start.11 = (bf16[4,128]{1,0:T(4,128)(2,1)S(1)}, bf16[4,128]{1,0:T(4,128)(2,1)}, u32[]{:S(2)}) copy-start(bf16[4,128]{1,0:T(4,128)(2,1)} %param.43) | copy-start | bytes 3076
  7.2 52.9 %copy-start.9 = (bf16[4,256]{1,0:T(4,128)(2,1)S(1)}, bf16[4,256]{1,0:T(4,128)(2,1)}, u32[]{:S(2)}) copy-start(bf16[4,256]{1,0:T(4,128)(2,1)} %param.41) | copy-start | bytes 6148
  7.2 53.0 %copy-start.15 = (f32[4]{0:T(128)S(1)}, f32[4]{0:T(128)}, u32[]{:S(2)}) copy-start(f32[4]{0:T(128)} %param.39) | copy-start | bytes 52
  7.2 53.0 %copy-start.16 = (bf16[256]{0:T(256)(128)(2,1)S(1)}, bf16[256]{0:T(256)(128)(2,1)}, u32[]{:S(2)}) copy-start(bf16[256]{0:T(256)(128)(2,1)} %param.48) | copy-start | bytes 1540
  7.2 53.0 %copy-start.12 = (bf16[2048]{0:T(1024)(128)(2,1)S(1)}, bf16[2048]{0:T(1024)(128)(2,1)}, u32[]{:S(2)}) copy-start(bf16[2048]{0:T(1024)(128)(2,1)} %param.32) | copy-start | bytes 12292
  7.2 53.0 %copy-start.7 = (bf16[32,3,128]{2,0,1:T(8,128)(2,1)S(1)}, bf16[32,3,128]{2,0,1:T(8,128)(2,1)}, u32[]{:S(2)}) copy-start(bf16[32,3,128]{2,0,1:T(8,128)(2,1)} %param.46) | copy-start | bytes 73732
  7.3 53.0 %copy-start.8 = (bf16[32,3,128]{2,0,1:T(8,128)(2,1)S(1)}, bf16[32,3,128]{2,0,1:T(8,128)(2,1)}, u32[]{:S(2)}) copy-start(bf16[32,3,128]{2,0,1:T(8,128)(2,1)} %param.45) | copy-start | bytes 73732
  7.3 43.2 %all-gather.5.cloned.1.call-start = ((), (), s32[]{:S(2)}) async-start(), calls=%async_computation.6 | async-start | bytes 2433024 | tf_op jit(solution)/shard_map/all_gather | solution.py:240
  10.7 73.2 %copy-start.6 = (bf16[32,3,256]{2,0,1:T(8,128)(2,1)S(1)}, bf16[32,3,256]{2,0,1:T(8,128)(2,1)}, u32[]{:S(2)}) copy-start(bf16[32,3,256]{2,0,1:T(8,128)(2,1)} %param.44) | copy-start | bytes 147460
  10.7 111.1 %all-gather.7.cloned.1.call-start = ((), (), s32[]{:S(2)}) async-start(), calls=%async_computation.7 | async-start | bytes 8921088 | tf_op jit(solution)/shard_map/all_gather | solution.py:243
  14.7 74.9 %copy-start.14 = (bf16[2048,4]{0,1:T(4,128)(2,1)S(1)}, bf16[2048,4]{0,1:T(4,128)(2,1)}, u32[]{:S(2)}) copy-start(bf16[2048,4]{0,1:T(4,128)(2,1)} %param.37) | copy-start | bytes 49156
  14.7 74.9 %copy-start.17 = (f32[4]{0:T(128)S(1)}, f32[4]{0:T(128)}, u32[]{:S(2)}) copy-start(f32[4]{0:T(128)} %param.38) | copy-start | bytes 52
  15.0 75.0 %copy-start.2 = (bf16[2048,256]{1,0:T(8,128)(2,1)S(1)}, bf16[2048,256]{1,0:T(8,128)(2,1)}, u32[]{:S(2)}) copy-start(bf16[2048,256]{1,0:T(8,128)(2,1)} %param.34) | copy-start | bytes 3145732
  50.4 40.0 %copy-start.4 = (bf16[2048,128]{1,0:T(8,128)(2,1)S(1)}, bf16[2048,128]{1,0:T(8,128)(2,1)}, u32[]{:S(2)}) copy-start(bf16[2048,128]{1,0:T(8,128)(2,1)} %param.36) | copy-start | bytes 1572868
  54.2 22.5 %all-to-all-start.1 = ((bf16[32,8,4,256]{3,2,1,0:T(4,128)(2,1)}), bf16[32,8,4,256]{3,2,1,0:T(4,128)(2,1)S(1)}, u32[]{:S(2)}, u32[]{:S(2)}) async-start(bf16[32,8,4,256]{3,2,1,0:T(4,128)(2,1)} %first_ffn.1), calls=%async_computation.1 | async-start | bytes 1048576 | tf_op jit(solution)/shard_map/all_to_all | solution.py:258
  76.9 13.8 %copy-start.5 = (bf16[2048,128]{1,0:T(8,128)(2,1)S(1)}, bf16[2048,128]{1,0:T(8,128)(2,1)}, u32[]{:S(2)}) copy-start(bf16[2048,128]{1,0:T(8,128)(2,1)} %param.35) | copy-start | bytes 1572868
  78.4 10.8 %all-to-all-start.2 = ((bf16[8,8,4,256]{3,1,2,0:T(8,128)(2,1)}), bf16[8,8,4,256]{3,1,2,0:T(8,128)(2,1)S(1)}, u32[]{:S(2)}, u32[]{:S(2)}) async-start(bf16[8,8,4,256]{3,1,2,0:T(8,128)(2,1)} %broadcast_in_dim.13), calls=%async_computation.2 | async-start | bytes 262144 | tf_op jit(solution)/shard_map/all_to_all | solution.py:27
  94.2 2.0 %copy-start.1 = (f32[32,4,64,128]{3,2,1,0:T(8,128)}, f32[32,4,64,128]{3,2,1,0:T(8,128)S(1)}, u32[]{:S(2)}) copy-start(f32[32,4,64,128]{3,2,1,0:T(8,128)S(1)} %multiply_add_fusion) | copy-start | bytes 12582916
  94.2 3.7 %copy-start.13 = (f32[4]{0:T(128)S(1)}, f32[4]{0:T(128)}, u32[]{:S(2)}) copy-start(f32[4]{0:T(128)} %param.40) | copy-start | bytes 52
  94.2 3.9 %copy-start.3 = (bf16[2048,256]{1,0:T(8,128)(2,1)S(1)}, bf16[2048,256]{1,0:T(8,128)(2,1)}, u32[]{:S(2)}) copy-start(bf16[2048,256]{1,0:T(8,128)(2,1)} %param.33) | copy-start | bytes 3145732
  99.6 9.3 %all-to-all-start.3 = ((bf16[8,4,2048]{2,1,0:T(4,128)(2,1)}), bf16[8,4,2048]{2,1,0:T(4,128)(2,1)S(1)}, u32[]{:S(2)}, u32[]{:S(2)}) async-start(bf16[8,4,2048]{2,1,0:T(4,128)(2,1)} %reshape.166), calls=%async_computation.3 | async-start | bytes 262144 | tf_op jit(solution)/shard_map/all_to_all | solution.py:204
Sparse Core Ops, SparseCore 0:
  10.8 34.3 all-gather.4
  47.7 61.4 all-gather.6

commit v3 on v2

v3 whole, which is shorter than its diff:
```python
import jax
import jax.numpy as jnp
from jax import lax
from jax.experimental import pallas as pl
from jax.experimental.pallas import tpu as pltpu
from jax.sharding import Mesh
from jax.sharding import PartitionSpec as P

D = 2048
HEAD_DIM = 64
STATE = 128
FEATS = 256
HIDDEN = 176
ROWS = 4
Z, Y, TP = 8, 4, 8

KV_AXES = ("z", "y")
TP_AXES = ("x", "core")

norm_eps = 1e-06

by_rows = (((1,), (1,)), ((), ()))


def sent_to_all(array, axis):
    length = lax.axis_size(axis)
    return lax.all_to_all(
        jnp.broadcast_to(array[None], (length, *array.shape)), axis, 0, 0, tiled=True
    )


def inverse_rms(values):
    return lax.rsqrt(jnp.mean(values * values, axis=-1, keepdims=True) + norm_eps)


def share_kernel(*refs):
    for gain, gate, lift, down, out in (refs[0:4] + refs[8:9], refs[4:8] + refs[9:10]):
        gain_f = gain[...].astype(jnp.float32)
        out[:HIDDEN] = (gate[...].astype(jnp.float32) * gain_f).astype(jnp.bfloat16)
        out[HIDDEN : 2 * HIDDEN] = (lift[...].astype(jnp.float32) * gain_f).astype(jnp.bfloat16)
        out[2 * HIDDEN :] = down[...]


def weight_shares(*sets):
    operands = []
    for gain, gate_weight, lift_weight, down_weight in sets:
        operands += [gain.reshape(1, FEATS), gate_weight.T, lift_weight.T, down_weight]
    return pl.pallas_call(
        share_kernel,
        out_shape=[jax.ShapeDtypeStruct((3 * HIDDEN, FEATS), jnp.bfloat16)] * 2,
        name="shares",
    )(*operands)


def hidden_units(normed_ref, weights, rows):
    gate = jnp.zeros((rows, HIDDEN), jnp.float32)
    lift = jnp.zeros((rows, HIDDEN), jnp.float32)
    for u in range(TP):
        block = normed_ref[u]
        gate += lax.dot_general(
            block, weights[u, :HIDDEN], by_rows, preferred_element_type=jnp.float32
        )
        lift += lax.dot_general(
            block, weights[u, HIDDEN : 2 * HIDDEN], by_rows, preferred_element_type=jnp.float32
        )
    return (gate * jax.nn.sigmoid(gate) * lift).astype(jnp.bfloat16)


def first_kernel(rows_ref, weights_ref, out_ref, normed_ref):
    blocks = Z * Y
    total = jnp.zeros((blocks, ROWS, 1), jnp.float32)
    for u in range(TP):
        values = rows_ref[:, u].astype(jnp.float32)
        total += jnp.sum(values * values, axis=-1, keepdims=True)
    factor = lax.rsqrt(total * (1.0 / D) + norm_eps)
    for u in range(TP):
        values = rows_ref[:, u].astype(jnp.float32) * factor
        normed_ref[u] = values.reshape(blocks * ROWS, FEATS).astype(jnp.bfloat16)
    hidden = hidden_units(normed_ref, weights_ref, blocks * ROWS)
    for u in range(TP):
        down = jnp.dot(hidden, weights_ref[u, 2 * HIDDEN :], preferred_element_type=jnp.float32)
        out_ref[:, u] = down.reshape(blocks, ROWS, FEATS).astype(jnp.bfloat16)


def first_partial(rows, weights):
    return pl.pallas_call(
        first_kernel,
        out_shape=jax.ShapeDtypeStruct(rows.shape, jnp.bfloat16),
        scratch_shapes=[pltpu.VMEM((TP, Z * Y * ROWS, FEATS), jnp.bfloat16)],
        name="first_ffn",
    )(rows, weights)


def second_kernel(place_ref, rows_ref, weights_ref, out_ref, normed_ref, sum_ref):
    step = pl.program_id(0)
    rows = Z * ROWS

    @pl.when(step == 0)
    def _():
        values = rows_ref[...].astype(jnp.float32).reshape(rows, D)
        factor = lax.rsqrt(jnp.sum(values * values, axis=-1, keepdims=True) * (1.0 / D) + norm_eps)
        row = lax.broadcasted_iota(jnp.int32, (rows, 1), 0)
        own = jnp.where(row // ROWS == place_ref[0], 2.0, 0.0)
        for u in range(TP):
            block = values[:, u * FEATS : (u + 1) * FEATS]
            normed_ref[u] = (block * factor).astype(jnp.bfloat16)
            sum_ref[u] = block * own

    hidden = hidden_units(normed_ref, weights_ref.at[0], rows)
    for u in range(TP):
        down = jnp.dot(hidden, weights_ref[0, u, 2 * HIDDEN :], preferred_element_type=jnp.float32)
        sum_ref[u] = sum_ref[u] + down

    @pl.when(step == pl.num_programs(0) - 1)
    def _():
        for u in range(TP):
            out_ref[:, u] = sum_ref[u].reshape(Z, ROWS, FEATS).astype(jnp.bfloat16)


def second_partial(rows, weights):
    place = lax.axis_index("z").astype(jnp.int32).reshape(1)
    return pl.pallas_call(
        second_kernel,
        grid=(Y,),
        out_shape=jax.ShapeDtypeStruct((Z, TP, ROWS, FEATS), jnp.bfloat16),
        in_specs=[
            pl.BlockSpec(memory_space=pltpu.SMEM),
            pl.BlockSpec(rows.shape, lambda i: (0, 0, 0)),
            pl.BlockSpec((1, TP, 3 * HIDDEN, FEATS), lambda i: (i, 0, 0, 0)),
        ],
        out_specs=pl.BlockSpec((Z, TP, ROWS, FEATS), lambda i: (0, 0, 0, 0)),
        scratch_shapes=[
            pltpu.VMEM((TP, Z * ROWS, FEATS), jnp.bfloat16),
            pltpu.VMEM((TP, Z * ROWS, FEATS), jnp.float32),
        ],
        name="second_ffn",
    )(place, rows, weights)


def conv_silu(newest, buffer_ref, taps_ref):
    taps = taps_ref[...].astype(jnp.float32)
    summed = newest.astype(jnp.float32) * taps[3:4]
    for k in range(3):
        summed += buffer_ref[k].astype(jnp.float32) * taps[k : k + 1]
    return summed * jax.nn.sigmoid(summed)


SEQS = TP * ROWS
BLOCK = 8
CHANNELS = 256
PER_DEVICE = 4


def mixer_kernel(
    rows_ref,
    gain_ref,
    gate_ref,
    input_ref,
    write_ref,
    read_ref,
    step_ref,
    bias_ref,
    rate_ref,
    skip_ref,
    taps_input_ref,
    taps_write_ref,
    taps_read_ref,
    buffer_input_ref,
    buffer_write_ref,
    buffer_read_ref,
    state_ref,
    group_ref,
    output_ref,
    mixed_ref,
    new_state_ref,
    normed_ref,
    gate_z_ref,
    xc_ref,
    added_ref,
    retain_ref,
    bc_ref,
    rc_ref,
    out_cols_ref,
):
    i = pl.program_id(0)

    @pl.when(i == 0)
    def _():
        total = jnp.zeros((TP, ROWS, 1), jnp.float32)
        for u in range(TP):
            values = rows_ref[:, u].astype(jnp.float32)
            total += jnp.sum(values * values, axis=-1, keepdims=True)
        factor = lax.rsqrt(total * (1.0 / D) + norm_eps)
        for u in range(TP):
            values = (rows_ref[:, u].astype(jnp.float32) * factor).reshape(SEQS, FEATS)
            cols = slice(u * FEATS, (u + 1) * FEATS)
            gain = gain_ref[:, cols].astype(jnp.float32)
            normed_ref[:, cols] = (values * gain).astype(jnp.bfloat16)
        normed = normed_ref[...]

        def project(weight_ref):
            return jnp.dot(normed, weight_ref[...], preferred_element_type=jnp.float32).astype(
                jnp.bfloat16
            )

        gate_z_ref[...] = project(gate_ref)
        step_raw = lax.dot_general(
            normed, step_ref[...], by_rows, preferred_element_type=jnp.float32
        ).astype(jnp.bfloat16)
        xc = conv_silu(project(input_ref), buffer_input_ref, taps_input_ref)
        bc_ref[...] = conv_silu(project(write_ref), buffer_write_ref, taps_write_ref)
        rc_ref[...] = conv_silu(project(read_ref), buffer_read_ref, taps_read_ref)
        xc_ref[...] = xc
        step = jax.nn.softplus(step_raw.astype(jnp.float32) + bias_ref[...])
        retain = jnp.exp(-step * jnp.exp(rate_ref[...]))
        head = lax.broadcasted_iota(jnp.int32, (SEQS, CHANNELS), 1) // HEAD_DIM
        step_wide = jnp.zeros((SEQS, CHANNELS), jnp.float32)
        retain_wide = jnp.zeros((SEQS, CHANNELS), jnp.float32)
        for h in range(PER_DEVICE):
            step_wide = jnp.where(head == h, step[:, h : h + 1], step_wide)
            retain_wide = jnp.where(head == h, retain[:, h : h + 1], retain_wide)
        added = (step_wide * xc).T
        retain_cols = retain_wide.T
        for s in range(SEQS // BLOCK):
            added_ref[s] = added[:, s * BLOCK : (s + 1) * BLOCK]
            retain_ref[s] = retain_cols[:, s * BLOCK : (s + 1) * BLOCK]

    added = added_ref[i]
    retain = retain_ref[i]
    writes = bc_ref[pl.ds(pl.multiple_of(i * BLOCK, BLOCK), BLOCK)]
    reads = rc_ref[pl.ds(pl.multiple_of(i * BLOCK, BLOCK), BLOCK)]
    column = lax.broadcasted_iota(jnp.int32, (CHANNELS, BLOCK), 1)
    cols = jnp.zeros((CHANNELS, BLOCK), jnp.float32)
    for b in range(BLOCK):
        old = state_ref[b].reshape(CHANNELS, STATE)
        new = retain[:, b : b + 1] * old + added[:, b : b + 1] * writes[b : b + 1]
        new_state_ref[b] = new.reshape(PER_DEVICE, HEAD_DIM, STATE)
        read = jnp.sum(new * reads[b : b + 1], axis=-1, keepdims=True)
        cols = jnp.where(column == b, read, cols)
    out_cols_ref[i] = cols

    @pl.when(i == pl.num_programs(0) - 1)
    def _():
        cols = jnp.concatenate([out_cols_ref[s] for s in range(SEQS // BLOCK)], axis=1)
        head = lax.broadcasted_iota(jnp.int32, (1, CHANNELS), 1) // HEAD_DIM
        skip = jnp.zeros((1, CHANNELS), jnp.float32)
        for h in range(PER_DEVICE):
            skip = jnp.where(head == h, skip_ref[:, h : h + 1], skip)
        head_out = (cols.T + skip * xc_ref[...]).astype(jnp.bfloat16).astype(jnp.float32)
        gate_z = gate_z_ref[...].astype(jnp.float32)
        gated = head_out * (gate_z * jax.nn.sigmoid(gate_z))
        gated = gated * inverse_rms(gated) * group_ref[...].astype(jnp.float32)
        part = jnp.dot(
            gated.astype(jnp.bfloat16), output_ref[...], preferred_element_type=jnp.float32
        )
        mixed_ref[...] = part.reshape(TP, ROWS, D).astype(jnp.bfloat16)


def state_mixer(first, small, buffers, scan_state, group_gain, proj_output):
    rows = sent_to_all(first, TP_AXES)
    operands = [rows, *small, *[b.transpose(1, 0, 2) for b in buffers]]
    operands += [scan_state, group_gain.reshape(1, CHANNELS), proj_output]
    specs = [pl.BlockSpec(o.shape, lambda i, n=o.ndim: (0,) * n) for o in operands]
    state_spec = pl.BlockSpec((BLOCK, PER_DEVICE, HEAD_DIM, STATE), lambda i: (i, 0, 0, 0))
    specs[-3] = state_spec
    blocks = SEQS // BLOCK
    partial_out, state_out = pl.pallas_call(
        mixer_kernel,
        grid=(blocks,),
        out_shape=[
            jax.ShapeDtypeStruct((TP, ROWS, D), jnp.bfloat16),
            jax.ShapeDtypeStruct(scan_state.shape, jnp.float32),
        ],
        in_specs=specs,
        out_specs=[pl.BlockSpec((TP, ROWS, D), lambda i: (0, 0, 0)), state_spec],
        scratch_shapes=[
            pltpu.VMEM((SEQS, D), jnp.bfloat16),
            pltpu.VMEM((SEQS, CHANNELS), jnp.bfloat16),
            pltpu.VMEM((SEQS, CHANNELS), jnp.float32),
            pltpu.VMEM((blocks, CHANNELS, BLOCK), jnp.float32),
            pltpu.VMEM((blocks, CHANNELS, BLOCK), jnp.float32),
            pltpu.VMEM((SEQS, STATE), jnp.float32),
            pltpu.VMEM((SEQS, STATE), jnp.float32),
            pltpu.VMEM((blocks, CHANNELS, BLOCK), jnp.float32),
        ],
        name="mixer",
    )(*operands)
    tiles = lax.all_to_all(partial_out, TP_AXES, 0, 0, tiled=True)
    mixed = jnp.sum(tiles.astype(jnp.float32), axis=0)
    own = first.astype(jnp.float32).transpose(1, 0, 2).reshape(ROWS, D)
    return ((own + mixed).astype(jnp.bfloat16), state_out)


def per_device(
    residual,
    first_gain,
    first_gate,
    first_lift,
    first_down,
    mixer_gain,
    proj_gate,
    proj_input,
    proj_write,
    proj_read,
    proj_step,
    step_bias,
    rate_log,
    skip_gain,
    taps_input,
    taps_write,
    taps_read,
    buffer_input,
    buffer_write,
    buffer_read,
    scan_state,
    group_gain,
    proj_output,
    second_gain,
    second_gate,
    second_lift,
    second_down,
):
    share_one, share_two = weight_shares(
        (first_gain, first_gate, first_lift, first_down),
        (second_gain, second_gate, second_lift, second_down),
    )
    weights_one = lax.all_gather(share_one, TP_AXES)
    weights_two = lax.all_gather(share_two, ("y", *TP_AXES)).reshape(
        Y, TP, 3 * HIDDEN, FEATS
    )

    split = residual.reshape(TP, ROWS, FEATS)
    tiles = lax.all_to_all(
        jnp.broadcast_to(split[None], (Z, TP, ROWS, FEATS)).reshape(-1, ROWS, FEATS),
        ("z", *TP_AXES),
        0,
        0,
        tiled=True,
    )
    tiles = sent_to_all(tiles, "y").reshape(Y * Z, TP, ROWS, FEATS)
    own_rows = lax.dynamic_index_in_dim(tiles, lax.axis_index(("y", "z")), 0, keepdims=False)
    share = first_partial(tiles, weights_one)
    share = lax.all_to_all(share, ("y", "z"), 0, 0, tiled=True)
    branch = jnp.sum(share.astype(jnp.float32), axis=0)
    first = (own_rows.astype(jnp.float32) + 0.5 * branch).astype(jnp.bfloat16)

    mixed, state_out = state_mixer(
        first,
        (
            mixer_gain.reshape(1, D),
            proj_gate,
            proj_input,
            proj_write,
            proj_read,
            proj_step.T,
            step_bias.reshape(1, -1),
            rate_log.reshape(1, -1),
            skip_gain.reshape(1, -1),
            taps_input,
            taps_write,
            taps_read,
        ),
        (buffer_input, buffer_write, buffer_read),
        scan_state,
        group_gain,
        proj_output,
    )

    share = second_partial(sent_to_all(mixed, "z"), weights_two)
    share = lax.all_to_all(
        share.reshape(-1, ROWS, FEATS), ("z", *TP_AXES), 0, 0, tiled=True
    ).reshape(Z, TP * ROWS, FEATS)
    residual_out = (0.5 * jnp.sum(share.astype(jnp.float32), axis=0)).astype(jnp.bfloat16)
    return (residual_out, state_out)


def solution(mesh):
    mesh = Mesh(mesh.devices.reshape(Z, Y, TP // 2, 2), (*KV_AXES, *TP_AXES))
    placed = (
        P(KV_AXES, TP_AXES),
        P(TP_AXES),
        P(TP_AXES, KV_AXES),
        P(TP_AXES, KV_AXES),
        P(KV_AXES, TP_AXES),
        P(),
        P(None, TP_AXES),
        P(None, TP_AXES),
        P(None, TP_AXES),
        P(None, TP_AXES),
        P(None, TP_AXES),
        P(TP_AXES),
        P(TP_AXES),
        P(TP_AXES),
        P(None, TP_AXES),
        P(None, TP_AXES),
        P(None, TP_AXES),
        P(KV_AXES, None, TP_AXES),
        P(KV_AXES, None, TP_AXES),
        P(KV_AXES, None, TP_AXES),
        P(KV_AXES, TP_AXES, None, None),
        P(TP_AXES),
        P(TP_AXES, None),
        P(TP_AXES),
        P(TP_AXES, KV_AXES),
        P(TP_AXES, KV_AXES),
        P(KV_AXES, TP_AXES),
    )
    return jax.shard_map(
        per_device,
        mesh=mesh,
        in_specs=placed,
        out_specs=(P(KV_AXES, TP_AXES), P(KV_AXES, TP_AXES, None, None)),
        check_vma=False,
    )
```

time: 155 us -> 153 us (0.987)
  Pallas kernels: 10.2 us -> 23 us
  other arithmetic: 12.8 us -> 2.39 us
  waiting for transfers between devices: 26.1 us -> 22.2 us
  blocking collectives: 64.5 us -> 67.9 us
  matrix products: 3.35 us -> 0 us
    all_to_all x1 -> x2, blocking collectives: 12 us -> 26.3 us  [sent_to_all(): lax.all_to_all(jnp.broadcast_to(array[None], (length, *array.shape)), axi...]
    pallas_call x0 -> x2, Pallas kernels: none -> 12.8 us  [the longest x1 10.8 us: state_mixer(): pl.pallas_call(mixer_kernel, grid=(blocks,), out_shape=[jax.ShapeDtypeStr...]
    all_to_all x1, blocking collectives: 35.4 us -> 23.9 us  [per_device(): lax.all_to_all(jnp.broadcast_to(split[None], (Z, TP, ROWS, FEATS)).reshap...]
    convert_element_type x12 -> x1, other arithmetic: 3.57 us -> 0.01 us  [state_mixer(): return ((own + mixed).astype(jnp.bfloat16), state_out)]
    all_to_all x2, waiting for transfers between devices: 20.9 us -> 17.4 us  [the longest x1 12.9 us: per_device(): share = lax.all_to_all(share, ('y', 'z'), 0, 0, tiled=True)]
    dot_general x7 -> x0, matrix products: 3.35 us -> none  [the longest x1 1.71 us: state_mixer(): head_out = jnp.einsum('bgrpn,bgn->bgrp', updated, read_groups)]
    add x1 -> x0, other arithmetic: 3.23 us -> none  [state_mixer(): retain_g[..., None, None] * old_state]
    concatenate x2 -> x0, other arithmetic: 3.22 us -> none  [weight_share(): return jnp.concatenate([gate_t, lift_t, down_weight], axis=0)]
  transfers between devices with their start and end apart: 5 -> 5, of which waited for: 3 -> 3; matrix products, arithmetic and copies ran while one was open for 10% -> 3% of each run, Pallas kernels for 2% -> 10%
where the time goes in v3:
time: 153 us; the launch traced here: 152 us
  blocking collectives  67.9 us (44%)
  Pallas kernels  23 us (15%)
  waiting for transfers between devices  22.2 us (15%)
  starting transfers between devices  16.8 us (11%)
  between operations  14.1 us (9%)
  local copies, waits for them, and re-layouts  5.96 us (4%)
  other arithmetic  2.39 us (2%)
    all_to_all x2, blocking collectives, sent_to_all(): lax.all_to_all(jnp.broadcast_to(array[None], (length, *array.shape)), axi...  26.3 us
    all_to_all x1, blocking collectives, per_device(): lax.all_to_all(jnp.broadcast_to(split[None], (Z, TP, ROWS, FEATS)).reshap...  23.9 us
    all_to_all x1, blocking collectives, per_device(): lax.all_to_all(share.reshape(-1, ROWS, FEATS), ('z', *TP_AXES), 0, 0, til...  17.7 us
    all_to_all x1, waiting for transfers between devices, per_device(): share = lax.all_to_all(share, ('y', 'z'), 0, 0, tiled=True)  12.9 us
    pallas_call x1, Pallas kernels, state_mixer(): pl.pallas_call(mixer_kernel, grid=(blocks,), out_shape=[jax.ShapeDtypeStr...  10.8 us
    all_to_all x1, starting transfers between devices, sent_to_all(): lax.all_to_all(jnp.broadcast_to(array[None], (length, *array.shape)), axi...  8.64 us
    pallas_call x1, Pallas kernels, second_partial(): pl.pallas_call(second_kernel, grid=(Y,), out_shape=jax.ShapeDtypeStruct((...  6.5 us
    all_to_all x1, waiting for transfers between devices, state_mixer(): tiles = lax.all_to_all(partial_out, TP_AXES, 0, 0, tiled=True)  4.53 us
  transfers between devices with their start and end apart: 5, of which 3 were waited for; matrix products, arithmetic and copies ran while one was open for 3% of the time, Pallas kernels for 10%

profile of v3, /device:TPU:1, one launch (start us, length us, event | category | flops | bytes accessed | tf_op | source)
XLA Modules:
  0.0 152.3 jit_solution(14174575956984130348)
XLA Ops:
  7.2 0.0 all-gather.5.cloned.1.call-start
  7.2 1.2 reshape.73.refs_0_
  8.4 1.2 reshape.74.refs_4_
  9.7 0.0 copy-start.2
  9.7 0.0 copy-start.1
  9.7 2.0 %shares.1 = (bf16[528,256]{1,0:T(8,128)(2,1)}, bf16[528,256]{1,0:T(8,128)(2,1)}) custom-call(bf16[1,256]{1,0:T(2,128)(2,1)} %reshape.73.refs_0_, bf16[176,256]{1,0:T(8,128)(2,1)} %bitcast.42, bf16[176,256]{1,0:T(8,128)(2,1)} %bitcast.43, bf16[176,256]{1,0:T(8,128)(2,1)} %refs_3_.1, bf16[1,256]{1,0:T(2,128)(2,1)} %reshape.74.refs_4_, ...), custom_call_target="tpu_custom_call" | custom-call | tf_op jit(solution)/shard_map/shares/pallas_call | solution.py:48
  11.6 0.0 all-gather.5.cloned.1.call-update
  11.7 0.0 all-gather.7.cloned.1.call-start
  11.7 0.7 all-gather.7.cloned.1.call-update
  12.4 0.7 broadcast_in_dim.12
  13.2 23.9 %all_to_all.35 = bf16[64,4,256]{2,1,0:T(4,128)(2,1)S(1)} all-to-all(bf16[64,4,256]{2,1,0:T(4,128)(2,1)S(1)} %bitcast.40), channel_id=1, replica_groups=mesh['z'=8,'y'=4,'x'=4,'core'=2] {'z','x','core'}, dimensions={0} | all-to-all | bytes 262144 | tf_op jit(solution)/shard_map/all_to_all | solution.py:333
  37.1 0.1 broadcast_in_dim.14
  37.2 12.7 %all_to_all.36 = bf16[4,64,4,256]{3,2,1,0:T(4,128)(2,1)} all-to-all(bf16[4,64,4,256]{3,2,1,0:T(4,128)(2,1)S(1)} %broadcast_in_dim.14), channel_id=1, replica_groups=mesh['z'=8,'y'=4,'x'=4,'core'=2] {'y'}, dimensions={0} | all-to-all | bytes 1048576 | tf_op jit(solution)/shard_map/all_to_all | solution.py:27
  49.9 0.0 all-gather.5.cloned.1.call-done
  49.9 3.7 %first_ffn.1 = bf16[32,8,4,256]{3,2,1,0:T(4,128)(2,1)} custom-call(bf16[32,8,4,256]{3,2,1,0:T(4,128)(2,1)} %bitcast.35, bf16[8,528,256]{2,1,0:T(8,128)(2,1)} %bitcast.38), custom_call_target="tpu_custom_call" | custom-call | tf_op jit(solution)/shard_map/first_ffn/pallas_call | solution.py:86
  53.6 3.9 %all-to-all-start.2 = ((bf16[32,8,4,256]{3,2,1,0:T(4,128)(2,1)}), bf16[32,8,4,256]{3,2,1,0:T(4,128)(2,1)S(1)}, u32[]{:S(2)}, u32[]{:S(2)}) async-start(bf16[32,8,4,256]{3,2,1,0:T(4,128)(2,1)} %first_ffn.1), calls=%async_computation.2 | async-start | bytes 1048576 | tf_op jit(solution)/shard_map/all_to_all | solution.py:343
  57.5 12.9 %all-to-all-done.2 = bf16[32,8,4,256]{3,2,1,0:T(4,128)(2,1)S(1)} async-done(((bf16[32,8,4,256]{3,2,1,0:T(4,128)(2,1)}), bf16[32,8,4,256]{3,2,1,0:T(4,128)(2,1)S(1)}, u32[]{:S(2)}, u32[]{:S(2)}) %all-to-all-start.2) | async-done | bytes 524320 | tf_op jit(solution)/shard_map/all_to_all | solution.py:343
  70.4 0.2 convert_reduce_fusion
  70.6 0.7 fusion.3
  71.4 0.7 broadcast_in_dim.31
  72.1 8.6 %all-to-all-start.3 = ((bf16[8,8,4,256]{3,2,1,0:T(4,128)(2,1)}), bf16[8,8,4,256]{3,2,1,0:T(4,128)(2,1)S(1)}, u32[]{:S(2)}, u32[]{:S(2)}) async-start(bf16[8,8,4,256]{3,2,1,0:T(4,128)(2,1)} %broadcast_in_dim.31), calls=%async_computation.3 | async-start | bytes 262144 | tf_op jit(solution)/shard_map/all_to_all | solution.py:27
  80.7 0.0 copy-done.2
  80.7 0.6 reshape.81.group_ref
  81.3 0.0 copy-done.1
  81.3 0.6 reshape.77.gain_ref
  81.9 4.1 %all-to-all-done.3.rows_ref = bf16[8,8,4,256]{3,2,1,0:T(4,128)(2,1)S(1)} async-done(((bf16[8,8,4,256]{3,2,1,0:T(4,128)(2,1)}), bf16[8,8,4,256]{3,2,1,0:T(4,128)(2,1)S(1)}, u32[]{:S(2)}, u32[]{:S(2)}) %all-to-all-start.3) | async-done | bytes 131104 | tf_op jit(solution)/shard_map/all_to_all | solution.py:27
  86.0 0.0 copy-start
  86.0 0.6 copy-done
  86.6 10.8 %mixer.1 = (bf16[8,4,2048]{2,1,0:T(4,128)(2,1)}, f32[32,4,64,128]{3,2,1,0:T(8,128)}) custom-call(bf16[8,8,4,256]{3,2,1,0:T(4,128)(2,1)} %copy-done, bf16[1,2048]{1,0:T(2,128)(2,1)} %reshape.77.gain_ref, bf16[2048,256]{1,0:T(8,128)(2,1)} %gate_ref.1, bf16[2048,256]{1,0:T(8,128)(2,1)} %input_ref.1, bf16[2048,128]{1,0:T(8,128)(2,1)} %write_ref.1, ...), custom_call_target="tpu_custom_call" | custom-call | tf_op jit(solution)/shard_map/mixer/pallas_call | solution.py:267
  97.4 4.2 %all-to-all-start.4 = ((bf16[8,4,2048]{2,1,0:T(4,128)(2,1)}), bf16[8,4,2048]{2,1,0:T(4,128)(2,1)S(1)}, u32[]{:S(2)}, u32[]{:S(2)}) async-start(bf16[8,4,2048]{2,1,0:T(4,128)(2,1)} %get-tuple-element.7), calls=%async_computation.4 | async-start | bytes 262144 | tf_op jit(solution)/shard_map/all_to_all | solution.py:288
  101.6 0.7 fusion.4
  102.3 4.5 %all-to-all-done.4 = bf16[8,4,2048]{2,1,0:T(4,128)(2,1)S(1)} async-done(((bf16[8,4,2048]{2,1,0:T(4,128)(2,1)}), bf16[8,4,2048]{2,1,0:T(4,128)(2,1)S(1)}, u32[]{:S(2)}, u32[]{:S(2)}) %all-to-all-start.4) | async-done | bytes 131104 | tf_op jit(solution)/shard_map/all_to_all | solution.py:288
  106.8 0.1 convert_reduce_fusion.1
  107.0 13.6 %all_to_all.37.rows_ref = bf16[8,4,2048]{2,1,0:T(4,128)(2,1)} all-to-all(bf16[8,4,2048]{2,1,0:T(4,128)(2,1)S(1)} %broadcast_in_dim.32), channel_id=1, replica_groups=mesh['z'=8,'y'=4,'x'=4,'core'=2] {'z'}, dimensions={0} | all-to-all | bytes 262144 | tf_op jit(solution)/shard_map/all_to_all | solution.py:27
  120.6 0.0 all-gather.7.cloned.1.call-done
  120.6 6.5 %second_ffn.1 = bf16[8,8,4,256]{3,2,1,0:T(4,128)(2,1)} custom-call(s32[1]{0:T(128)} %bitcast.place_ref, bf16[8,4,2048]{2,1,0:T(4,128)(2,1)} %all_to_all.37.rows_ref, bf16[4,8,528,256]{3,2,1,0:T(8,128)(2,1)} %bitcast.34), custom_call_target="tpu_custom_call" | custom-call | tf_op jit(solution)/shard_map/second_ffn/pallas_call | solution.py:122
  127.1 17.7 %all_to_all.38 = bf16[64,4,256]{2,1,0:T(4,128)(2,1)S(1)} all-to-all(bf16[64,4,256]{2,1,0:T(4,128)(2,1)} %bitcast.39), channel_id=1, replica_groups=mesh['z'=8,'y'=4,'x'=4,'core'=2] {'z','x','core'}, dimensions={0} | all-to-all | bytes 262144 | tf_op jit(solution)/shard_map/all_to_all | solution.py:370
  144.9 0.6 multiply_convert_fusion
  (5 shorter events, 0.1 us)
Async XLA Ops:
  7.2 42.7 %all-gather.5.cloned.1.call-start = ((), (), s32[]{:S(2)}) async-start(), calls=%async_computation.7 | async-start | bytes 2433024 | tf_op jit(solution)/shard_map/all_gather | solution.py:327
  9.7 71.0 %copy-start.2 = (bf16[256]{0:T(256)(128)(2,1)S(1)}, bf16[256]{0:T(256)(128)(2,1)}, u32[]{:S(2)}) copy-start(bf16[256]{0:T(256)(128)(2,1)} %param.48) | copy-start | bytes 1540
  9.7 71.6 %copy-start.1 = (bf16[2048]{0:T(1024)(128)(2,1)S(1)}, bf16[2048]{0:T(1024)(128)(2,1)}, u32[]{:S(2)}) copy-start(bf16[2048]{0:T(1024)(128)(2,1)} %param.32) | copy-start | bytes 12292
  11.7 108.9 %all-gather.7.cloned.1.call-start = ((), (), s32[]{:S(2)}) async-start(), calls=%async_computation.8 | async-start | bytes 8921088 | tf_op jit(solution)/shard_map/all_gather | solution.py:328
  53.6 16.8 %all-to-all-start.2 = ((bf16[32,8,4,256]{3,2,1,0:T(4,128)(2,1)}), bf16[32,8,4,256]{3,2,1,0:T(4,128)(2,1)S(1)}, u32[]{:S(2)}, u32[]{:S(2)}) async-start(bf16[32,8,4,256]{3,2,1,0:T(4,128)(2,1)} %first_ffn.1), calls=%async_computation.2 | async-start | bytes 1048576 | tf_op jit(solution)/shard_map/all_to_all | solution.py:343
  72.1 13.9 %all-to-all-start.3 = ((bf16[8,8,4,256]{3,2,1,0:T(4,128)(2,1)}), bf16[8,8,4,256]{3,2,1,0:T(4,128)(2,1)S(1)}, u32[]{:S(2)}, u32[]{:S(2)}) async-start(bf16[8,8,4,256]{3,2,1,0:T(4,128)(2,1)} %broadcast_in_dim.31), calls=%async_computation.3 | async-start | bytes 262144 | tf_op jit(solution)/shard_map/all_to_all | solution.py:27
  86.0 0.7 copy-start
  97.4 9.4 %all-to-all-start.4 = ((bf16[8,4,2048]{2,1,0:T(4,128)(2,1)}), bf16[8,4,2048]{2,1,0:T(4,128)(2,1)S(1)}, u32[]{:S(2)}, u32[]{:S(2)}) async-start(bf16[8,4,2048]{2,1,0:T(4,128)(2,1)} %get-tuple-element.7), calls=%async_computation.4 | async-start | bytes 262144 | tf_op jit(solution)/shard_map/all_to_all | solution.py:288
Sparse Core Ops, SparseCore 0:
  11.8 32.7 all-gather.4
  47.2 60.2 all-gather.6

commit v4 on v3

--- a/solution.py
+++ b/solution.py
@@ -35,7 +35,7 @@
 
 def share_kernel(*refs):
     for gain, gate, lift, down, out in (refs[0:4] + refs[8:9], refs[4:8] + refs[9:10]):
-        gain_f = gain[...].astype(jnp.float32)
+        gain_f = gain[...].astype(jnp.float32).reshape(1, FEATS)
         out[:HIDDEN] = (gate[...].astype(jnp.float32) * gain_f).astype(jnp.bfloat16)
         out[HIDDEN : 2 * HIDDEN] = (lift[...].astype(jnp.float32) * gain_f).astype(jnp.bfloat16)
         out[2 * HIDDEN :] = down[...]
@@ -44,10 +44,11 @@
 def weight_shares(*sets):
     operands = []
     for gain, gate_weight, lift_weight, down_weight in sets:
-        operands += [gain.reshape(1, FEATS), gate_weight.T, lift_weight.T, down_weight]
+        operands += [gain, gate_weight.T, lift_weight.T, down_weight]
     return pl.pallas_call(
         share_kernel,
         out_shape=[jax.ShapeDtypeStruct((3 * HIDDEN, FEATS), jnp.bfloat16)] * 2,
+        compiler_params=pltpu.CompilerParams(vmem_limit_bytes=24 << 20),
         name="shares",
     )(*operands)
 
@@ -87,6 +88,7 @@
         first_kernel,
         out_shape=jax.ShapeDtypeStruct(rows.shape, jnp.bfloat16),
         scratch_shapes=[pltpu.VMEM((TP, Z * Y * ROWS, FEATS), jnp.bfloat16)],
+        compiler_params=pltpu.CompilerParams(vmem_limit_bytes=24 << 20),
         name="first_ffn",
     )(rows, weights)
 
@@ -194,7 +196,7 @@
         for u in range(TP):
             values = (rows_ref[:, u].astype(jnp.float32) * factor).reshape(SEQS, FEATS)
             cols = slice(u * FEATS, (u + 1) * FEATS)
-            gain = gain_ref[:, cols].astype(jnp.float32)
+            gain = gain_ref[cols].astype(jnp.float32).reshape(1, FEATS)
             normed_ref[:, cols] = (values * gain).astype(jnp.bfloat16)
         normed = normed_ref[...]
 
@@ -211,8 +213,8 @@
         bc_ref[...] = conv_silu(project(write_ref), buffer_write_ref, taps_write_ref)
         rc_ref[...] = conv_silu(project(read_ref), buffer_read_ref, taps_read_ref)
         xc_ref[...] = xc
-        step = jax.nn.softplus(step_raw.astype(jnp.float32) + bias_ref[...])
-        retain = jnp.exp(-step * jnp.exp(rate_ref[...]))
+        step = jax.nn.softplus(step_raw.astype(jnp.float32) + bias_ref[...].reshape(1, PER_DEVICE))
+        retain = jnp.exp(-step * jnp.exp(rate_ref[...].reshape(1, PER_DEVICE)))
         head = lax.broadcasted_iota(jnp.int32, (SEQS, CHANNELS), 1) // HEAD_DIM
         step_wide = jnp.zeros((SEQS, CHANNELS), jnp.float32)
         retain_wide = jnp.zeros((SEQS, CHANNELS), jnp.float32)
@@ -228,14 +230,22 @@
     added = added_ref[i]
     retain = retain_ref[i]
     writes = bc_ref[pl.ds(pl.multiple_of(i * BLOCK, BLOCK), BLOCK)]
-    reads = rc_ref[pl.ds(pl.multiple_of(i * BLOCK, BLOCK), BLOCK)]
+    reads = rc_ref[pl.ds(pl.multiple_of(i * BLOCK, BLOCK), BLOCK)].astype(jnp.bfloat16)
     column = lax.broadcasted_iota(jnp.int32, (CHANNELS, BLOCK), 1)
     cols = jnp.zeros((CHANNELS, BLOCK), jnp.float32)
     for b in range(BLOCK):
-        old = state_ref[b].reshape(CHANNELS, STATE)
-        new = retain[:, b : b + 1] * old + added[:, b : b + 1] * writes[b : b + 1]
-        new_state_ref[b] = new.reshape(PER_DEVICE, HEAD_DIM, STATE)
-        read = jnp.sum(new * reads[b : b + 1], axis=-1, keepdims=True)
+        new = []
+        for h in range(PER_DEVICE):
+            top = h * HEAD_DIM
+            kept = jnp.broadcast_to(retain[top : top + 8, b : b + 1], (8, STATE))
+            old = state_ref[b, h].reshape(HEAD_DIM // 8, 8, STATE) * kept[None]
+            new.append(
+                old.reshape(HEAD_DIM, STATE)
+                + added[top : top + HEAD_DIM, b : b + 1] * writes[b : b + 1]
+            )
+            new_state_ref[b, h] = new[h]
+        new = jnp.concatenate(new, axis=0).astype(jnp.bfloat16)
+        read = lax.dot_general(new, reads, by_rows, preferred_element_type=jnp.float32)
         cols = jnp.where(column == b, read, cols)
     out_cols_ref[i] = cols
 
@@ -243,13 +253,14 @@
     def _():
         cols = jnp.concatenate([out_cols_ref[s] for s in range(SEQS // BLOCK)], axis=1)
         head = lax.broadcasted_iota(jnp.int32, (1, CHANNELS), 1) // HEAD_DIM
+        skip_own = skip_ref[...].reshape(1, PER_DEVICE)
         skip = jnp.zeros((1, CHANNELS), jnp.float32)
         for h in range(PER_DEVICE):
-            skip = jnp.where(head == h, skip_ref[:, h : h + 1], skip)
+            skip = jnp.where(head == h, skip_own[:, h : h + 1], skip)
         head_out = (cols.T + skip * xc_ref[...]).astype(jnp.bfloat16).astype(jnp.float32)
         gate_z = gate_z_ref[...].astype(jnp.float32)
         gated = head_out * (gate_z * jax.nn.sigmoid(gate_z))
-        gated = gated * inverse_rms(gated) * group_ref[...].astype(jnp.float32)
+        gated = gated * inverse_rms(gated) * group_ref[...].astype(jnp.float32).reshape(1, CHANNELS)
         part = jnp.dot(
             gated.astype(jnp.bfloat16), output_ref[...], preferred_element_type=jnp.float32
         )
@@ -259,10 +270,15 @@
 def state_mixer(first, small, buffers, scan_state, group_gain, proj_output):
     rows = sent_to_all(first, TP_AXES)
     operands = [rows, *small, *[b.transpose(1, 0, 2) for b in buffers]]
-    operands += [scan_state, group_gain.reshape(1, CHANNELS), proj_output]
-    specs = [pl.BlockSpec(o.shape, lambda i, n=o.ndim: (0,) * n) for o in operands]
+    operands += [scan_state, group_gain, proj_output]
+    state_place = len(operands) - 3
+    operands = [
+        o if n == state_place else pltpu.with_memory_space_constraint(o, pltpu.VMEM)
+        for n, o in enumerate(operands)
+    ]
+    specs = [pl.BlockSpec(memory_space=pltpu.VMEM) for _ in operands]
     state_spec = pl.BlockSpec((BLOCK, PER_DEVICE, HEAD_DIM, STATE), lambda i: (i, 0, 0, 0))
-    specs[-3] = state_spec
+    specs[state_place] = state_spec
     blocks = SEQS // BLOCK
     partial_out, state_out = pl.pallas_call(
         mixer_kernel,
@@ -283,6 +299,7 @@
             pltpu.VMEM((SEQS, STATE), jnp.float32),
             pltpu.VMEM((blocks, CHANNELS, BLOCK), jnp.float32),
         ],
+        compiler_params=pltpu.CompilerParams(vmem_limit_bytes=24 << 20),
         name="mixer",
     )(*operands)
     tiles = lax.all_to_all(partial_out, TP_AXES, 0, 0, tiled=True)
@@ -331,31 +348,30 @@
 
     split = residual.reshape(TP, ROWS, FEATS)
     tiles = lax.all_to_all(
-        jnp.broadcast_to(split[None], (Z, TP, ROWS, FEATS)).reshape(-1, ROWS, FEATS),
-        ("z", *TP_AXES),
+        jnp.broadcast_to(split[None], (Z * Y, TP, ROWS, FEATS)).reshape(-1, ROWS, FEATS),
+        (*KV_AXES, *TP_AXES),
         0,
         0,
         tiled=True,
-    )
-    tiles = sent_to_all(tiles, "y").reshape(Y * Z, TP, ROWS, FEATS)
-    own_rows = lax.dynamic_index_in_dim(tiles, lax.axis_index(("y", "z")), 0, keepdims=False)
+    ).reshape(Z * Y, TP, ROWS, FEATS)
+    own_rows = lax.dynamic_index_in_dim(tiles, lax.axis_index(KV_AXES), 0, keepdims=False)
     share = first_partial(tiles, weights_one)
-    share = lax.all_to_all(share, ("y", "z"), 0, 0, tiled=True)
+    share = lax.all_to_all(share, KV_AXES, 0, 0, tiled=True)
     branch = jnp.sum(share.astype(jnp.float32), axis=0)
     first = (own_rows.astype(jnp.float32) + 0.5 * branch).astype(jnp.bfloat16)
 
     mixed, state_out = state_mixer(
         first,
         (
-            mixer_gain.reshape(1, D),
+            mixer_gain,
             proj_gate,
             proj_input,
             proj_write,
             proj_read,
             proj_step.T,
-            step_bias.reshape(1, -1),
-            rate_log.reshape(1, -1),
-            skip_gain.reshape(1, -1),
+            step_bias,
+            rate_log,
+            skip_gain,
             taps_input,
             taps_write,
             taps_read,

time: 153 us -> 158 us (1.033)
  Pallas kernels: 23 us -> 14.4 us
  local copies, waits for them, and re-layouts: 5.96 us -> 14 us
  blocking collectives: 67.9 us -> 75.2 us
  starting transfers between devices: 16.8 us -> 13 us
  waiting for transfers between devices: 22.2 us -> 23.8 us
    unnamed x6 -> x54, local copies, waits for them, and re-layouts: 0.66 us -> 12.9 us
    all_to_all x1, blocking collectives: 23.9 us -> 35.3 us  [per_device(): lax.all_to_all(jnp.broadcast_to(split[None], (Z * Y, TP, ROWS, FEATS)).re...]
    pallas_call x1, Pallas kernels: 10.8 us -> 5.1 us  [state_mixer(): pl.pallas_call(mixer_kernel, grid=(blocks,), out_shape=[jax.ShapeDtypeStr...]
    all_to_all x2, blocking collectives: 26.3 us -> 22 us  [sent_to_all(): lax.all_to_all(jnp.broadcast_to(array[None], (length, *array.shape)), axi...]
    all_to_all x2 -> x1, starting transfers between devices: 12.5 us -> 8.78 us  [per_device(): share = lax.all_to_all(share, KV_AXES, 0, 0, tiled=True)]
    reshape x4 -> x0, local copies, waits for them, and re-layouts: 3.64 us -> none  [the longest x2 2.46 us: weight_shares(): gain.reshape(1, FEATS)]
    all_to_all x1, waiting for transfers between devices: 4.53 us -> 6.56 us  [state_mixer(): tiles = lax.all_to_all(partial_out, TP_AXES, 0, 0, tiled=True)]
    pallas_call x1, Pallas kernels: 3.7 us -> 1.91 us  [first_partial(): pl.pallas_call(first_kernel, out_shape=jax.ShapeDtypeStruct(rows.shape, j...]
  transfers between devices with their start and end apart: 5 -> 4, of which waited for: 3 -> 2; matrix products, arithmetic and copies ran while one was open for 3% -> 2% of each run, Pallas kernels for 10% -> 4%
where the time goes in v4:
time: 158 us; the launch traced here: 157 us
  blocking collectives  75.2 us (48%)
  waiting for transfers between devices  23.8 us (15%)
  Pallas kernels  14.4 us (9%)
  between operations  14.3 us (9%)
  local copies, waits for them, and re-layouts  14 us (9%)
  starting transfers between devices  13 us (8%)
  other arithmetic  2.01 us (1%)
    all_to_all x1, blocking collectives, per_device(): lax.all_to_all(jnp.broadcast_to(split[None], (Z * Y, TP, ROWS, FEATS)).re...  35.3 us
    all_to_all x2, blocking collectives, sent_to_all(): lax.all_to_all(jnp.broadcast_to(array[None], (length, *array.shape)), axi...  22 us
    all_to_all x1, blocking collectives, per_device(): lax.all_to_all(share.reshape(-1, ROWS, FEATS), ('z', *TP_AXES), 0, 0, til...  17.8 us
    all_to_all x1, waiting for transfers between devices, per_device(): share = lax.all_to_all(share, KV_AXES, 0, 0, tiled=True)  16.5 us
    unnamed x54, local copies, waits for them, and re-layouts  12.9 us
    all_to_all x1, starting transfers between devices, per_device(): share = lax.all_to_all(share, KV_AXES, 0, 0, tiled=True)  8.78 us
    all_to_all x1, waiting for transfers between devices, state_mixer(): tiles = lax.all_to_all(partial_out, TP_AXES, 0, 0, tiled=True)  6.56 us
    pallas_call x1, Pallas kernels, second_partial(): pl.pallas_call(second_kernel, grid=(Y,), out_shape=jax.ShapeDtypeStruct((...  6.51 us
  transfers between devices with their start and end apart: 4, of which 2 were waited for; matrix products, arithmetic and copies ran while one was open for 2% of the time, Pallas kernels for 4%

profile of v4, /device:TPU:1, one launch (start us, length us, event | category | flops | bytes accessed | tf_op | source)
XLA Modules:
  0.0 156.7 jit_solution(16716031604120301162)
XLA Ops:
  7.2 0.0 copy-start.5
  7.2 0.0 copy-start.3
  7.2 0.0 copy-start.2
  7.2 0.0 all-gather.5.cloned.1.call-start
  7.2 0.0 copy-start.7
  7.3 1.0 copy-done.7
  8.3 0.0 copy-start.8
  8.3 0.9 copy-done.8
  9.2 0.0 copy-start.9
  9.2 0.9 copy-done.9
  10.1 0.0 copy-start.10
  10.1 0.9 copy-done.10
  11.0 0.0 copy-start.11
  11.0 0.9 copy-done.11
  11.9 0.0 copy-start.12
  11.9 0.9 copy-done.12
  12.7 0.7 copy-done.25
  13.4 0.7 copy-done.26
  14.1 0.0 copy-start.18
  14.1 0.0 copy-start.19
  14.1 0.0 copy-start.20
  14.1 0.0 copy-start.21
  14.1 0.0 copy-start.22
  14.1 0.0 copy-start.23
  14.1 0.8 shares.1
  15.0 0.0 all-gather.5.cloned.1.call-update
  15.0 0.0 all-gather.7.cloned.1.call-start
  15.0 0.7 all-gather.7.cloned.1.call-update
  15.7 0.7 broadcast_in_dim.10
  16.5 0.2 broadcast_in_dim.22
  16.7 35.3 %all_to_all.30 = bf16[256,4,256]{2,1,0:T(4,128)(2,1)S(1)} all-to-all(bf16[256,4,256]{2,1,0:T(4,128)(2,1)S(1)} %bitcast.44), channel_id=1, replica_groups=mesh['z'=8,'y'=4,'x'=4,'core'=2] {'z','y','x','core'}, dimensions={0} | all-to-all | bytes 1048576 | tf_op jit(solution)/shard_map/all_to_all | solution.py:350
  52.1 1.6 %copy-done.1 = bf16[4224,256]{1,0:T(8,128)(2,1)S(1)} copy-done((bf16[4224,256]{1,0:T(8,128)(2,1)S(1)}, bf16[4224,256]{1,0:T(8,128)(2,1)}, u32[]{:S(2)}) %copy-start.1) | copy-done | bytes 2162712
  53.7 1.9 %first_ffn.1 = bf16[32,8,4,256]{3,2,1,0:T(4,128)(2,1)} custom-call(bf16[32,8,4,256]{3,2,1,0:T(4,128)(2,1)S(1)} %bitcast.31, bf16[8,528,256]{2,1,0:T(8,128)(2,1)S(1)} %bitcast.34), custom_call_target="tpu_custom_call" | custom-call | tf_op jit(solution)/shard_map/first_ffn/pallas_call | solution.py:87
  55.6 8.8 %all-to-all-start.1 = ((bf16[32,8,4,256]{3,2,1,0:T(4,128)(2,1)}), bf16[32,8,4,256]{3,2,1,0:T(4,128)(2,1)}, u32[]{:S(2)}, u32[]{:S(2)}) async-start(bf16[32,8,4,256]{3,2,1,0:T(4,128)(2,1)} %first_ffn.1), calls=%async_computation.1 | async-start | bytes 1048576 | tf_op jit(solution)/shard_map/all_to_all | solution.py:359
  64.4 16.5 %all-to-all-done.1 = bf16[32,8,4,256]{3,2,1,0:T(4,128)(2,1)} async-done(((bf16[32,8,4,256]{3,2,1,0:T(4,128)(2,1)}), bf16[32,8,4,256]{3,2,1,0:T(4,128)(2,1)}, u32[]{:S(2)}, u32[]{:S(2)}) %all-to-all-start.1) | async-done | bytes 524320 | tf_op jit(solution)/shard_map/all_to_all | solution.py:359
  80.9 1.3 convert_reduce_fusion
  82.3 11.0 %all_to_all.31.rows_ref = bf16[8,8,4,256]{3,2,1,0:T(4,128)(2,1)S(1)} all-to-all(bf16[8,8,4,256]{3,2,1,0:T(4,128)(2,1)S(1)} %broadcast_in_dim.24), channel_id=1, replica_groups=mesh['z'=8,'y'=4,'x'=4,'core'=2] {'x','core'}, dimensions={0} | all-to-all | bytes 262144 | tf_op jit(solution)/shard_map/all_to_all | solution.py:27
  93.3 0.0 copy-done.5
  93.3 0.0 copy-done.3
  93.3 0.0 copy-done.2
  93.3 0.0 copy-done.13
  93.3 0.0 copy-done.14
  93.3 0.0 copy-done.15
  93.3 0.0 copy-done.17
  93.3 0.0 copy-done.18
  93.3 0.0 copy-done.19
  93.3 0.0 copy-done.20
  93.3 0.0 copy-done.21
  93.3 0.0 copy-done.22
  93.4 0.0 copy-done.23
  93.4 0.0 copy-done.16
  93.4 0.0 copy-done.24
  93.4 0.0 copy-start
  93.4 2.2 %copy-done = f32[32,4,64,128]{3,2,1,0:T(8,128)S(1)} copy-done((f32[32,4,64,128]{3,2,1,0:T(8,128)S(1)}, f32[32,4,64,128]{3,2,1,0:T(8,128)}, u32[]{:S(2)}) %copy-start) | copy-done | bytes 4194328
  95.6 1.2 copy-done.4
  96.8 1.1 copy-done.6
  97.9 5.1 %mixer.1 = (bf16[8,4,2048]{2,1,0:T(4,128)(2,1)}, f32[32,4,64,128]{3,2,1,0:T(8,128)}) custom-call(bf16[8,8,4,256]{3,2,1,0:T(4,128)(2,1)S(1)} %all_to_all.31.rows_ref, bf16[2048]{0:T(1024)(128)(2,1)S(1)} %copy-done.17, bf16[2048,256]{1,0:T(8,128)(2,1)S(1)} %copy-done.2, bf16[2048,256]{1,0:T(8,128)(2,1)S(1)} %copy-done.3, bf16[2048,128]{1,0:T(8,128)(2,1)S(1)} %copy-done.5, ...), custom_call_target="tpu_custom_call" | custom-call | tf_op jit(solution)/shard_map/mixer/pallas_call | solution.py:283
  103.0 4.1 %all-to-all-start.3 = ((bf16[8,4,2048]{2,1,0:T(4,128)(2,1)}), bf16[8,4,2048]{2,1,0:T(4,128)(2,1)S(1)}, u32[]{:S(2)}, u32[]{:S(2)}) async-start(bf16[8,4,2048]{2,1,0:T(4,128)(2,1)} %get-tuple-element.7), calls=%async_computation.3 | async-start | bytes 262144 | tf_op jit(solution)/shard_map/all_to_all | solution.py:305
  107.1 6.6 %all-to-all-done.3 = bf16[8,4,2048]{2,1,0:T(4,128)(2,1)S(1)} async-done(((bf16[8,4,2048]{2,1,0:T(4,128)(2,1)}), bf16[8,4,2048]{2,1,0:T(4,128)(2,1)S(1)}, u32[]{:S(2)}, u32[]{:S(2)}) %all-to-all-start.3) | async-done | bytes 131104 | tf_op jit(solution)/shard_map/all_to_all | solution.py:305
  113.7 0.1 convert_reduce_fusion.1
  113.8 11.0 %all_to_all.32.rows_ref = bf16[8,4,2048]{2,1,0:T(4,128)(2,1)} all-to-all(bf16[8,4,2048]{2,1,0:T(4,128)(2,1)S(1)} %broadcast_in_dim.25), channel_id=1, replica_groups=mesh['z'=8,'y'=4,'x'=4,'core'=2] {'z'}, dimensions={0} | all-to-all | bytes 262144 | tf_op jit(solution)/shard_map/all_to_all | solution.py:27
  124.8 6.5 %second_ffn.1 = bf16[8,8,4,256]{3,2,1,0:T(4,128)(2,1)} custom-call(s32[1]{0:T(128)} %bitcast.place_ref, bf16[8,4,2048]{2,1,0:T(4,128)(2,1)} %all_to_all.32.rows_ref, bf16[4,8,528,256]{3,2,1,0:T(8,128)(2,1)} %bitcast.43), custom_call_target="tpu_custom_call" | custom-call | tf_op jit(solution)/shard_map/second_ffn/pallas_call | solution.py:124
  131.3 17.8 %all_to_all.33 = bf16[64,4,256]{2,1,0:T(4,128)(2,1)S(1)} all-to-all(bf16[64,4,256]{2,1,0:T(4,128)(2,1)} %bitcast.45), channel_id=1, replica_groups=mesh['z'=8,'y'=4,'x'=4,'core'=2] {'z','x','core'}, dimensions={0} | all-to-all | bytes 262144 | tf_op jit(solution)/shard_map/all_to_all | solution.py:386
  149.2 0.6 multiply_convert_fusion
  (20 shorter events, 0.2 us)
Async XLA Ops:
  7.2 86.1 %copy-start.5 = (bf16[2048,128]{1,0:T(8,128)(2,1)S(1)}, bf16[2048,128]{1,0:T(8,128)(2,1)}, u32[]{:S(2)}) copy-start(bf16[2048,128]{1,0:T(8,128)(2,1)} %write_ref.1) | copy-start | bytes 1572868
  7.2 86.1 %copy-start.3 = (bf16[2048,256]{1,0:T(8,128)(2,1)S(1)}, bf16[2048,256]{1,0:T(8,128)(2,1)}, u32[]{:S(2)}) copy-start(bf16[2048,256]{1,0:T(8,128)(2,1)} %input_ref.1) | copy-start | bytes 3145732
  7.2 86.1 %copy-start.2 = (bf16[2048,256]{1,0:T(8,128)(2,1)S(1)}, bf16[2048,256]{1,0:T(8,128)(2,1)}, u32[]{:S(2)}) copy-start(bf16[2048,256]{1,0:T(8,128)(2,1)} %gate_ref.1) | copy-start | bytes 3145732
  7.2 44.9 %all-gather.5.cloned.1.call-start = ((), (), s32[]{:S(2)}) async-start(), calls=%async_computation.6 | async-start | bytes 2433024 | tf_op jit(solution)/shard_map/all_gather | solution.py:344
  7.2 1.0 copy-start.7
  8.3 0.9 copy-start.8
  9.2 0.9 copy-start.9
  10.1 0.9 copy-start.10
  11.0 0.9 copy-start.11
  11.9 0.9 copy-start.12
  12.7 0.7 copy-start.25
  13.4 0.7 copy-start.26
  14.1 79.2 %copy-start.13 = (bf16[32,3,256]{2,0,1:T(8,128)(2,1)S(1)}, bf16[32,3,256]{2,0,1:T(8,128)(2,1)}, u32[]{:S(2)}) copy-start(bf16[32,3,256]{2,0,1:T(8,128)(2,1)} %param.44) | copy-start | bytes 147460
  14.1 79.2 %copy-start.14 = (bf16[32,3,128]{2,0,1:T(8,128)(2,1)S(1)}, bf16[32,3,128]{2,0,1:T(8,128)(2,1)}, u32[]{:S(2)}) copy-start(bf16[32,3,128]{2,0,1:T(8,128)(2,1)} %param.45) | copy-start | bytes 73732
  14.1 79.2 %copy-start.15 = (bf16[32,3,128]{2,0,1:T(8,128)(2,1)S(1)}, bf16[32,3,128]{2,0,1:T(8,128)(2,1)}, u32[]{:S(2)}) copy-start(bf16[32,3,128]{2,0,1:T(8,128)(2,1)} %param.46) | copy-start | bytes 73732
  14.1 79.2 %copy-start.17 = (bf16[2048]{0:T(1024)(128)(2,1)S(1)}, bf16[2048]{0:T(1024)(128)(2,1)}, u32[]{:S(2)}) copy-start(bf16[2048]{0:T(1024)(128)(2,1)} %gain_ref.1) | copy-start | bytes 12292
  14.1 79.2 %copy-start.18 = (bf16[4,256]{1,0:T(4,128)(2,1)S(1)}, bf16[4,256]{1,0:T(4,128)(2,1)}, u32[]{:S(2)}) copy-start(bf16[4,256]{1,0:T(4,128)(2,1)} %taps_input_ref.1) | copy-start | bytes 6148
  14.1 79.2 %copy-start.19 = (bf16[4,128]{1,0:T(4,128)(2,1)S(1)}, bf16[4,128]{1,0:T(4,128)(2,1)}, u32[]{:S(2)}) copy-start(bf16[4,128]{1,0:T(4,128)(2,1)} %taps_write_ref.1) | copy-start | bytes 3076
  14.1 79.2 %copy-start.20 = (bf16[4,128]{1,0:T(4,128)(2,1)S(1)}, bf16[4,128]{1,0:T(4,128)(2,1)}, u32[]{:S(2)}) copy-start(bf16[4,128]{1,0:T(4,128)(2,1)} %taps_read_ref.1) | copy-start | bytes 3076
  14.1 79.2 %copy-start.21 = (f32[4]{0:T(128)S(1)}, f32[4]{0:T(128)}, u32[]{:S(2)}) copy-start(f32[4]{0:T(128)} %bias_ref.1) | copy-start | bytes 52
  14.1 79.2 %copy-start.22 = (f32[4]{0:T(128)S(1)}, f32[4]{0:T(128)}, u32[]{:S(2)}) copy-start(f32[4]{0:T(128)} %rate_ref.1) | copy-start | bytes 52
  14.1 79.2 %copy-start.23 = (f32[4]{0:T(128)S(1)}, f32[4]{0:T(128)}, u32[]{:S(2)}) copy-start(f32[4]{0:T(128)} %skip_ref.1) | copy-start | bytes 52
  15.0 109.8 %all-gather.7.cloned.1.call-start = ((), (), s32[]{:S(2)}) async-start(), calls=%async_computation.7 | async-start | bytes 8921088 | tf_op jit(solution)/shard_map/all_gather | solution.py:345
  52.1 1.6 %copy-start.1 = (bf16[4224,256]{1,0:T(8,128)(2,1)S(1)}, bf16[4224,256]{1,0:T(8,128)(2,1)}, u32[]{:S(2)}) copy-start(bf16[4224,256]{1,0:T(8,128)(2,1)} %all-gather.5.cloned.1.call-done) | copy-start | bytes 6488068
  53.7 39.7 %copy-start.16 = (bf16[2048,4]{0,1:T(4,128)(2,1)S(1)}, bf16[2048,4]{0,1:T(4,128)(2,1)}, u32[]{:S(2)}) copy-start(bf16[2048,4]{0,1:T(4,128)(2,1)} %param.37) | copy-start | bytes 49156
  53.7 39.7 %copy-start.24 = (bf16[256]{0:T(256)(128)(2,1)S(1)}, bf16[256]{0:T(256)(128)(2,1)}, u32[]{:S(2)}) copy-start(bf16[256]{0:T(256)(128)(2,1)} %group_ref.1) | copy-start | bytes 1540
  55.6 25.3 %all-to-all-start.1 = ((bf16[32,8,4,256]{3,2,1,0:T(4,128)(2,1)}), bf16[32,8,4,256]{3,2,1,0:T(4,128)(2,1)}, u32[]{:S(2)}, u32[]{:S(2)}) async-start(bf16[32,8,4,256]{3,2,1,0:T(4,128)(2,1)} %first_ffn.1), calls=%async_computation.1 | async-start | bytes 1048576 | tf_op jit(solution)/shard_map/all_to_all | solution.py:359
  93.4 2.2 %copy-start = (f32[32,4,64,128]{3,2,1,0:T(8,128)S(1)}, f32[32,4,64,128]{3,2,1,0:T(8,128)}, u32[]{:S(2)}) copy-start(f32[32,4,64,128]{3,2,1,0:T(8,128)} %state_ref.1) | copy-start | bytes 12582916
  95.6 1.2 copy-start.4
  96.8 1.1 copy-start.6
  103.0 10.7 %all-to-all-start.3 = ((bf16[8,4,2048]{2,1,0:T(4,128)(2,1)}), bf16[8,4,2048]{2,1,0:T(4,128)(2,1)S(1)}, u32[]{:S(2)}, u32[]{:S(2)}) async-start(bf16[8,4,2048]{2,1,0:T(4,128)(2,1)} %get-tuple-element.7), calls=%async_computation.3 | async-start | bytes 262144 | tf_op jit(solution)/shard_map/all_to_all | solution.py:305
Sparse Core Ops, SparseCore 0:
  15.1 35.5 all-gather.4
  53.2 61.6 all-gather.6

commit v5 on v4

--- a/solution.py
+++ b/solution.py
@@ -33,42 +33,39 @@
     return lax.rsqrt(jnp.mean(values * values, axis=-1, keepdims=True) + norm_eps)
 
 
-def share_kernel(*refs):
-    for gain, gate, lift, down, out in (refs[0:4] + refs[8:9], refs[4:8] + refs[9:10]):
-        gain_f = gain[...].astype(jnp.float32).reshape(1, FEATS)
-        out[:HIDDEN] = (gate[...].astype(jnp.float32) * gain_f).astype(jnp.bfloat16)
-        out[HIDDEN : 2 * HIDDEN] = (lift[...].astype(jnp.float32) * gain_f).astype(jnp.bfloat16)
-        out[2 * HIDDEN :] = down[...]
-
-
-def weight_shares(*sets):
-    operands = []
-    for gain, gate_weight, lift_weight, down_weight in sets:
-        operands += [gain, gate_weight.T, lift_weight.T, down_weight]
+def in_hbm(array):
+    return pltpu.with_memory_space_constraint(array, pltpu.HBM)
+
+
+def in_vmem(array):
+    return pltpu.with_memory_space_constraint(array, pltpu.VMEM)
+
+
+def share_kernel(gain, gate, lift, down, out):
+    gain_f = gain[...].astype(jnp.float32).reshape(1, FEATS)
+    out[:HIDDEN] = (gate[...].astype(jnp.float32) * gain_f).astype(jnp.bfloat16)
+    out[HIDDEN : 2 * HIDDEN] = (lift[...].astype(jnp.float32) * gain_f).astype(jnp.bfloat16)
+    out[2 * HIDDEN :] = down[...]
+
+
+def weight_share(gain, gate_weight, lift_weight, down_weight):
+    operands = [gain, gate_weight.T, lift_weight.T, down_weight]
     return pl.pallas_call(
         share_kernel,
-        out_shape=[jax.ShapeDtypeStruct((3 * HIDDEN, FEATS), jnp.bfloat16)] * 2,
-        compiler_params=pltpu.CompilerParams(vmem_limit_bytes=24 << 20),
-        name="shares",
-    )(*operands)
-
-
-def hidden_units(normed_ref, weights, rows):
-    gate = jnp.zeros((rows, HIDDEN), jnp.float32)
-    lift = jnp.zeros((rows, HIDDEN), jnp.float32)
-    for u in range(TP):
-        block = normed_ref[u]
-        gate += lax.dot_general(
-            block, weights[u, :HIDDEN], by_rows, preferred_element_type=jnp.float32
-        )
-        lift += lax.dot_general(
-            block, weights[u, HIDDEN : 2 * HIDDEN], by_rows, preferred_element_type=jnp.float32
-        )
-    return (gate * jax.nn.sigmoid(gate) * lift).astype(jnp.bfloat16)
-
-
-def first_kernel(rows_ref, weights_ref, out_ref, normed_ref):
+        out_shape=jax.ShapeDtypeStruct((3 * HIDDEN, FEATS), jnp.bfloat16),
+        name="share",
+    )(*[in_hbm(operand) for operand in operands])
+
+
+def first_kernel(rows_ref, weights_hbm, out_ref, normed_ref, weights_ref, arrived):
     blocks = Z * Y
+    count = blocks * ROWS
+    copies = [
+        pltpu.make_async_copy(weights_hbm.at[u], weights_ref.at[u], arrived.at[u])
+        for u in range(TP)
+    ]
+    for copy in copies:
+        copy.start()
     total = jnp.zeros((blocks, ROWS, 1), jnp.float32)
     for u in range(TP):
         values = rows_ref[:, u].astype(jnp.float32)
@@ -76,8 +73,19 @@
     factor = lax.rsqrt(total * (1.0 / D) + norm_eps)
     for u in range(TP):
         values = rows_ref[:, u].astype(jnp.float32) * factor
-        normed_ref[u] = values.reshape(blocks * ROWS, FEATS).astype(jnp.bfloat16)
-    hidden = hidden_units(normed_ref, weights_ref, blocks * ROWS)
+        normed_ref[u] = values.reshape(count, FEATS).astype(jnp.bfloat16)
+    gate = jnp.zeros((count, HIDDEN), jnp.float32)
+    lift = jnp.zeros((count, HIDDEN), jnp.float32)
+    for u in range(TP):
+        copies[u].wait()
+        block = normed_ref[u]
+        gate += lax.dot_general(
+            block, weights_ref[u, :HIDDEN], by_rows, preferred_element_type=jnp.float32
+        )
+        lift += lax.dot_general(
+            block, weights_ref[u, HIDDEN : 2 * HIDDEN], by_rows, preferred_element_type=jnp.float32
+        )
+    hidden = (gate * jax.nn.sigmoid(gate) * lift).astype(jnp.bfloat16)
     for u in range(TP):
         down = jnp.dot(hidden, weights_ref[u, 2 * HIDDEN :], preferred_element_type=jnp.float32)
         out_ref[:, u] = down.reshape(blocks, ROWS, FEATS).astype(jnp.bfloat16)
@@ -87,10 +95,18 @@
     return pl.pallas_call(
         first_kernel,
         out_shape=jax.ShapeDtypeStruct(rows.shape, jnp.bfloat16),
-        scratch_shapes=[pltpu.VMEM((TP, Z * Y * ROWS, FEATS), jnp.bfloat16)],
+        in_specs=[
+            pl.BlockSpec(memory_space=pltpu.VMEM),
+            pl.BlockSpec(memory_space=pltpu.HBM),
+        ],
+        scratch_shapes=[
+            pltpu.VMEM((TP, Z * Y * ROWS, FEATS), jnp.bfloat16),
+            pltpu.VMEM(weights.shape, jnp.bfloat16),
+            pltpu.SemaphoreType.DMA((TP,)),
+        ],
         compiler_params=pltpu.CompilerParams(vmem_limit_bytes=24 << 20),
         name="first_ffn",
-    )(rows, weights)
+    )(in_vmem(rows), in_hbm(weights))
 
 
 def second_kernel(place_ref, rows_ref, weights_ref, out_ref, normed_ref, sum_ref):
@@ -108,7 +124,16 @@
             normed_ref[u] = (block * factor).astype(jnp.bfloat16)
             sum_ref[u] = block * own
 
-    hidden = hidden_units(normed_ref, weights_ref.at[0], rows)
+    both = jnp.zeros((2 * HIDDEN, rows), jnp.float32)
+    for u in range(TP):
+        both += lax.dot_general(
+            weights_ref[0, u, : 2 * HIDDEN],
+            normed_ref[u],
+            by_rows,
+            preferred_element_type=jnp.float32,
+        )
+    gate, lift = both[:HIDDEN], both[HIDDEN:]
+    hidden = (gate * jax.nn.sigmoid(gate) * lift).T.astype(jnp.bfloat16)
     for u in range(TP):
         down = jnp.dot(hidden, weights_ref[0, u, 2 * HIDDEN :], preferred_element_type=jnp.float32)
         sum_ref[u] = sum_ref[u] + down
@@ -127,7 +152,7 @@
         out_shape=jax.ShapeDtypeStruct((Z, TP, ROWS, FEATS), jnp.bfloat16),
         in_specs=[
             pl.BlockSpec(memory_space=pltpu.SMEM),
-            pl.BlockSpec(rows.shape, lambda i: (0, 0, 0)),
+            pl.BlockSpec(memory_space=pltpu.VMEM),
             pl.BlockSpec((1, TP, 3 * HIDDEN, FEATS), lambda i: (i, 0, 0, 0)),
         ],
         out_specs=pl.BlockSpec((Z, TP, ROWS, FEATS), lambda i: (0, 0, 0, 0)),
@@ -135,8 +160,9 @@
             pltpu.VMEM((TP, Z * ROWS, FEATS), jnp.bfloat16),
             pltpu.VMEM((TP, Z * ROWS, FEATS), jnp.float32),
         ],
+        compiler_params=pltpu.CompilerParams(vmem_limit_bytes=24 << 20),
         name="second_ffn",
-    )(place, rows, weights)
+    )(place, in_vmem(rows), in_hbm(weights))
 
 
 def conv_silu(newest, buffer_ref, taps_ref):
@@ -159,7 +185,7 @@
     gate_ref,
     input_ref,
     write_ref,
-    read_ref,
+    read_hbm,
     step_ref,
     bias_ref,
     rate_ref,
@@ -172,7 +198,7 @@
     buffer_read_ref,
     state_ref,
     group_ref,
-    output_ref,
+    output_hbm,
     mixed_ref,
     new_state_ref,
     normed_ref,
@@ -183,11 +209,18 @@
     bc_ref,
     rc_ref,
     out_cols_ref,
+    read_ref,
+    output_ref,
+    arrived,
 ):
     i = pl.program_id(0)
+    read_copy = pltpu.make_async_copy(read_hbm, read_ref, arrived.at[0])
+    output_copy = pltpu.make_async_copy(output_hbm, output_ref, arrived.at[1])
 
     @pl.when(i == 0)
     def _():
+        read_copy.start()
+        output_copy.start()
         total = jnp.zeros((TP, ROWS, 1), jnp.float32)
         for u in range(TP):
             values = rows_ref[:, u].astype(jnp.float32)
@@ -211,6 +244,7 @@
         ).astype(jnp.bfloat16)
         xc = conv_silu(project(input_ref), buffer_input_ref, taps_input_ref)
         bc_ref[...] = conv_silu(project(write_ref), buffer_write_ref, taps_write_ref)
+        read_copy.wait()
         rc_ref[...] = conv_silu(project(read_ref), buffer_read_ref, taps_read_ref)
         xc_ref[...] = xc
         step = jax.nn.softplus(step_raw.astype(jnp.float32) + bias_ref[...].reshape(1, PER_DEVICE))
@@ -261,6 +295,7 @@
         gate_z = gate_z_ref[...].astype(jnp.float32)
         gated = head_out * (gate_z * jax.nn.sigmoid(gate_z))
         gated = gated * inverse_rms(gated) * group_ref[...].astype(jnp.float32).reshape(1, CHANNELS)
+        output_copy.wait()
         part = jnp.dot(
             gated.astype(jnp.bfloat16), output_ref[...], preferred_element_type=jnp.float32
         )
@@ -272,11 +307,11 @@
     operands = [rows, *small, *[b.transpose(1, 0, 2) for b in buffers]]
     operands += [scan_state, group_gain, proj_output]
     state_place = len(operands) - 3
-    operands = [
-        o if n == state_place else pltpu.with_memory_space_constraint(o, pltpu.VMEM)
-        for n, o in enumerate(operands)
-    ]
+    from_hbm = (5, state_place, len(operands) - 1)
+    operands = [in_hbm(o) if n in from_hbm else in_vmem(o) for n, o in enumerate(operands)]
     specs = [pl.BlockSpec(memory_space=pltpu.VMEM) for _ in operands]
+    for n in from_hbm:
+        specs[n] = pl.BlockSpec(memory_space=pltpu.HBM)
     state_spec = pl.BlockSpec((BLOCK, PER_DEVICE, HEAD_DIM, STATE), lambda i: (i, 0, 0, 0))
     specs[state_place] = state_spec
     blocks = SEQS // BLOCK
@@ -298,6 +333,9 @@
             pltpu.VMEM((SEQS, STATE), jnp.float32),
             pltpu.VMEM((SEQS, STATE), jnp.float32),
             pltpu.VMEM((blocks, CHANNELS, BLOCK), jnp.float32),
+            pltpu.VMEM((D, STATE), jnp.bfloat16),
+            pltpu.VMEM((CHANNELS, D), jnp.bfloat16),
+            pltpu.SemaphoreType.DMA((2,)),
         ],
         compiler_params=pltpu.CompilerParams(vmem_limit_bytes=24 << 20),
         name="mixer",
@@ -337,14 +375,12 @@
     second_lift,
     second_down,
 ):
-    share_one, share_two = weight_shares(
-        (first_gain, first_gate, first_lift, first_down),
-        (second_gain, second_gate, second_lift, second_down),
+    weights_one = lax.all_gather(
+        weight_share(first_gain, first_gate, first_lift, first_down), TP_AXES
     )
-    weights_one = lax.all_gather(share_one, TP_AXES)
-    weights_two = lax.all_gather(share_two, ("y", *TP_AXES)).reshape(
-        Y, TP, 3 * HIDDEN, FEATS
-    )
+    weights_two = lax.all_gather(
+        weight_share(second_gain, second_gate, second_lift, second_down), ("y", *TP_AXES)
+    ).reshape(Y, TP, 3 * HIDDEN, FEATS)
 
     split = residual.reshape(TP, ROWS, FEATS)
     tiles = lax.all_to_all(

time: 158 us -> 150 us (0.949)
  local copies, waits for them, and re-layouts: 14 us -> 1.13 us
  Pallas kernels: 14.4 us -> 21.1 us
    unnamed x54 -> x30, local copies, waits for them, and re-layouts: 12.9 us -> 0.07 us
    pallas_call x1, Pallas kernels: 5.1 us -> 8.17 us  [state_mixer(): pl.pallas_call(mixer_kernel, grid=(blocks,), out_shape=[jax.ShapeDtypeStr...]
    pallas_call x1 -> x2, Pallas kernels: 0.83 us -> 3.6 us  [weight_share(): pl.pallas_call(share_kernel, out_shape=jax.ShapeDtypeStruct((3 * HIDDEN,...]
  transfers between devices with their start and end apart: 4 -> 4, of which waited for: 2 -> 2; matrix products, arithmetic and copies ran while one was open for 2% -> 2% of each run, Pallas kernels for 4% -> 9%
where the time goes in v5:
time: 150 us; the launch traced here: 149 us
  blocking collectives  73.7 us (49%)
  waiting for transfers between devices  23.7 us (16%)
  Pallas kernels  21.1 us (14%)
  between operations  14.4 us (10%)
  starting transfers between devices  13.1 us (9%)
  other arithmetic  2.01 us (1%)
    all_to_all x1, blocking collectives, per_device(): lax.all_to_all(jnp.broadcast_to(split[None], (Z * Y, TP, ROWS, FEATS)).re...  35.3 us
    all_to_all x2, blocking collectives, sent_to_all(): lax.all_to_all(jnp.broadcast_to(array[None], (length, *array.shape)), axi...  21.4 us
    all_to_all x1, blocking collectives, per_device(): lax.all_to_all(share.reshape(-1, ROWS, FEATS), ('z', *TP_AXES), 0, 0, til...  17 us
    all_to_all x1, waiting for transfers between devices, per_device(): share = lax.all_to_all(share, KV_AXES, 0, 0, tiled=True)  16.5 us
    all_to_all x1, starting transfers between devices, per_device(): share = lax.all_to_all(share, KV_AXES, 0, 0, tiled=True)  8.8 us
    pallas_call x1, Pallas kernels, state_mixer(): pl.pallas_call(mixer_kernel, grid=(blocks,), out_shape=[jax.ShapeDtypeStr...  8.17 us
    all_to_all x1, waiting for transfers between devices, state_mixer(): tiles = lax.all_to_all(partial_out, TP_AXES, 0, 0, tiled=True)  7.09 us
    pallas_call x1, Pallas kernels, second_partial(): pl.pallas_call(second_kernel, grid=(Y,), out_shape=jax.ShapeDtypeStruct((...  6.39 us
  transfers between devices with their start and end apart: 4, of which 2 were waited for; matrix products, arithmetic and copies ran while one was open for 2% of the time, Pallas kernels for 9%

profile of v5, /device:TPU:1, one launch (start us, length us, event | category | flops | bytes accessed | tf_op | source)
XLA Modules:
  0.0 149.0 jit_solution(8355809202075853534)
XLA Ops:
  7.2 0.0 all-gather.5.cloned.1.call-start
  7.2 0.0 copy-start
  7.2 0.0 copy-start.1
  7.2 0.0 copy-start.2
  7.2 0.0 copy-start.3
  7.3 0.0 copy-start.4
  7.3 0.0 copy-start.5
  7.3 0.0 copy-start.6
  7.3 0.0 copy-start.7
  7.3 0.0 copy-start.8
  7.3 0.0 copy-start.9
  7.3 0.0 copy-start.10
  7.3 0.0 copy-start.11
  7.3 0.0 copy-start.12
  7.3 0.0 copy-start.13
  7.4 0.0 copy-start.14
  7.4 1.9 %share.2 = bf16[528,256]{1,0:T(8,128)(2,1)} custom-call(bf16[256]{0:T(256)(128)(2,1)} %gain.2, bf16[176,256]{1,0:T(8,128)(2,1)} %bitcast.43, bf16[176,256]{1,0:T(8,128)(2,1)} %bitcast.44, bf16[176,256]{1,0:T(8,128)(2,1)} %down.2), custom_call_target="tpu_custom_call" | custom-call | tf_op jit(solution)/shard_map/share/pallas_call | solution.py:53
  9.2 0.0 all-gather.5.cloned.1.call-update
  9.3 0.0 all-gather.7.cloned.1.call-start
  9.3 1.7 %share.3 = bf16[528,256]{1,0:T(8,128)(2,1)} custom-call(bf16[256]{0:T(256)(128)(2,1)} %gain.3, bf16[176,256]{1,0:T(8,128)(2,1)} %bitcast.45, bf16[176,256]{1,0:T(8,128)(2,1)} %bitcast.46, bf16[176,256]{1,0:T(8,128)(2,1)} %down.3), custom_call_target="tpu_custom_call" | custom-call | tf_op jit(solution)/shard_map/share/pallas_call | solution.py:53
  11.1 0.0 all-gather.7.cloned.1.call-update
  11.1 0.7 broadcast_in_dim.10
  11.8 0.2 broadcast_in_dim.22
  12.0 35.3 %all_to_all.30 = bf16[256,4,256]{2,1,0:T(4,128)(2,1)S(1)} all-to-all(bf16[256,4,256]{2,1,0:T(4,128)(2,1)S(1)} %bitcast.41), channel_id=1, replica_groups=mesh['z'=8,'y'=4,'x'=4,'core'=2] {'z','y','x','core'}, dimensions={0} | all-to-all | bytes 1048576 | tf_op jit(solution)/shard_map/all_to_all | solution.py:386
  47.4 0.0 all-gather.5.cloned.1.call-done
  47.4 3.0 %first_ffn.1 = bf16[32,8,4,256]{3,2,1,0:T(4,128)(2,1)} custom-call(bf16[32,8,4,256]{3,2,1,0:T(4,128)(2,1)S(1)} %bitcast.31, bf16[8,528,256]{2,1,0:T(8,128)(2,1)} %bitcast.40), custom_call_target="tpu_custom_call" | custom-call | tf_op jit(solution)/shard_map/first_ffn/pallas_call | solution.py:95
  50.4 8.8 %all-to-all-start.1 = ((bf16[32,8,4,256]{3,2,1,0:T(4,128)(2,1)}), bf16[32,8,4,256]{3,2,1,0:T(4,128)(2,1)}, u32[]{:S(2)}, u32[]{:S(2)}) async-start(bf16[32,8,4,256]{3,2,1,0:T(4,128)(2,1)} %first_ffn.1), calls=%async_computation.1 | async-start | bytes 1048576 | tf_op jit(solution)/shard_map/all_to_all | solution.py:395
  59.2 16.5 %all-to-all-done.1 = bf16[32,8,4,256]{3,2,1,0:T(4,128)(2,1)} async-done(((bf16[32,8,4,256]{3,2,1,0:T(4,128)(2,1)}), bf16[32,8,4,256]{3,2,1,0:T(4,128)(2,1)}, u32[]{:S(2)}, u32[]{:S(2)}) %all-to-all-start.1) | async-done | bytes 524320 | tf_op jit(solution)/shard_map/all_to_all | solution.py:395
  75.7 1.3 convert_reduce_fusion
  77.1 10.9 %all_to_all.31.rows_ref = bf16[8,8,4,256]{3,2,1,0:T(4,128)(2,1)S(1)} all-to-all(bf16[8,8,4,256]{3,2,1,0:T(4,128)(2,1)S(1)} %broadcast_in_dim.24), channel_id=1, replica_groups=mesh['z'=8,'y'=4,'x'=4,'core'=2] {'x','core'}, dimensions={0} | all-to-all | bytes 262144 | tf_op jit(solution)/shard_map/all_to_all | solution.py:27
  88.0 0.0 copy-done
  88.0 0.0 copy-done.1
  88.0 0.0 copy-done.2
  88.0 0.0 copy-done.3
  88.0 0.0 copy-done.4
  88.0 0.0 copy-done.5
  88.0 0.0 copy-done.6
  88.0 0.0 copy-done.7
  88.1 0.0 copy-done.8
  88.1 0.0 copy-done.9
  88.1 0.0 copy-done.10
  88.1 0.0 copy-done.11
  88.1 0.0 copy-done.12
  88.1 0.0 copy-done.13
  88.1 0.0 copy-done.14
  88.1 8.2 %mixer.1 = (bf16[8,4,2048]{2,1,0:T(4,128)(2,1)}, f32[32,4,64,128]{3,2,1,0:T(8,128)}) custom-call(bf16[8,8,4,256]{3,2,1,0:T(4,128)(2,1)S(1)} %all_to_all.31.rows_ref, bf16[2048]{0:T(1024)(128)(2,1)S(1)} %copy-done.7, bf16[2048,256]{1,0:T(8,128)(2,1)S(1)} %copy-done, bf16[2048,256]{1,0:T(8,128)(2,1)S(1)} %copy-done.1, bf16[2048,128]{1,0:T(8,128)(2,1)S(1)} %copy-done.2, ...), custom_call_target="tpu_custom_call" | custom-call | tf_op jit(solution)/shard_map/mixer/pallas_call | solution.py:318
  96.3 4.2 %all-to-all-start.3 = ((bf16[8,4,2048]{2,1,0:T(4,128)(2,1)}), bf16[8,4,2048]{2,1,0:T(4,128)(2,1)S(1)}, u32[]{:S(2)}, u32[]{:S(2)}) async-start(bf16[8,4,2048]{2,1,0:T(4,128)(2,1)} %get-tuple-element.4), calls=%async_computation.3 | async-start | bytes 262144 | tf_op jit(solution)/shard_map/all_to_all | solution.py:343
  100.5 7.1 %all-to-all-done.3 = bf16[8,4,2048]{2,1,0:T(4,128)(2,1)S(1)} async-done(((bf16[8,4,2048]{2,1,0:T(4,128)(2,1)}), bf16[8,4,2048]{2,1,0:T(4,128)(2,1)S(1)}, u32[]{:S(2)}, u32[]{:S(2)}) %all-to-all-start.3) | async-done | bytes 131104 | tf_op jit(solution)/shard_map/all_to_all | solution.py:343
  107.6 0.1 convert_reduce_fusion.1
  107.7 10.4 %all_to_all.32.rows_ref = bf16[8,4,2048]{2,1,0:T(4,128)(2,1)S(1)} all-to-all(bf16[8,4,2048]{2,1,0:T(4,128)(2,1)S(1)} %broadcast_in_dim.25), channel_id=1, replica_groups=mesh['z'=8,'y'=4,'x'=4,'core'=2] {'z'}, dimensions={0} | all-to-all | bytes 262144 | tf_op jit(solution)/shard_map/all_to_all | solution.py:27
  118.1 0.0 all-gather.7.cloned.1.call-done
  118.1 6.4 %second_ffn.1 = bf16[8,8,4,256]{3,2,1,0:T(4,128)(2,1)S(1)} custom-call(s32[1]{0:T(128)} %bitcast.place_ref, bf16[8,4,2048]{2,1,0:T(4,128)(2,1)S(1)} %all_to_all.32.rows_ref, bf16[4,8,528,256]{3,2,1,0:T(8,128)(2,1)} %bitcast.39), custom_call_target="tpu_custom_call" | custom-call | tf_op jit(solution)/shard_map/second_ffn/pallas_call | solution.py:149
  124.5 17.0 %all_to_all.33 = bf16[64,4,256]{2,1,0:T(4,128)(2,1)S(1)} all-to-all(bf16[64,4,256]{2,1,0:T(4,128)(2,1)S(1)} %bitcast.34), channel_id=1, replica_groups=mesh['z'=8,'y'=4,'x'=4,'core'=2] {'z','x','core'}, dimensions={0} | all-to-all | bytes 262144 | tf_op jit(solution)/shard_map/all_to_all | solution.py:422
  141.6 0.6 multiply_convert_fusion
  (7 shorter events, 0.2 us)
Async XLA Ops:
  7.2 40.2 %all-gather.5.cloned.1.call-start = ((), (), s32[]{:S(2)}) async-start(), calls=%async_computation.6 | async-start | bytes 2433024 | tf_op jit(solution)/shard_map/all_gather | solution.py:378
  7.2 80.8 %copy-start = (bf16[2048,256]{1,0:T(8,128)(2,1)S(1)}, bf16[2048,256]{1,0:T(8,128)(2,1)}, u32[]{:S(2)}) copy-start(bf16[2048,256]{1,0:T(8,128)(2,1)} %gate_ref.1) | copy-start | bytes 3145732
  7.2 80.8 %copy-start.1 = (bf16[2048,256]{1,0:T(8,128)(2,1)S(1)}, bf16[2048,256]{1,0:T(8,128)(2,1)}, u32[]{:S(2)}) copy-start(bf16[2048,256]{1,0:T(8,128)(2,1)} %input_ref.1) | copy-start | bytes 3145732
  7.2 80.8 %copy-start.2 = (bf16[2048,128]{1,0:T(8,128)(2,1)S(1)}, bf16[2048,128]{1,0:T(8,128)(2,1)}, u32[]{:S(2)}) copy-start(bf16[2048,128]{1,0:T(8,128)(2,1)} %write_ref.1) | copy-start | bytes 1572868
  7.2 80.8 %copy-start.3 = (bf16[32,3,256]{2,0,1:T(8,128)(2,1)S(1)}, bf16[32,3,256]{2,0,1:T(8,128)(2,1)}, u32[]{:S(2)}) copy-start(bf16[32,3,256]{2,0,1:T(8,128)(2,1)} %param.44) | copy-start | bytes 147460
  7.3 80.8 %copy-start.4 = (bf16[32,3,128]{2,0,1:T(8,128)(2,1)S(1)}, bf16[32,3,128]{2,0,1:T(8,128)(2,1)}, u32[]{:S(2)}) copy-start(bf16[32,3,128]{2,0,1:T(8,128)(2,1)} %param.45) | copy-start | bytes 73732
  7.3 80.8 %copy-start.5 = (bf16[32,3,128]{2,0,1:T(8,128)(2,1)S(1)}, bf16[32,3,128]{2,0,1:T(8,128)(2,1)}, u32[]{:S(2)}) copy-start(bf16[32,3,128]{2,0,1:T(8,128)(2,1)} %param.46) | copy-start | bytes 73732
  7.3 80.8 %copy-start.6 = (bf16[2048,4]{0,1:T(4,128)(2,1)S(1)}, bf16[2048,4]{0,1:T(4,128)(2,1)}, u32[]{:S(2)}) copy-start(bf16[2048,4]{0,1:T(4,128)(2,1)} %param.37) | copy-start | bytes 49156
  7.3 80.8 %copy-start.7 = (bf16[2048]{0:T(1024)(128)(2,1)S(1)}, bf16[2048]{0:T(1024)(128)(2,1)}, u32[]{:S(2)}) copy-start(bf16[2048]{0:T(1024)(128)(2,1)} %gain_ref.1) | copy-start | bytes 12292
  7.3 80.8 %copy-start.8 = (bf16[4,256]{1,0:T(4,128)(2,1)S(1)}, bf16[4,256]{1,0:T(4,128)(2,1)}, u32[]{:S(2)}) copy-start(bf16[4,256]{1,0:T(4,128)(2,1)} %taps_input_ref.1) | copy-start | bytes 6148
  7.3 80.8 %copy-start.9 = (bf16[4,128]{1,0:T(4,128)(2,1)S(1)}, bf16[4,128]{1,0:T(4,128)(2,1)}, u32[]{:S(2)}) copy-start(bf16[4,128]{1,0:T(4,128)(2,1)} %taps_write_ref.1) | copy-start | bytes 3076
  7.3 80.8 %copy-start.10 = (bf16[4,128]{1,0:T(4,128)(2,1)S(1)}, bf16[4,128]{1,0:T(4,128)(2,1)}, u32[]{:S(2)}) copy-start(bf16[4,128]{1,0:T(4,128)(2,1)} %taps_read_ref.1) | copy-start | bytes 3076
  7.3 80.8 %copy-start.11 = (f32[4]{0:T(128)S(1)}, f32[4]{0:T(128)}, u32[]{:S(2)}) copy-start(f32[4]{0:T(128)} %bias_ref.1) | copy-start | bytes 52
  7.3 80.8 %copy-start.12 = (f32[4]{0:T(128)S(1)}, f32[4]{0:T(128)}, u32[]{:S(2)}) copy-start(f32[4]{0:T(128)} %rate_ref.1) | copy-start | bytes 52
  7.3 80.8 %copy-start.13 = (f32[4]{0:T(128)S(1)}, f32[4]{0:T(128)}, u32[]{:S(2)}) copy-start(f32[4]{0:T(128)} %skip_ref.1) | copy-start | bytes 52
  7.4 80.8 %copy-start.14 = (bf16[256]{0:T(256)(128)(2,1)S(1)}, bf16[256]{0:T(256)(128)(2,1)}, u32[]{:S(2)}) copy-start(bf16[256]{0:T(256)(128)(2,1)} %group_ref.1) | copy-start | bytes 1540
  9.3 108.9 %all-gather.7.cloned.1.call-start = ((), (), s32[]{:S(2)}) async-start(), calls=%async_computation.7 | async-start | bytes 8921088 | tf_op jit(solution)/shard_map/all_gather | solution.py:381
  50.4 25.4 %all-to-all-start.1 = ((bf16[32,8,4,256]{3,2,1,0:T(4,128)(2,1)}), bf16[32,8,4,256]{3,2,1,0:T(4,128)(2,1)}, u32[]{:S(2)}, u32[]{:S(2)}) async-start(bf16[32,8,4,256]{3,2,1,0:T(4,128)(2,1)} %first_ffn.1), calls=%async_computation.1 | async-start | bytes 1048576 | tf_op jit(solution)/shard_map/all_to_all | solution.py:395
  96.3 11.3 %all-to-all-start.3 = ((bf16[8,4,2048]{2,1,0:T(4,128)(2,1)}), bf16[8,4,2048]{2,1,0:T(4,128)(2,1)S(1)}, u32[]{:S(2)}, u32[]{:S(2)}) async-start(bf16[8,4,2048]{2,1,0:T(4,128)(2,1)} %get-tuple-element.4), calls=%async_computation.3 | async-start | bytes 262144 | tf_op jit(solution)/shard_map/all_to_all | solution.py:343
Sparse Core Ops, SparseCore 0:
  10.4 35.5 all-gather.4
  48.5 62.0 all-gather.6

commit v6 on v5

--- a/solution.py
+++ b/solution.py
@@ -41,23 +41,29 @@
     return pltpu.with_memory_space_constraint(array, pltpu.VMEM)
 
 
-def share_kernel(gain, gate, lift, down, out):
+def share_kernel(*refs):
+    gain, gate, lift, down, out = refs[-5:]
     gain_f = gain[...].astype(jnp.float32).reshape(1, FEATS)
     out[:HIDDEN] = (gate[...].astype(jnp.float32) * gain_f).astype(jnp.bfloat16)
     out[HIDDEN : 2 * HIDDEN] = (lift[...].astype(jnp.float32) * gain_f).astype(jnp.bfloat16)
     out[2 * HIDDEN :] = down[...]
 
 
-def weight_share(gain, gate_weight, lift_weight, down_weight):
+def weight_share(gain, gate_weight, lift_weight, down_weight, *early):
     operands = [gain, gate_weight.T, lift_weight.T, down_weight]
     return pl.pallas_call(
         share_kernel,
         out_shape=jax.ShapeDtypeStruct((3 * HIDDEN, FEATS), jnp.bfloat16),
+        compiler_params=pltpu.CompilerParams(vmem_limit_bytes=4 << 20),
+        in_specs=[pl.BlockSpec(memory_space=pltpu.SMEM) for _ in early]
+        + [pl.BlockSpec(memory_space=pltpu.VMEM) for _ in operands],
         name="share",
-    )(*[in_hbm(operand) for operand in operands])
-
-
-def first_kernel(rows_ref, weights_hbm, out_ref, normed_ref, weights_ref, arrived):
+    )(*early, *[in_hbm(operand) for operand in operands])
+
+
+def first_kernel(
+    place_ref, rows_ref, weights_hbm, out_ref, own_ref, normed_ref, weights_ref, arrived
+):
     blocks = Z * Y
     count = blocks * ROWS
     copies = [
@@ -74,6 +80,7 @@
     for u in range(TP):
         values = rows_ref[:, u].astype(jnp.float32) * factor
         normed_ref[u] = values.reshape(count, FEATS).astype(jnp.bfloat16)
+    own_ref[...] = rows_ref[place_ref[0]]
     gate = jnp.zeros((count, HIDDEN), jnp.float32)
     lift = jnp.zeros((count, HIDDEN), jnp.float32)
     for u in range(TP):
@@ -91,14 +98,20 @@
         out_ref[:, u] = down.reshape(blocks, ROWS, FEATS).astype(jnp.bfloat16)
 
 
-def first_partial(rows, weights):
+def first_partial(place, rows, weights):
+    vmem = pl.BlockSpec(memory_space=pltpu.VMEM)
     return pl.pallas_call(
         first_kernel,
-        out_shape=jax.ShapeDtypeStruct(rows.shape, jnp.bfloat16),
+        out_shape=[
+            pltpu.VMEM(rows.shape, jnp.bfloat16),
+            pltpu.VMEM(rows.shape[1:], jnp.bfloat16),
+        ],
         in_specs=[
-            pl.BlockSpec(memory_space=pltpu.VMEM),
+            pl.BlockSpec(memory_space=pltpu.SMEM),
+            vmem,
             pl.BlockSpec(memory_space=pltpu.HBM),
         ],
+        out_specs=[vmem, vmem],
         scratch_shapes=[
             pltpu.VMEM((TP, Z * Y * ROWS, FEATS), jnp.bfloat16),
             pltpu.VMEM(weights.shape, jnp.bfloat16),
@@ -106,59 +119,106 @@
         ],
         compiler_params=pltpu.CompilerParams(vmem_limit_bytes=24 << 20),
         name="first_ffn",
-    )(in_vmem(rows), in_hbm(weights))
-
-
-def second_kernel(place_ref, rows_ref, weights_ref, out_ref, normed_ref, sum_ref):
-    step = pl.program_id(0)
+    )(place, in_vmem(rows), in_hbm(weights))
+
+
+def settle_kernel(rows_ref, share_ref, first_ref, copies_ref):
+    for u in range(TP):
+        branch = jnp.sum(share_ref[:, u].astype(jnp.float32), axis=0)
+        own = rows_ref[u].astype(jnp.float32)
+        first = (own + 0.5 * branch).astype(jnp.bfloat16)
+        first_ref[u] = first
+        for t in range(TP):
+            copies_ref[t, u] = first
+
+
+def settled(rows, share):
+    shape = (TP, ROWS, FEATS)
+    vmem = pl.BlockSpec(memory_space=pltpu.VMEM)
+    return pl.pallas_call(
+        settle_kernel,
+        out_shape=[pltpu.VMEM(shape, jnp.bfloat16), pltpu.VMEM((TP, *shape), jnp.bfloat16)],
+        in_specs=[vmem, vmem],
+        out_specs=[vmem, vmem],
+        compiler_params=pltpu.CompilerParams(vmem_limit_bytes=24 << 20),
+        name="settle",
+    )(in_vmem(rows), in_vmem(share))
+
+
+def mix_kernel(first_ref, tiles_ref, copies_ref):
+    mixed = jnp.sum(tiles_ref[...].astype(jnp.float32), axis=0)
+    for u in range(TP):
+        cols = slice(u * FEATS, (u + 1) * FEATS)
+        rows = (first_ref[u].astype(jnp.float32) + mixed[:, cols]).astype(jnp.bfloat16)
+        for z in range(Z):
+            copies_ref[z, :, cols] = rows
+
+
+def mixed_copies(first, tiles):
+    vmem = pl.BlockSpec(memory_space=pltpu.VMEM)
+    return pl.pallas_call(
+        mix_kernel,
+        out_shape=pltpu.VMEM((Z, ROWS, D), jnp.bfloat16),
+        in_specs=[vmem, vmem],
+        out_specs=vmem,
+        compiler_params=pltpu.CompilerParams(vmem_limit_bytes=8 << 20),
+        name="mix",
+    )(in_vmem(first), in_vmem(tiles))
+
+
+def second_kernel(place_ref, rows_ref, weights_hbm, out_ref, normed_ref, weights_ref, arrived):
     rows = Z * ROWS
-
-    @pl.when(step == 0)
-    def _():
-        values = rows_ref[...].astype(jnp.float32).reshape(rows, D)
-        factor = lax.rsqrt(jnp.sum(values * values, axis=-1, keepdims=True) * (1.0 / D) + norm_eps)
-        row = lax.broadcasted_iota(jnp.int32, (rows, 1), 0)
-        own = jnp.where(row // ROWS == place_ref[0], 2.0, 0.0)
+    copies = [
+        pltpu.make_async_copy(weights_hbm.at[n], weights_ref.at[n], arrived.at[n])
+        for n in range(Y * TP)
+    ]
+    for copy in copies:
+        copy.start()
+    values = rows_ref[...].astype(jnp.float32).reshape(rows, D)
+    factor = lax.rsqrt(jnp.sum(values * values, axis=-1, keepdims=True) * (1.0 / D) + norm_eps)
+    row = lax.broadcasted_iota(jnp.int32, (rows, 1), 0)
+    own = jnp.where(row // ROWS == place_ref[1], 2.0, 0.0)
+    for u in range(TP):
+        normed_ref[u] = (values[:, u * FEATS : (u + 1) * FEATS] * factor).astype(jnp.bfloat16)
+    hidden = []
+    for y in range(Y):
+        both = jnp.zeros((2 * HIDDEN, rows), jnp.float32)
         for u in range(TP):
-            block = values[:, u * FEATS : (u + 1) * FEATS]
-            normed_ref[u] = (block * factor).astype(jnp.bfloat16)
-            sum_ref[u] = block * own
-
-    both = jnp.zeros((2 * HIDDEN, rows), jnp.float32)
-    for u in range(TP):
-        both += lax.dot_general(
-            weights_ref[0, u, : 2 * HIDDEN],
-            normed_ref[u],
-            by_rows,
-            preferred_element_type=jnp.float32,
-        )
-    gate, lift = both[:HIDDEN], both[HIDDEN:]
-    hidden = (gate * jax.nn.sigmoid(gate) * lift).T.astype(jnp.bfloat16)
-    for u in range(TP):
-        down = jnp.dot(hidden, weights_ref[0, u, 2 * HIDDEN :], preferred_element_type=jnp.float32)
-        sum_ref[u] = sum_ref[u] + down
-
-    @pl.when(step == pl.num_programs(0) - 1)
-    def _():
-        for u in range(TP):
-            out_ref[:, u] = sum_ref[u].reshape(Z, ROWS, FEATS).astype(jnp.bfloat16)
-
-
-def second_partial(rows, weights):
-    place = lax.axis_index("z").astype(jnp.int32).reshape(1)
+            copies[y * TP + u].wait()
+            both += lax.dot_general(
+                weights_ref[y * TP + u, : 2 * HIDDEN],
+                normed_ref[u],
+                by_rows,
+                preferred_element_type=jnp.float32,
+            )
+        gate, lift = both[:HIDDEN], both[HIDDEN:]
+        hidden.append((gate * jax.nn.sigmoid(gate) * lift).T.astype(jnp.bfloat16))
+    for u in range(TP):
+        down = values[:, u * FEATS : (u + 1) * FEATS] * own
+        for y in range(Y):
+            down += jnp.dot(
+                hidden[y],
+                weights_ref[y * TP + u, 2 * HIDDEN :],
+                preferred_element_type=jnp.float32,
+            )
+        out_ref[:, u] = down.reshape(Z, ROWS, FEATS).astype(jnp.bfloat16)
+
+
+def second_partial(place, rows, weights):
+    vmem = pl.BlockSpec(memory_space=pltpu.VMEM)
     return pl.pallas_call(
         second_kernel,
-        grid=(Y,),
-        out_shape=jax.ShapeDtypeStruct((Z, TP, ROWS, FEATS), jnp.bfloat16),
+        out_shape=pltpu.VMEM((Z, TP, ROWS, FEATS), jnp.bfloat16),
         in_specs=[
             pl.BlockSpec(memory_space=pltpu.SMEM),
-            pl.BlockSpec(memory_space=pltpu.VMEM),
-            pl.BlockSpec((1, TP, 3 * HIDDEN, FEATS), lambda i: (i, 0, 0, 0)),
-        ],
-        out_specs=pl.BlockSpec((Z, TP, ROWS, FEATS), lambda i: (0, 0, 0, 0)),
+            vmem,
+            pl.BlockSpec(memory_space=pltpu.HBM),
+        ],
+        out_specs=vmem,
         scratch_shapes=[
             pltpu.VMEM((TP, Z * ROWS, FEATS), jnp.bfloat16),
-            pltpu.VMEM((TP, Z * ROWS, FEATS), jnp.float32),
+            pltpu.VMEM(weights.shape, jnp.bfloat16),
+            pltpu.SemaphoreType.DMA((Y * TP,)),
         ],
         compiler_params=pltpu.CompilerParams(vmem_limit_bytes=24 << 20),
         name="second_ffn",
@@ -272,7 +332,7 @@
         for h in range(PER_DEVICE):
             top = h * HEAD_DIM
             kept = jnp.broadcast_to(retain[top : top + 8, b : b + 1], (8, STATE))
-            old = state_ref[b, h].reshape(HEAD_DIM // 8, 8, STATE) * kept[None]
+            old = state_ref[i * BLOCK + b, h].reshape(HEAD_DIM // 8, 8, STATE) * kept[None]
             new.append(
                 old.reshape(HEAD_DIM, STATE)
                 + added[top : top + HEAD_DIM, b : b + 1] * writes[b : b + 1]
@@ -302,28 +362,25 @@
         mixed_ref[...] = part.reshape(TP, ROWS, D).astype(jnp.bfloat16)
 
 
-def state_mixer(first, small, buffers, scan_state, group_gain, proj_output):
-    rows = sent_to_all(first, TP_AXES)
+def state_mixer(first, rows, small, buffers, scan_state, group_gain, proj_output):
     operands = [rows, *small, *[b.transpose(1, 0, 2) for b in buffers]]
     operands += [scan_state, group_gain, proj_output]
-    state_place = len(operands) - 3
-    from_hbm = (5, state_place, len(operands) - 1)
+    from_hbm = (5, len(operands) - 1)
     operands = [in_hbm(o) if n in from_hbm else in_vmem(o) for n, o in enumerate(operands)]
     specs = [pl.BlockSpec(memory_space=pltpu.VMEM) for _ in operands]
     for n in from_hbm:
         specs[n] = pl.BlockSpec(memory_space=pltpu.HBM)
     state_spec = pl.BlockSpec((BLOCK, PER_DEVICE, HEAD_DIM, STATE), lambda i: (i, 0, 0, 0))
-    specs[state_place] = state_spec
     blocks = SEQS // BLOCK
     partial_out, state_out = pl.pallas_call(
         mixer_kernel,
         grid=(blocks,),
         out_shape=[
-            jax.ShapeDtypeStruct((TP, ROWS, D), jnp.bfloat16),
+            pltpu.VMEM((TP, ROWS, D), jnp.bfloat16),
             jax.ShapeDtypeStruct(scan_state.shape, jnp.float32),
         ],
         in_specs=specs,
-        out_specs=[pl.BlockSpec((TP, ROWS, D), lambda i: (0, 0, 0)), state_spec],
+        out_specs=[pl.BlockSpec(memory_space=pltpu.VMEM), state_spec],
         scratch_shapes=[
             pltpu.VMEM((SEQS, D), jnp.bfloat16),
             pltpu.VMEM((SEQS, CHANNELS), jnp.bfloat16),
@@ -341,9 +398,7 @@
         name="mixer",
     )(*operands)
     tiles = lax.all_to_all(partial_out, TP_AXES, 0, 0, tiled=True)
-    mixed = jnp.sum(tiles.astype(jnp.float32), axis=0)
-    own = first.astype(jnp.float32).transpose(1, 0, 2).reshape(ROWS, D)
-    return ((own + mixed).astype(jnp.bfloat16), state_out)
+    return (mixed_copies(first, tiles), state_out)
 
 
 def per_device(
@@ -375,12 +430,13 @@
     second_lift,
     second_down,
 ):
+    place = jnp.stack([lax.axis_index(KV_AXES), lax.axis_index("z")]).astype(jnp.int32)
     weights_one = lax.all_gather(
         weight_share(first_gain, first_gate, first_lift, first_down), TP_AXES
     )
     weights_two = lax.all_gather(
-        weight_share(second_gain, second_gate, second_lift, second_down), ("y", *TP_AXES)
-    ).reshape(Y, TP, 3 * HIDDEN, FEATS)
+        weight_share(second_gain, second_gate, second_lift, second_down, place), ("y", *TP_AXES)
+    )
 
     split = residual.reshape(TP, ROWS, FEATS)
     tiles = lax.all_to_all(
@@ -390,14 +446,13 @@
         0,
         tiled=True,
     ).reshape(Z * Y, TP, ROWS, FEATS)
-    own_rows = lax.dynamic_index_in_dim(tiles, lax.axis_index(KV_AXES), 0, keepdims=False)
-    share = first_partial(tiles, weights_one)
+    share, own = first_partial(place, tiles, weights_one)
     share = lax.all_to_all(share, KV_AXES, 0, 0, tiled=True)
-    branch = jnp.sum(share.astype(jnp.float32), axis=0)
-    first = (own_rows.astype(jnp.float32) + 0.5 * branch).astype(jnp.bfloat16)
+    first, copies = settled(own, share)
 
     mixed, state_out = state_mixer(
         first,
+        lax.all_to_all(copies, TP_AXES, 0, 0, tiled=True),
         (
             mixer_gain,
             proj_gate,
@@ -418,7 +473,8 @@
         proj_output,
     )
 
-    share = second_partial(sent_to_all(mixed, "z"), weights_two)
+    rows = lax.all_to_all(mixed, "z", 0, 0, tiled=True)
+    share = second_partial(place, rows, weights_two)
     share = lax.all_to_all(
         share.reshape(-1, ROWS, FEATS), ("z", *TP_AXES), 0, 0, tiled=True
     ).reshape(Z, TP * ROWS, FEATS)

time: 150 us -> 145 us (0.967)
  blocking collectives: 73.7 us -> 109 us
  waiting for transfers between devices: 23.7 us -> 0.04 us
  starting transfers between devices: 13.1 us -> 0.08 us
  Pallas kernels: 21.1 us -> 18.9 us
    all_to_all x2 -> x4, blocking collectives: 21.4 us -> 56.7 us  [the longest x1 25 us: per_device(): share = lax.all_to_all(share, KV_AXES, 0, 0, tiled=True)]
    all_to_all x2 -> x0, waiting for transfers between devices: 23.6 us -> none  [the longest x1 16.5 us: per_device(): share = lax.all_to_all(share, KV_AXES, 0, 0, tiled=True)]
    all_to_all x2 -> x0, starting transfers between devices: 13 us -> none  [the longest x1 8.8 us: per_device(): share = lax.all_to_all(share, KV_AXES, 0, 0, tiled=True)]
    pallas_call x3 -> x5, Pallas kernels: 17.5 us -> 15.3 us  [the longest x1 6.21 us: second_partial(): pl.pallas_call(second_kernel, out_shape=pltpu.VMEM((Z, TP, ROWS, FEATS),...]
  transfers between devices with their start and end apart: 4 -> 2, of which waited for: 2 -> 0; matrix products, arithmetic and copies ran while one was open for 2% -> 1% of each run, Pallas kernels for 9% -> 8%
where the time goes in v6:
time: 145 us; the launch traced here: 144 us
  blocking collectives  109 us (75%)
  Pallas kernels  18.9 us (13%)
  between operations  14.3 us (10%)
    all_to_all x1, blocking collectives, per_device(): lax.all_to_all(jnp.broadcast_to(split[None], (Z * Y, TP, ROWS, FEATS)).re...  35.3 us
    all_to_all x1, blocking collectives, per_device(): share = lax.all_to_all(share, KV_AXES, 0, 0, tiled=True)  25 us
    all_to_all x1, blocking collectives, per_device(): lax.all_to_all(share.reshape(-1, ROWS, FEATS), ('z', *TP_AXES), 0, 0, til...  17.2 us
    all_to_all x1, blocking collectives, per_device(): lax.all_to_all(copies, TP_AXES, 0, 0, tiled=True)  11 us
    all_to_all x1, blocking collectives, per_device(): rows = lax.all_to_all(mixed, 'z', 0, 0, tiled=True)  10.3 us
    all_to_all x1, blocking collectives, state_mixer(): tiles = lax.all_to_all(partial_out, TP_AXES, 0, 0, tiled=True)  10.3 us
    pallas_call x1, Pallas kernels, second_partial(): pl.pallas_call(second_kernel, out_shape=pltpu.VMEM((Z, TP, ROWS, FEATS),...  6.21 us
    pallas_call x1, Pallas kernels, state_mixer(): pl.pallas_call(mixer_kernel, grid=(blocks,), out_shape=[pltpu.VMEM((TP, R...  5.83 us
  transfers between devices with their start and end apart: 2, of which 0 were waited for; matrix products, arithmetic and copies ran while one was open for 1% of the time, Pallas kernels for 8%

profile of v6, /device:TPU:1, one launch (start us, length us, event | category | flops | bytes accessed | tf_op | source)
XLA Modules:
  0.0 144.4 jit_solution(733090487033836882)
XLA Ops:
  7.2 0.0 copy-start.15
  7.2 0.0 copy-start.6
  7.2 0.0 copy-start.5
  7.2 0.0 copy-start.4
  7.2 0.0 copy-start.11
  7.2 0.0 copy-start.10
  7.2 0.0 copy-start.9
  7.2 0.0 copy-start.14
  7.3 0.0 copy-start.13
  7.3 0.0 copy-start.12
  7.3 0.0 copy-start.7
  7.3 0.0 copy-start.3
  7.3 0.0 copy-start.2
  7.3 0.0 copy-start.1
  7.3 0.0 copy-start.8
  7.3 0.0 all-gather.5.cloned.1.call-start
  7.4 1.9 %share.2 = bf16[528,256]{1,0:T(8,128)(2,1)} custom-call(bf16[256]{0:T(256)(128)(2,1)} %refs_0_.1, bf16[176,256]{1,0:T(8,128)(2,1)} %bitcast.24, bf16[176,256]{1,0:T(8,128)(2,1)} %bitcast.25, bf16[176,256]{1,0:T(8,128)(2,1)} %refs_3_.1), custom_call_target="tpu_custom_call" | custom-call | tf_op jit(solution)/shard_map/share/pallas_call | solution.py:54
  9.3 0.0 all-gather.5.cloned.1.call-update
  9.3 0.0 all-gather.7.cloned.1.call-start
  9.3 0.1 pad_add_fusion.place_ref.refs_0_
  9.4 1.8 %share.3 = bf16[528,256]{1,0:T(8,128)(2,1)} custom-call(s32[2]{0:T(128)S(1)} %pad_add_fusion.place_ref.refs_0_, bf16[256]{0:T(256)(128)(2,1)} %refs_1_.1, bf16[176,256]{1,0:T(8,128)(2,1)} %bitcast.26, bf16[176,256]{1,0:T(8,128)(2,1)} %bitcast.27, bf16[176,256]{1,0:T(8,128)(2,1)} %refs_4_.1), custom_call_target="tpu_custom_call" | custom-call | tf_op jit(solution)/shard_map/share/pallas_call | solution.py:54
  11.2 0.0 all-gather.7.cloned.1.call-update
  11.2 0.7 broadcast_in_dim.7
  11.9 0.2 broadcast_in_dim.8
  12.2 35.3 %all_to_all.30 = bf16[256,4,256]{2,1,0:T(4,128)(2,1)S(1)} all-to-all(bf16[256,4,256]{2,1,0:T(4,128)(2,1)S(1)} %bitcast.23), channel_id=1, replica_groups=mesh['z'=8,'y'=4,'x'=4,'core'=2] {'z','y','x','core'}, dimensions={0} | all-to-all | bytes 1048576 | tf_op jit(solution)/shard_map/all_to_all | solution.py:442
  47.5 0.0 all-gather.5.cloned.1.call-done
  47.5 0.0 copy-start
  47.5 3.0 %first_ffn.1 = (bf16[32,8,4,256]{3,2,1,0:T(4,128)(2,1)S(1)}, bf16[8,4,256]{2,1,0:T(4,128)(2,1)S(1)}) custom-call(s32[2]{0:T(128)S(1)} %pad_add_fusion.place_ref.refs_0_, bf16[32,8,4,256]{3,2,1,0:T(4,128)(2,1)S(1)} %bitcast.15, bf16[8,528,256]{2,1,0:T(8,128)(2,1)} %bitcast.22), custom_call_target="tpu_custom_call" | custom-call | tf_op jit(solution)/shard_map/first_ffn/pallas_call | solution.py:103
  50.5 25.0 %all_to_all.31.share_ref = bf16[32,8,4,256]{3,2,1,0:T(4,128)(2,1)S(1)} all-to-all(bf16[32,8,4,256]{3,2,1,0:T(4,128)(2,1)S(1)} %get-tuple-element.9), channel_id=1, replica_groups=mesh['z'=8,'y'=4,'x'=4,'core'=2] {'z','y'}, dimensions={0} | all-to-all | bytes 1048576 | tf_op jit(solution)/shard_map/all_to_all | solution.py:450
  75.5 0.2 settle.1
  75.7 11.0 %all_to_all.32.rows_ref = bf16[8,8,4,256]{3,2,1,0:T(4,128)(2,1)S(1)} all-to-all(bf16[8,8,4,256]{3,2,1,0:T(4,128)(2,1)S(1)} %get-tuple-element.11), channel_id=1, replica_groups=mesh['z'=8,'y'=4,'x'=4,'core'=2] {'x','core'}, dimensions={0} | all-to-all | bytes 262144 | tf_op jit(solution)/shard_map/all_to_all | solution.py:455
  86.7 0.0 copy-done.15
  86.7 0.0 copy-done.6
  86.7 0.0 copy-done.5
  86.7 0.0 copy-done.4
  86.7 0.0 copy-done.11
  86.7 0.0 copy-done.10
  86.7 0.0 copy-done.9
  86.8 0.0 copy-done.14
  86.8 0.0 copy-done.13
  86.8 0.0 copy-done.12
  86.8 0.0 copy-done.7
  86.8 0.0 copy-done.3
  86.8 0.0 copy-done.2
  86.8 0.0 copy-done.1
  86.8 0.0 copy-done.8
  86.8 0.0 copy-done
  86.8 5.8 %mixer.1 = (bf16[8,4,2048]{2,1,0:T(4,128)(2,1)S(1)}, f32[32,4,64,128]{3,2,1,0:T(8,128)}) custom-call(bf16[8,8,4,256]{3,2,1,0:T(4,128)(2,1)S(1)} %all_to_all.32.rows_ref, bf16[2048]{0:T(1024)(128)(2,1)S(1)} %copy-done.8, bf16[2048,256]{1,0:T(8,128)(2,1)S(1)} %copy-done.1, bf16[2048,256]{1,0:T(8,128)(2,1)S(1)} %copy-done.2, bf16[2048,128]{1,0:T(8,128)(2,1)S(1)} %copy-done.3, ...), custom_call_target="tpu_custom_call" | custom-call | tf_op jit(solution)/shard_map/mixer/pallas_call | solution.py:375
  92.7 10.3 %all_to_all.33.tiles_ref = bf16[8,4,2048]{2,1,0:T(4,128)(2,1)S(1)} all-to-all(bf16[8,4,2048]{2,1,0:T(4,128)(2,1)S(1)} %get-tuple-element.12), channel_id=1, replica_groups=mesh['z'=8,'y'=4,'x'=4,'core'=2] {'x','core'}, dimensions={0} | all-to-all | bytes 262144 | tf_op jit(solution)/shard_map/all_to_all | solution.py:400
  103.0 0.1 mix.1
  103.1 10.3 %all_to_all.34.rows_ref = bf16[8,4,2048]{2,1,0:T(4,128)(2,1)S(1)} all-to-all(bf16[8,4,2048]{2,1,0:T(4,128)(2,1)S(1)} %mix.1), channel_id=1, replica_groups=mesh['z'=8,'y'=4,'x'=4,'core'=2] {'z'}, dimensions={0} | all-to-all | bytes 262144 | tf_op jit(solution)/shard_map/all_to_all | solution.py:476
  113.4 0.0 all-gather.7.cloned.1.call-done
  113.4 6.2 %second_ffn.1 = bf16[8,8,4,256]{3,2,1,0:T(4,128)(2,1)S(1)} custom-call(s32[2]{0:T(128)S(1)} %pad_add_fusion.place_ref.refs_0_, bf16[8,4,2048]{2,1,0:T(4,128)(2,1)S(1)} %all_to_all.34.rows_ref, bf16[32,528,256]{2,1,0:T(8,128)(2,1)} %bitcast.21), custom_call_target="tpu_custom_call" | custom-call | tf_op jit(solution)/shard_map/second_ffn/pallas_call | solution.py:209
  119.6 17.2 %all_to_all.35 = bf16[64,4,256]{2,1,0:T(4,128)(2,1)S(1)} all-to-all(bf16[64,4,256]{2,1,0:T(4,128)(2,1)S(1)} %bitcast.16), channel_id=1, replica_groups=mesh['z'=8,'y'=4,'x'=4,'core'=2] {'z','x','core'}, dimensions={0} | all-to-all | bytes 262144 | tf_op jit(solution)/shard_map/all_to_all | solution.py:478
  136.9 0.6 multiply_convert_fusion
  (2 shorter events, 0.0 us)
Async XLA Ops:
  7.2 79.5 %copy-start.15 = (bf16[256]{0:T(256)(128)(2,1)S(1)}, bf16[256]{0:T(256)(128)(2,1)}, u32[]{:S(2)}) copy-start(bf16[256]{0:T(256)(128)(2,1)} %group_ref.1) | copy-start | bytes 1540
  7.2 79.5 %copy-start.6 = (bf16[32,3,128]{2,0,1:T(8,128)(2,1)S(1)}, bf16[32,3,128]{2,0,1:T(8,128)(2,1)}, u32[]{:S(2)}) copy-start(bf16[32,3,128]{2,0,1:T(8,128)(2,1)} %param.46) | copy-start | bytes 73732
  7.2 79.5 %copy-start.5 = (bf16[32,3,128]{2,0,1:T(8,128)(2,1)S(1)}, bf16[32,3,128]{2,0,1:T(8,128)(2,1)}, u32[]{:S(2)}) copy-start(bf16[32,3,128]{2,0,1:T(8,128)(2,1)} %param.45) | copy-start | bytes 73732
  7.2 79.5 %copy-start.4 = (bf16[32,3,256]{2,0,1:T(8,128)(2,1)S(1)}, bf16[32,3,256]{2,0,1:T(8,128)(2,1)}, u32[]{:S(2)}) copy-start(bf16[32,3,256]{2,0,1:T(8,128)(2,1)} %param.44) | copy-start | bytes 147460
  7.2 79.5 %copy-start.11 = (bf16[4,128]{1,0:T(4,128)(2,1)S(1)}, bf16[4,128]{1,0:T(4,128)(2,1)}, u32[]{:S(2)}) copy-start(bf16[4,128]{1,0:T(4,128)(2,1)} %taps_read_ref.1) | copy-start | bytes 3076
  7.2 79.5 %copy-start.10 = (bf16[4,128]{1,0:T(4,128)(2,1)S(1)}, bf16[4,128]{1,0:T(4,128)(2,1)}, u32[]{:S(2)}) copy-start(bf16[4,128]{1,0:T(4,128)(2,1)} %taps_write_ref.1) | copy-start | bytes 3076
  7.2 79.5 %copy-start.9 = (bf16[4,256]{1,0:T(4,128)(2,1)S(1)}, bf16[4,256]{1,0:T(4,128)(2,1)}, u32[]{:S(2)}) copy-start(bf16[4,256]{1,0:T(4,128)(2,1)} %taps_input_ref.1) | copy-start | bytes 6148
  7.2 79.5 %copy-start.14 = (f32[4]{0:T(128)S(1)}, f32[4]{0:T(128)}, u32[]{:S(2)}) copy-start(f32[4]{0:T(128)} %skip_ref.1) | copy-start | bytes 52
  7.3 79.5 %copy-start.13 = (f32[4]{0:T(128)S(1)}, f32[4]{0:T(128)}, u32[]{:S(2)}) copy-start(f32[4]{0:T(128)} %rate_ref.1) | copy-start | bytes 52
  7.3 79.5 %copy-start.12 = (f32[4]{0:T(128)S(1)}, f32[4]{0:T(128)}, u32[]{:S(2)}) copy-start(f32[4]{0:T(128)} %bias_ref.1) | copy-start | bytes 52
  7.3 79.5 %copy-start.7 = (bf16[2048,4]{0,1:T(4,128)(2,1)S(1)}, bf16[2048,4]{0,1:T(4,128)(2,1)}, u32[]{:S(2)}) copy-start(bf16[2048,4]{0,1:T(4,128)(2,1)} %param.37) | copy-start | bytes 49156
  7.3 79.5 %copy-start.3 = (bf16[2048,128]{1,0:T(8,128)(2,1)S(1)}, bf16[2048,128]{1,0:T(8,128)(2,1)}, u32[]{:S(2)}) copy-start(bf16[2048,128]{1,0:T(8,128)(2,1)} %write_ref.1) | copy-start | bytes 1572868
  7.3 79.5 %copy-start.2 = (bf16[2048,256]{1,0:T(8,128)(2,1)S(1)}, bf16[2048,256]{1,0:T(8,128)(2,1)}, u32[]{:S(2)}) copy-start(bf16[2048,256]{1,0:T(8,128)(2,1)} %input_ref.1) | copy-start | bytes 3145732
  7.3 79.5 %copy-start.1 = (bf16[2048,256]{1,0:T(8,128)(2,1)S(1)}, bf16[2048,256]{1,0:T(8,128)(2,1)}, u32[]{:S(2)}) copy-start(bf16[2048,256]{1,0:T(8,128)(2,1)} %gate_ref.1) | copy-start | bytes 3145732
  7.3 79.5 %copy-start.8 = (bf16[2048]{0:T(1024)(128)(2,1)S(1)}, bf16[2048]{0:T(1024)(128)(2,1)}, u32[]{:S(2)}) copy-start(bf16[2048]{0:T(1024)(128)(2,1)} %gain_ref.1) | copy-start | bytes 12292
  7.3 40.2 %all-gather.5.cloned.1.call-start = ((), (), s32[]{:S(2)}) async-start(), calls=%async_computation.6 | async-start | bytes 2433024 | tf_op jit(solution)/shard_map/all_gather | solution.py:434
  9.3 104.1 %all-gather.7.cloned.1.call-start = ((), (), s32[]{:S(2)}) async-start(), calls=%async_computation.7 | async-start | bytes 8921088 | tf_op jit(solution)/shard_map/all_gather | solution.py:437
  47.5 39.3 %copy-start = (f32[32,4,64,128]{3,2,1,0:T(8,128)S(1)}, f32[32,4,64,128]{3,2,1,0:T(8,128)}, u32[]{:S(2)}) copy-start(f32[32,4,64,128]{3,2,1,0:T(8,128)} %state_ref.1) | copy-start | bytes 12582916
Sparse Core Ops, SparseCore 0:
  10.5 35.5 all-gather.4
  48.6 61.9 all-gather.6

commit v7 on v6

--- a/solution.py
+++ b/solution.py
@@ -16,6 +16,7 @@
 
 KV_AXES = ("z", "y")
 TP_AXES = ("x", "core")
+BLOCK_AXES = ("y", "z")
 
 norm_eps = 1e-06
 
@@ -166,7 +167,9 @@
     )(in_vmem(first), in_vmem(tiles))
 
 
-def second_kernel(place_ref, rows_ref, weights_hbm, out_ref, normed_ref, weights_ref, arrived):
+def second_kernel(
+    place_ref, rows_ref, weights_hbm, out_ref, normed_ref, sum_ref, weights_ref, arrived
+):
     rows = Z * ROWS
     copies = [
         pltpu.make_async_copy(weights_hbm.at[n], weights_ref.at[n], arrived.at[n])
@@ -180,7 +183,6 @@
     own = jnp.where(row // ROWS == place_ref[1], 2.0, 0.0)
     for u in range(TP):
         normed_ref[u] = (values[:, u * FEATS : (u + 1) * FEATS] * factor).astype(jnp.bfloat16)
-    hidden = []
     for y in range(Y):
         both = jnp.zeros((2 * HIDDEN, rows), jnp.float32)
         for u in range(TP):
@@ -192,16 +194,19 @@
                 preferred_element_type=jnp.float32,
             )
         gate, lift = both[:HIDDEN], both[HIDDEN:]
-        hidden.append((gate * jax.nn.sigmoid(gate) * lift).T.astype(jnp.bfloat16))
-    for u in range(TP):
-        down = values[:, u * FEATS : (u + 1) * FEATS] * own
-        for y in range(Y):
-            down += jnp.dot(
-                hidden[y],
-                weights_ref[y * TP + u, 2 * HIDDEN :],
-                preferred_element_type=jnp.float32,
+        hidden = (gate * jax.nn.sigmoid(gate) * lift).T.astype(jnp.bfloat16)
+        for u in range(TP):
+            down = jnp.dot(
+                hidden, weights_ref[y * TP + u, 2 * HIDDEN :], preferred_element_type=jnp.float32
             )
-        out_ref[:, u] = down.reshape(Z, ROWS, FEATS).astype(jnp.bfloat16)
+            if y == 0:
+                down += values[:, u * FEATS : (u + 1) * FEATS] * own
+            else:
+                down += sum_ref[u]
+            if y < Y - 1:
+                sum_ref[u] = down
+            else:
+                out_ref[:, u] = down.reshape(Z, ROWS, FEATS).astype(jnp.bfloat16)
 
 
 def second_partial(place, rows, weights):
@@ -217,12 +222,28 @@
         out_specs=vmem,
         scratch_shapes=[
             pltpu.VMEM((TP, Z * ROWS, FEATS), jnp.bfloat16),
+            pltpu.VMEM((TP, Z * ROWS, FEATS), jnp.float32),
             pltpu.VMEM(weights.shape, jnp.bfloat16),
             pltpu.SemaphoreType.DMA((Y * TP,)),
         ],
         compiler_params=pltpu.CompilerParams(vmem_limit_bytes=24 << 20),
         name="second_ffn",
     )(place, in_vmem(rows), in_hbm(weights))
+
+
+def last_kernel(share_ref, out_ref):
+    branch = jnp.sum(share_ref[...].astype(jnp.float32), axis=0)
+    out_ref[...] = (0.5 * branch).reshape(TP * ROWS, FEATS).astype(jnp.bfloat16)
+
+
+def last_sum(share):
+    return pl.pallas_call(
+        last_kernel,
+        out_shape=jax.ShapeDtypeStruct((TP * ROWS, FEATS), jnp.bfloat16),
+        in_specs=[pl.BlockSpec(memory_space=pltpu.VMEM)],
+        compiler_params=pltpu.CompilerParams(vmem_limit_bytes=8 << 20),
+        name="last",
+    )(in_vmem(share))
 
 
 def conv_silu(newest, buffer_ref, taps_ref):
@@ -430,7 +451,7 @@
     second_lift,
     second_down,
 ):
-    place = jnp.stack([lax.axis_index(KV_AXES), lax.axis_index("z")]).astype(jnp.int32)
+    place = jnp.stack([lax.axis_index(BLOCK_AXES), lax.axis_index("z")]).astype(jnp.int32)
     weights_one = lax.all_gather(
         weight_share(first_gain, first_gate, first_lift, first_down), TP_AXES
     )
@@ -438,16 +459,10 @@
         weight_share(second_gain, second_gate, second_lift, second_down, place), ("y", *TP_AXES)
     )
 
-    split = residual.reshape(TP, ROWS, FEATS)
-    tiles = lax.all_to_all(
-        jnp.broadcast_to(split[None], (Z * Y, TP, ROWS, FEATS)).reshape(-1, ROWS, FEATS),
-        (*KV_AXES, *TP_AXES),
-        0,
-        0,
-        tiled=True,
-    ).reshape(Z * Y, TP, ROWS, FEATS)
+    mine = lax.all_to_all(residual.reshape(TP, ROWS, FEATS), TP_AXES, 0, 0, tiled=True)
+    tiles = sent_to_all(mine, BLOCK_AXES).reshape(Z * Y, TP, ROWS, FEATS)
     share, own = first_partial(place, tiles, weights_one)
-    share = lax.all_to_all(share, KV_AXES, 0, 0, tiled=True)
+    share = lax.all_to_all(share, BLOCK_AXES, 0, 0, tiled=True)
     first, copies = settled(own, share)
 
     mixed, state_out = state_mixer(
@@ -475,10 +490,8 @@
 
     rows = lax.all_to_all(mixed, "z", 0, 0, tiled=True)
     share = second_partial(place, rows, weights_two)
-    share = lax.all_to_all(
-        share.reshape(-1, ROWS, FEATS), ("z", *TP_AXES), 0, 0, tiled=True
-    ).reshape(Z, TP * ROWS, FEATS)
-    residual_out = (0.5 * jnp.sum(share.astype(jnp.float32), axis=0)).astype(jnp.bfloat16)
+    share = lax.all_to_all(share.reshape(-1, ROWS, FEATS), ("z", *TP_AXES), 0, 0, tiled=True)
+    residual_out = last_sum(share.reshape(Z, TP, ROWS, FEATS))
     return (residual_out, state_out)
 
 

time: 145 us -> 143 us (0.986)
  blocking collectives: 109 us -> 107 us
    all_to_all x2 -> x3, blocking collectives: 60.4 us -> 56.6 us  [the longest x1 25.6 us: sent_to_all(): lax.all_to_all(jnp.broadcast_to(array[None], (length, *array.shape)), axi...]
where the time goes in v7:
time: 143 us
  blocking collectives  107 us (75%)
  Pallas kernels  20.1 us (14%)
  between operations  14.3 us (10%)
    all_to_all x1, blocking collectives, sent_to_all(): lax.all_to_all(jnp.broadcast_to(array[None], (length, *array.shape)), axi...  25.6 us
    all_to_all x1, blocking collectives, per_device(): share = lax.all_to_all(share, BLOCK_AXES, 0, 0, tiled=True)  20.8 us
    all_to_all x1, blocking collectives, per_device(): lax.all_to_all(share.reshape(-1, ROWS, FEATS), ('z', *TP_AXES), 0, 0, til...  17 us
    all_to_all x1, blocking collectives, per_device(): lax.all_to_all(copies, TP_AXES, 0, 0, tiled=True)  12 us
    all_to_all x1, blocking collectives, per_device(): rows = lax.all_to_all(mixed, 'z', 0, 0, tiled=True)  11.4 us
    all_to_all x1, blocking collectives, state_mixer(): tiles = lax.all_to_all(partial_out, TP_AXES, 0, 0, tiled=True)  10.3 us
    all_to_all x1, blocking collectives, per_device(): lax.all_to_all(residual.reshape(TP, ROWS, FEATS), TP_AXES, 0, 0, tiled=True)  10.2 us
    pallas_call x1, Pallas kernels, second_partial(): pl.pallas_call(second_kernel, out_shape=pltpu.VMEM((Z, TP, ROWS, FEATS),...  6.71 us
  transfers between devices with their start and end apart: 2, of which 0 were waited for; matrix products, arithmetic and copies ran while one was open for 1% of the time, Pallas kernels for 8%

profile of v7, /device:TPU:1, one launch (start us, length us, event | category | flops | bytes accessed | tf_op | source)
XLA Modules:
  0.0 143.0 jit_solution(8396301238369561475)
XLA Ops:
  7.2 0.0 copy-start.15
  7.2 0.0 copy-start.6
  7.2 0.0 copy-start.5
  7.2 0.0 copy-start.4
  7.2 0.0 copy-start.11
  7.2 0.0 copy-start.10
  7.2 0.0 copy-start.9
  7.2 0.0 copy-start.14
  7.3 0.0 copy-start.13
  7.3 0.0 copy-start.12
  7.3 0.0 copy-start.7
  7.3 0.0 copy-start.3
  7.3 0.0 copy-start.2
  7.3 0.0 copy-start.1
  7.3 0.0 copy-start.8
  7.3 0.0 all-gather.5.cloned.1.call-start
  7.4 1.9 %share.2 = bf16[528,256]{1,0:T(8,128)(2,1)} custom-call(bf16[256]{0:T(256)(128)(2,1)} %refs_0_.1, bf16[176,256]{1,0:T(8,128)(2,1)} %bitcast.22, bf16[176,256]{1,0:T(8,128)(2,1)} %bitcast.23, bf16[176,256]{1,0:T(8,128)(2,1)} %refs_3_.1), custom_call_target="tpu_custom_call" | custom-call | tf_op jit(solution)/shard_map/share/pallas_call | solution.py:55
  9.3 0.0 all-gather.5.cloned.1.call-update
  9.3 0.0 all-gather.7.cloned.1.call-start
  9.3 0.1 pad_add_fusion.place_ref.refs_0_
  9.4 1.8 %share.3 = bf16[528,256]{1,0:T(8,128)(2,1)} custom-call(s32[2]{0:T(128)S(1)} %pad_add_fusion.place_ref.refs_0_, bf16[256]{0:T(256)(128)(2,1)} %refs_1_.1, bf16[176,256]{1,0:T(8,128)(2,1)} %bitcast.24, bf16[176,256]{1,0:T(8,128)(2,1)} %bitcast.25, bf16[176,256]{1,0:T(8,128)(2,1)} %refs_4_.1), custom_call_target="tpu_custom_call" | custom-call | tf_op jit(solution)/shard_map/share/pallas_call | solution.py:55
  11.2 0.0 all-gather.7.cloned.1.call-update
  11.2 0.7 reshape.14
  11.9 10.2 %all_to_all.35 = bf16[8,4,256]{2,1,0:T(4,128)(2,1)S(1)} all-to-all(bf16[8,4,256]{2,1,0:T(4,128)(2,1)S(1)} %reshape.14), channel_id=1, replica_groups=mesh['z'=8,'y'=4,'x'=4,'core'=2] {'x','core'}, dimensions={0} | all-to-all | bytes 32768 | tf_op jit(solution)/shard_map/all_to_all | solution.py:462
  22.1 0.2 broadcast_in_dim.2
  22.4 25.6 %all_to_all.36.rows_ref = bf16[32,8,4,256]{3,2,1,0:T(4,128)(2,1)S(1)} all-to-all(bf16[32,8,4,256]{3,2,1,0:T(4,128)(2,1)S(1)} %broadcast_in_dim.2), channel_id=1, replica_groups=mesh['z'=8,'y'=4,'x'=4,'core'=2] {'y','z'}, dimensions={0} | all-to-all | bytes 1048576 | tf_op jit(solution)/shard_map/all_to_all | solution.py:28
  48.0 0.0 all-gather.5.cloned.1.call-done
  48.0 0.0 copy-start
  48.0 3.0 %first_ffn.1 = (bf16[32,8,4,256]{3,2,1,0:T(4,128)(2,1)S(1)}, bf16[8,4,256]{2,1,0:T(4,128)(2,1)S(1)}) custom-call(s32[2]{0:T(128)S(1)} %pad_add_fusion.place_ref.refs_0_, bf16[32,8,4,256]{3,2,1,0:T(4,128)(2,1)S(1)} %all_to_all.36.rows_ref, bf16[8,528,256]{2,1,0:T(8,128)(2,1)} %bitcast.21), custom_call_target="tpu_custom_call" | custom-call | tf_op jit(solution)/shard_map/first_ffn/pallas_call | solution.py:104
  51.0 20.8 %all_to_all.37.share_ref = bf16[32,8,4,256]{3,2,1,0:T(4,128)(2,1)S(1)} all-to-all(bf16[32,8,4,256]{3,2,1,0:T(4,128)(2,1)S(1)} %get-tuple-element.9), channel_id=1, replica_groups=mesh['z'=8,'y'=4,'x'=4,'core'=2] {'y','z'}, dimensions={0} | all-to-all | bytes 1048576 | tf_op jit(solution)/shard_map/all_to_all | solution.py:465
  71.8 0.2 settle.1
  72.0 12.0 %all_to_all.38.rows_ref = bf16[8,8,4,256]{3,2,1,0:T(4,128)(2,1)S(1)} all-to-all(bf16[8,8,4,256]{3,2,1,0:T(4,128)(2,1)S(1)} %get-tuple-element.11), channel_id=1, replica_groups=mesh['z'=8,'y'=4,'x'=4,'core'=2] {'x','core'}, dimensions={0} | all-to-all | bytes 262144 | tf_op jit(solution)/shard_map/all_to_all | solution.py:470
  84.0 0.0 copy-done.15
  84.0 0.0 copy-done.6
  84.0 0.0 copy-done.5
  84.0 0.0 copy-done.4
  84.0 0.0 copy-done.11
  84.0 0.0 copy-done.10
  84.0 0.0 copy-done.9
  84.0 0.0 copy-done.14
  84.0 0.0 copy-done.13
  84.1 0.0 copy-done.12
  84.1 0.0 copy-done.7
  84.1 0.0 copy-done.3
  84.1 0.0 copy-done.2
  84.1 0.0 copy-done.1
  84.1 0.0 copy-done.8
  84.1 0.0 copy-done
  84.1 5.9 %mixer.1 = (bf16[8,4,2048]{2,1,0:T(4,128)(2,1)S(1)}, f32[32,4,64,128]{3,2,1,0:T(8,128)}) custom-call(bf16[8,8,4,256]{3,2,1,0:T(4,128)(2,1)S(1)} %all_to_all.38.rows_ref, bf16[2048]{0:T(1024)(128)(2,1)S(1)} %copy-done.8, bf16[2048,256]{1,0:T(8,128)(2,1)S(1)} %copy-done.1, bf16[2048,256]{1,0:T(8,128)(2,1)S(1)} %copy-done.2, bf16[2048,128]{1,0:T(8,128)(2,1)S(1)} %copy-done.3, ...), custom_call_target="tpu_custom_call" | custom-call | tf_op jit(solution)/shard_map/mixer/pallas_call | solution.py:396
  90.0 10.3 %all_to_all.39.tiles_ref = bf16[8,4,2048]{2,1,0:T(4,128)(2,1)S(1)} all-to-all(bf16[8,4,2048]{2,1,0:T(4,128)(2,1)S(1)} %get-tuple-element.12), channel_id=1, replica_groups=mesh['z'=8,'y'=4,'x'=4,'core'=2] {'x','core'}, dimensions={0} | all-to-all | bytes 262144 | tf_op jit(solution)/shard_map/all_to_all | solution.py:421
  100.3 0.1 mix.1
  100.4 11.4 %all_to_all.40.rows_ref = bf16[8,4,2048]{2,1,0:T(4,128)(2,1)S(1)} all-to-all(bf16[8,4,2048]{2,1,0:T(4,128)(2,1)S(1)} %mix.1), channel_id=1, replica_groups=mesh['z'=8,'y'=4,'x'=4,'core'=2] {'z'}, dimensions={0} | all-to-all | bytes 262144 | tf_op jit(solution)/shard_map/all_to_all | solution.py:491
  111.8 0.0 all-gather.7.cloned.1.call-done
  111.8 6.7 %second_ffn.1 = bf16[8,8,4,256]{3,2,1,0:T(4,128)(2,1)S(1)} custom-call(s32[2]{0:T(128)S(1)} %pad_add_fusion.place_ref.refs_0_, bf16[8,4,2048]{2,1,0:T(4,128)(2,1)S(1)} %all_to_all.40.rows_ref, bf16[32,528,256]{2,1,0:T(8,128)(2,1)} %bitcast.20), custom_call_target="tpu_custom_call" | custom-call | tf_op jit(solution)/shard_map/second_ffn/pallas_call | solution.py:214
  118.5 17.0 %all_to_all.41 = bf16[64,4,256]{2,1,0:T(4,128)(2,1)S(1)} all-to-all(bf16[64,4,256]{2,1,0:T(4,128)(2,1)S(1)} %bitcast.14), channel_id=1, replica_groups=mesh['z'=8,'y'=4,'x'=4,'core'=2] {'z','x','core'}, dimensions={0} | all-to-all | bytes 262144 | tf_op jit(solution)/shard_map/all_to_all | solution.py:493
  135.5 0.7 last.1
Async XLA Ops:
  7.2 76.8 %copy-start.15 = (bf16[256]{0:T(256)(128)(2,1)S(1)}, bf16[256]{0:T(256)(128)(2,1)}, u32[]{:S(2)}) copy-start(bf16[256]{0:T(256)(128)(2,1)} %group_ref.1) | copy-start | bytes 1540
  7.2 76.8 %copy-start.6 = (bf16[32,3,128]{2,0,1:T(8,128)(2,1)S(1)}, bf16[32,3,128]{2,0,1:T(8,128)(2,1)}, u32[]{:S(2)}) copy-start(bf16[32,3,128]{2,0,1:T(8,128)(2,1)} %param.46) | copy-start | bytes 73732
  7.2 76.8 %copy-start.5 = (bf16[32,3,128]{2,0,1:T(8,128)(2,1)S(1)}, bf16[32,3,128]{2,0,1:T(8,128)(2,1)}, u32[]{:S(2)}) copy-start(bf16[32,3,128]{2,0,1:T(8,128)(2,1)} %param.45) | copy-start | bytes 73732
  7.2 76.8 %copy-start.4 = (bf16[32,3,256]{2,0,1:T(8,128)(2,1)S(1)}, bf16[32,3,256]{2,0,1:T(8,128)(2,1)}, u32[]{:S(2)}) copy-start(bf16[32,3,256]{2,0,1:T(8,128)(2,1)} %param.44) | copy-start | bytes 147460
  7.2 76.8 %copy-start.11 = (bf16[4,128]{1,0:T(4,128)(2,1)S(1)}, bf16[4,128]{1,0:T(4,128)(2,1)}, u32[]{:S(2)}) copy-start(bf16[4,128]{1,0:T(4,128)(2,1)} %taps_read_ref.1) | copy-start | bytes 3076
  7.2 76.8 %copy-start.10 = (bf16[4,128]{1,0:T(4,128)(2,1)S(1)}, bf16[4,128]{1,0:T(4,128)(2,1)}, u32[]{:S(2)}) copy-start(bf16[4,128]{1,0:T(4,128)(2,1)} %taps_write_ref.1) | copy-start | bytes 3076
  7.2 76.8 %copy-start.9 = (bf16[4,256]{1,0:T(4,128)(2,1)S(1)}, bf16[4,256]{1,0:T(4,128)(2,1)}, u32[]{:S(2)}) copy-start(bf16[4,256]{1,0:T(4,128)(2,1)} %taps_input_ref.1) | copy-start | bytes 6148
  7.2 76.8 %copy-start.14 = (f32[4]{0:T(128)S(1)}, f32[4]{0:T(128)}, u32[]{:S(2)}) copy-start(f32[4]{0:T(128)} %skip_ref.1) | copy-start | bytes 52
  7.3 76.8 %copy-start.13 = (f32[4]{0:T(128)S(1)}, f32[4]{0:T(128)}, u32[]{:S(2)}) copy-start(f32[4]{0:T(128)} %rate_ref.1) | copy-start | bytes 52
  7.3 76.8 %copy-start.12 = (f32[4]{0:T(128)S(1)}, f32[4]{0:T(128)}, u32[]{:S(2)}) copy-start(f32[4]{0:T(128)} %bias_ref.1) | copy-start | bytes 52
  7.3 76.8 %copy-start.7 = (bf16[2048,4]{0,1:T(4,128)(2,1)S(1)}, bf16[2048,4]{0,1:T(4,128)(2,1)}, u32[]{:S(2)}) copy-start(bf16[2048,4]{0,1:T(4,128)(2,1)} %param.37) | copy-start | bytes 49156
  7.3 76.8 %copy-start.3 = (bf16[2048,128]{1,0:T(8,128)(2,1)S(1)}, bf16[2048,128]{1,0:T(8,128)(2,1)}, u32[]{:S(2)}) copy-start(bf16[2048,128]{1,0:T(8,128)(2,1)} %write_ref.1) | copy-start | bytes 1572868
  7.3 76.8 %copy-start.2 = (bf16[2048,256]{1,0:T(8,128)(2,1)S(1)}, bf16[2048,256]{1,0:T(8,128)(2,1)}, u32[]{:S(2)}) copy-start(bf16[2048,256]{1,0:T(8,128)(2,1)} %input_ref.1) | copy-start | bytes 3145732
  7.3 76.8 %copy-start.1 = (bf16[2048,256]{1,0:T(8,128)(2,1)S(1)}, bf16[2048,256]{1,0:T(8,128)(2,1)}, u32[]{:S(2)}) copy-start(bf16[2048,256]{1,0:T(8,128)(2,1)} %gate_ref.1) | copy-start | bytes 3145732
  7.3 76.8 %copy-start.8 = (bf16[2048]{0:T(1024)(128)(2,1)S(1)}, bf16[2048]{0:T(1024)(128)(2,1)}, u32[]{:S(2)}) copy-start(bf16[2048]{0:T(1024)(128)(2,1)} %gain_ref.1) | copy-start | bytes 12292
  7.3 40.7 %all-gather.5.cloned.1.call-start = ((), (), s32[]{:S(2)}) async-start(), calls=%async_computation.7 | async-start | bytes 2433024 | tf_op jit(solution)/shard_map/all_gather | solution.py:455
  9.3 102.5 %all-gather.7.cloned.1.call-start = ((), (), s32[]{:S(2)}) async-start(), calls=%async_computation.8 | async-start | bytes 8921088 | tf_op jit(solution)/shard_map/all_gather | solution.py:458
  48.0 36.1 %copy-start = (f32[32,4,64,128]{3,2,1,0:T(8,128)S(1)}, f32[32,4,64,128]{3,2,1,0:T(8,128)}, u32[]{:S(2)}) copy-start(f32[32,4,64,128]{3,2,1,0:T(8,128)} %state_ref.1) | copy-start | bytes 12582916
Sparse Core Ops, SparseCore 0:
  10.5 32.0 all-gather.4
  45.2 62.7 all-gather.6

commit v8 on v7

--- a/solution.py
+++ b/solution.py
@@ -42,24 +42,32 @@
     return pltpu.with_memory_space_constraint(array, pltpu.VMEM)
 
 
-def share_kernel(*refs):
-    gain, gate, lift, down, out = refs[-5:]
-    gain_f = gain[...].astype(jnp.float32).reshape(1, FEATS)
-    out[:HIDDEN] = (gate[...].astype(jnp.float32) * gain_f).astype(jnp.bfloat16)
-    out[HIDDEN : 2 * HIDDEN] = (lift[...].astype(jnp.float32) * gain_f).astype(jnp.bfloat16)
-    out[2 * HIDDEN :] = down[...]
-
-
-def weight_share(gain, gate_weight, lift_weight, down_weight, *early):
-    operands = [gain, gate_weight.T, lift_weight.T, down_weight]
+def share_kernel(place_ref, rows_ref, *refs):
+    pieces_ref = refs[-1]
+    pieces_ref[...] = rows_ref[...].astype(jnp.float32).reshape(TP, ROWS, FEATS).astype(
+        jnp.bfloat16
+    )
+    for gain, gate, lift, down, out in (refs[0:4] + refs[8:9], refs[4:8] + refs[9:10]):
+        gain_f = gain[...].astype(jnp.float32).reshape(1, FEATS)
+        out[:HIDDEN] = (gate[...].astype(jnp.float32) * gain_f).astype(jnp.bfloat16)
+        out[HIDDEN : 2 * HIDDEN] = (lift[...].astype(jnp.float32) * gain_f).astype(jnp.bfloat16)
+        out[2 * HIDDEN :] = down[...]
+
+
+def weight_shares(place, residual, *sets):
+    operands = [residual]
+    for gain, gate_weight, lift_weight, down_weight in sets:
+        operands += [gain, gate_weight.T, lift_weight.T, down_weight]
+    vmem = pl.BlockSpec(memory_space=pltpu.VMEM)
+    share = jax.ShapeDtypeStruct((3 * HIDDEN, FEATS), jnp.bfloat16)
     return pl.pallas_call(
         share_kernel,
-        out_shape=jax.ShapeDtypeStruct((3 * HIDDEN, FEATS), jnp.bfloat16),
+        out_shape=[share, share, pltpu.VMEM((TP, ROWS, FEATS), jnp.bfloat16)],
         compiler_params=pltpu.CompilerParams(vmem_limit_bytes=4 << 20),
-        in_specs=[pl.BlockSpec(memory_space=pltpu.SMEM) for _ in early]
-        + [pl.BlockSpec(memory_space=pltpu.VMEM) for _ in operands],
-        name="share",
-    )(*early, *[in_hbm(operand) for operand in operands])
+        in_specs=[pl.BlockSpec(memory_space=pltpu.SMEM)] + [vmem for _ in operands],
+        out_specs=[vmem] * 3,
+        name="shares",
+    )(place, *[in_hbm(operand) for operand in operands])
 
 
 def first_kernel(
@@ -168,7 +176,7 @@
 
 
 def second_kernel(
-    place_ref, rows_ref, weights_hbm, out_ref, normed_ref, sum_ref, weights_ref, arrived
+    place_ref, rows_ref, weights_hbm, out_ref, normed_ref, weights_ref, arrived
 ):
     rows = Z * ROWS
     copies = [
@@ -183,30 +191,29 @@
     own = jnp.where(row // ROWS == place_ref[1], 2.0, 0.0)
     for u in range(TP):
         normed_ref[u] = (values[:, u * FEATS : (u + 1) * FEATS] * factor).astype(jnp.bfloat16)
+    hidden = []
     for y in range(Y):
-        both = jnp.zeros((2 * HIDDEN, rows), jnp.float32)
+        both = jnp.zeros((rows, 2 * HIDDEN), jnp.float32)
         for u in range(TP):
             copies[y * TP + u].wait()
+        for u in range(TP):
             both += lax.dot_general(
+                normed_ref[u],
                 weights_ref[y * TP + u, : 2 * HIDDEN],
-                normed_ref[u],
                 by_rows,
                 preferred_element_type=jnp.float32,
             )
-        gate, lift = both[:HIDDEN], both[HIDDEN:]
-        hidden = (gate * jax.nn.sigmoid(gate) * lift).T.astype(jnp.bfloat16)
-        for u in range(TP):
-            down = jnp.dot(
-                hidden, weights_ref[y * TP + u, 2 * HIDDEN :], preferred_element_type=jnp.float32
+        gate, lift = both[:, :HIDDEN], both[:, HIDDEN:]
+        hidden.append((gate * jax.nn.sigmoid(gate) * lift).astype(jnp.bfloat16))
+    for u in range(TP):
+        down = values[:, u * FEATS : (u + 1) * FEATS] * own
+        for y in range(Y):
+            down += jnp.dot(
+                hidden[y],
+                weights_ref[y * TP + u, 2 * HIDDEN :],
+                preferred_element_type=jnp.float32,
             )
-            if y == 0:
-                down += values[:, u * FEATS : (u + 1) * FEATS] * own
-            else:
-                down += sum_ref[u]
-            if y < Y - 1:
-                sum_ref[u] = down
-            else:
-                out_ref[:, u] = down.reshape(Z, ROWS, FEATS).astype(jnp.bfloat16)
+        out_ref[:, u] = down.reshape(Z, ROWS, FEATS).astype(jnp.bfloat16)
 
 
 def second_partial(place, rows, weights):
@@ -222,7 +229,6 @@
         out_specs=vmem,
         scratch_shapes=[
             pltpu.VMEM((TP, Z * ROWS, FEATS), jnp.bfloat16),
-            pltpu.VMEM((TP, Z * ROWS, FEATS), jnp.float32),
             pltpu.VMEM(weights.shape, jnp.bfloat16),
             pltpu.SemaphoreType.DMA((Y * TP,)),
         ],
@@ -452,14 +458,16 @@
     second_down,
 ):
     place = jnp.stack([lax.axis_index(BLOCK_AXES), lax.axis_index("z")]).astype(jnp.int32)
-    weights_one = lax.all_gather(
-        weight_share(first_gain, first_gate, first_lift, first_down), TP_AXES
+    share_one, share_two, pieces = weight_shares(
+        place,
+        residual,
+        (first_gain, first_gate, first_lift, first_down),
+        (second_gain, second_gate, second_lift, second_down),
     )
-    weights_two = lax.all_gather(
-        weight_share(second_gain, second_gate, second_lift, second_down, place), ("y", *TP_AXES)
-    )
-
-    mine = lax.all_to_all(residual.reshape(TP, ROWS, FEATS), TP_AXES, 0, 0, tiled=True)
+    weights_one = lax.all_gather(share_one, TP_AXES)
+    weights_two = lax.all_gather(share_two, ("y", *TP_AXES))
+
+    mine = lax.all_to_all(pieces, TP_AXES, 0, 0, tiled=True)
     tiles = sent_to_all(mine, BLOCK_AXES).reshape(Z * Y, TP, ROWS, FEATS)
     share, own = first_partial(place, tiles, weights_one)
     share = lax.all_to_all(share, BLOCK_AXES, 0, 0, tiled=True)

time: 143 us -> 142 us (level)
  Pallas kernels: 20.1 us -> 18.5 us
    pallas_call x2 -> x1, Pallas kernels: 3.64 us -> 2.14 us  [weight_shares(): pl.pallas_call(share_kernel, out_shape=[share, share, pltpu.VMEM((TP, ROW...]
  transfers between devices with their start and end apart: 2 -> 2, of which waited for: 0 -> 0; matrix products, arithmetic and copies ran while one was open for 1% -> 0% of each run, Pallas kernels for 8% -> 6%
where the time goes in v8:
time: 142 us; the launch traced here: 141 us
  blocking collectives  107 us (75%)
  Pallas kernels  18.5 us (13%)
  between operations  14.3 us (10%)
    all_to_all x1, blocking collectives, sent_to_all(): lax.all_to_all(jnp.broadcast_to(array[None], (length, *array.shape)), axi...  25.6 us
    all_to_all x1, blocking collectives, per_device(): share = lax.all_to_all(share, BLOCK_AXES, 0, 0, tiled=True)  20.8 us
    all_to_all x1, blocking collectives, per_device(): lax.all_to_all(share.reshape(-1, ROWS, FEATS), ('z', *TP_AXES), 0, 0, til...  17 us
    all_to_all x1, blocking collectives, per_device(): lax.all_to_all(copies, TP_AXES, 0, 0, tiled=True)  12 us
    all_to_all x1, blocking collectives, per_device(): rows = lax.all_to_all(mixed, 'z', 0, 0, tiled=True)  11.2 us
    all_to_all x1, blocking collectives, state_mixer(): tiles = lax.all_to_all(partial_out, TP_AXES, 0, 0, tiled=True)  10.3 us
    all_to_all x1, blocking collectives, per_device(): mine = lax.all_to_all(pieces, TP_AXES, 0, 0, tiled=True)  10.2 us
    pallas_call x1, Pallas kernels, second_partial(): pl.pallas_call(second_kernel, out_shape=pltpu.VMEM((Z, TP, ROWS, FEATS),...  6.53 us
  transfers between devices with their start and end apart: 2, of which 0 were waited for; matrix products, arithmetic and copies ran while one was open for 0% of the time, Pallas kernels for 6%

profile of v8, /device:TPU:1, one launch (start us, length us, event | category | flops | bytes accessed | tf_op | source)
XLA Modules:
  0.0 141.2 jit_solution(10542328271391654821)
XLA Ops:
  7.2 0.0 copy-start.15
  7.2 0.0 copy-start.6
  7.2 0.0 copy-start.5
  7.2 0.0 copy-start.4
  7.2 0.0 copy-start.11
  7.2 0.0 copy-start.10
  7.2 0.0 copy-start.9
  7.2 0.0 copy-start.14
  7.3 0.0 copy-start.13
  7.3 0.0 copy-start.12
  7.3 0.0 copy-start.7
  7.3 0.0 copy-start.3
  7.3 0.0 copy-start.2
  7.3 0.0 copy-start.1
  7.3 0.0 copy-start.8
  7.3 0.0 all-gather.5.cloned.1.call-start
  7.4 0.1 pad_add_fusion.place_ref
  7.4 2.1 %shares.1 = (bf16[528,256]{1,0:T(8,128)(2,1)}, bf16[528,256]{1,0:T(8,128)(2,1)}, bf16[8,4,256]{2,1,0:T(4,128)(2,1)S(1)}) custom-call(s32[2]{0:T(128)S(1)} %pad_add_fusion.place_ref, bf16[32,256]{1,0:T(8,128)(2,1)} %rows_ref.1, bf16[256]{0:T(256)(128)(2,1)} %refs_0_.1, bf16[176,256]{1,0:T(8,128)(2,1)} %bitcast.22, bf16[176,256]{1,0:T(8,128)(2,1)} %bitcast.23, ...), custom_call_target="tpu_custom_call" | custom-call | tf_op jit(solution)/shard_map/shares/pallas_call | solution.py:63
  9.6 0.0 all-gather.5.cloned.1.call-update
  9.6 0.0 all-gather.7.cloned.1.call-start
  9.7 0.7 all-gather.7.cloned.1.call-update
  10.4 10.2 %all_to_all.35 = bf16[8,4,256]{2,1,0:T(4,128)(2,1)S(1)} all-to-all(bf16[8,4,256]{2,1,0:T(4,128)(2,1)S(1)} %get-tuple-element.11), channel_id=1, replica_groups=mesh['z'=8,'y'=4,'x'=4,'core'=2] {'x','core'}, dimensions={0} | all-to-all | bytes 32768 | tf_op jit(solution)/shard_map/all_to_all | solution.py:470
  20.6 0.2 broadcast_in_dim.2
  20.8 25.6 %all_to_all.36.rows_ref = bf16[32,8,4,256]{3,2,1,0:T(4,128)(2,1)S(1)} all-to-all(bf16[32,8,4,256]{3,2,1,0:T(4,128)(2,1)S(1)} %broadcast_in_dim.2), channel_id=1, replica_groups=mesh['z'=8,'y'=4,'x'=4,'core'=2] {'y','z'}, dimensions={0} | all-to-all | bytes 1048576 | tf_op jit(solution)/shard_map/all_to_all | solution.py:28
  46.5 0.0 all-gather.5.cloned.1.call-done
  46.5 0.0 copy-start
  46.5 3.0 %first_ffn.1 = (bf16[32,8,4,256]{3,2,1,0:T(4,128)(2,1)S(1)}, bf16[8,4,256]{2,1,0:T(4,128)(2,1)S(1)}) custom-call(s32[2]{0:T(128)S(1)} %pad_add_fusion.place_ref, bf16[32,8,4,256]{3,2,1,0:T(4,128)(2,1)S(1)} %all_to_all.36.rows_ref, bf16[8,528,256]{2,1,0:T(8,128)(2,1)} %bitcast.21), custom_call_target="tpu_custom_call" | custom-call | tf_op jit(solution)/shard_map/first_ffn/pallas_call | solution.py:112
  49.5 20.8 %all_to_all.37.share_ref = bf16[32,8,4,256]{3,2,1,0:T(4,128)(2,1)S(1)} all-to-all(bf16[32,8,4,256]{3,2,1,0:T(4,128)(2,1)S(1)} %get-tuple-element.14), channel_id=1, replica_groups=mesh['z'=8,'y'=4,'x'=4,'core'=2] {'y','z'}, dimensions={0} | all-to-all | bytes 1048576 | tf_op jit(solution)/shard_map/all_to_all | solution.py:473
  70.2 0.2 settle.1
  70.5 12.0 %all_to_all.38.rows_ref = bf16[8,8,4,256]{3,2,1,0:T(4,128)(2,1)S(1)} all-to-all(bf16[8,8,4,256]{3,2,1,0:T(4,128)(2,1)S(1)} %get-tuple-element.16), channel_id=1, replica_groups=mesh['z'=8,'y'=4,'x'=4,'core'=2] {'x','core'}, dimensions={0} | all-to-all | bytes 262144 | tf_op jit(solution)/shard_map/all_to_all | solution.py:478
  82.4 0.0 copy-done.15
  82.4 0.0 copy-done.6
  82.4 0.0 copy-done.5
  82.4 0.0 copy-done.4
  82.5 0.0 copy-done.11
  82.5 0.0 copy-done.10
  82.5 0.0 copy-done.9
  82.5 0.0 copy-done.14
  82.5 0.0 copy-done.13
  82.5 0.0 copy-done.12
  82.5 0.0 copy-done.7
  82.5 0.0 copy-done.3
  82.5 0.0 copy-done.2
  82.5 0.0 copy-done.1
  82.6 0.0 copy-done.8
  82.6 0.0 copy-done
  82.6 5.9 %mixer.1 = (bf16[8,4,2048]{2,1,0:T(4,128)(2,1)S(1)}, f32[32,4,64,128]{3,2,1,0:T(8,128)}) custom-call(bf16[8,8,4,256]{3,2,1,0:T(4,128)(2,1)S(1)} %all_to_all.38.rows_ref, bf16[2048]{0:T(1024)(128)(2,1)S(1)} %copy-done.8, bf16[2048,256]{1,0:T(8,128)(2,1)S(1)} %copy-done.1, bf16[2048,256]{1,0:T(8,128)(2,1)S(1)} %copy-done.2, bf16[2048,128]{1,0:T(8,128)(2,1)S(1)} %copy-done.3, ...), custom_call_target="tpu_custom_call" | custom-call | tf_op jit(solution)/shard_map/mixer/pallas_call | solution.py:402
  88.5 10.3 %all_to_all.39.tiles_ref = bf16[8,4,2048]{2,1,0:T(4,128)(2,1)S(1)} all-to-all(bf16[8,4,2048]{2,1,0:T(4,128)(2,1)S(1)} %get-tuple-element.17), channel_id=1, replica_groups=mesh['z'=8,'y'=4,'x'=4,'core'=2] {'x','core'}, dimensions={0} | all-to-all | bytes 262144 | tf_op jit(solution)/shard_map/all_to_all | solution.py:427
  98.8 0.1 mix.1
  98.9 11.2 %all_to_all.40.rows_ref = bf16[8,4,2048]{2,1,0:T(4,128)(2,1)S(1)} all-to-all(bf16[8,4,2048]{2,1,0:T(4,128)(2,1)S(1)} %mix.1), channel_id=1, replica_groups=mesh['z'=8,'y'=4,'x'=4,'core'=2] {'z'}, dimensions={0} | all-to-all | bytes 262144 | tf_op jit(solution)/shard_map/all_to_all | solution.py:499
  110.1 0.0 all-gather.7.cloned.1.call-done
  110.1 6.5 %second_ffn.1 = bf16[8,8,4,256]{3,2,1,0:T(4,128)(2,1)S(1)} custom-call(s32[2]{0:T(128)S(1)} %pad_add_fusion.place_ref, bf16[8,4,2048]{2,1,0:T(4,128)(2,1)S(1)} %all_to_all.40.rows_ref, bf16[32,528,256]{2,1,0:T(8,128)(2,1)} %bitcast.20), custom_call_target="tpu_custom_call" | custom-call | tf_op jit(solution)/shard_map/second_ffn/pallas_call | solution.py:221
  116.7 17.0 %all_to_all.41 = bf16[64,4,256]{2,1,0:T(4,128)(2,1)S(1)} all-to-all(bf16[64,4,256]{2,1,0:T(4,128)(2,1)S(1)} %bitcast.14), channel_id=1, replica_groups=mesh['z'=8,'y'=4,'x'=4,'core'=2] {'z','x','core'}, dimensions={0} | all-to-all | bytes 262144 | tf_op jit(solution)/shard_map/all_to_all | solution.py:501
  133.7 0.7 last.1
Async XLA Ops:
  7.2 75.3 %copy-start.15 = (bf16[256]{0:T(256)(128)(2,1)S(1)}, bf16[256]{0:T(256)(128)(2,1)}, u32[]{:S(2)}) copy-start(bf16[256]{0:T(256)(128)(2,1)} %group_ref.1) | copy-start | bytes 1540
  7.2 75.3 %copy-start.6 = (bf16[32,3,128]{2,0,1:T(8,128)(2,1)S(1)}, bf16[32,3,128]{2,0,1:T(8,128)(2,1)}, u32[]{:S(2)}) copy-start(bf16[32,3,128]{2,0,1:T(8,128)(2,1)} %param.46) | copy-start | bytes 73732
  7.2 75.3 %copy-start.5 = (bf16[32,3,128]{2,0,1:T(8,128)(2,1)S(1)}, bf16[32,3,128]{2,0,1:T(8,128)(2,1)}, u32[]{:S(2)}) copy-start(bf16[32,3,128]{2,0,1:T(8,128)(2,1)} %param.45) | copy-start | bytes 73732
  7.2 75.2 %copy-start.4 = (bf16[32,3,256]{2,0,1:T(8,128)(2,1)S(1)}, bf16[32,3,256]{2,0,1:T(8,128)(2,1)}, u32[]{:S(2)}) copy-start(bf16[32,3,256]{2,0,1:T(8,128)(2,1)} %param.44) | copy-start | bytes 147460
  7.2 75.2 %copy-start.11 = (bf16[4,128]{1,0:T(4,128)(2,1)S(1)}, bf16[4,128]{1,0:T(4,128)(2,1)}, u32[]{:S(2)}) copy-start(bf16[4,128]{1,0:T(4,128)(2,1)} %taps_read_ref.1) | copy-start | bytes 3076
  7.2 75.2 %copy-start.10 = (bf16[4,128]{1,0:T(4,128)(2,1)S(1)}, bf16[4,128]{1,0:T(4,128)(2,1)}, u32[]{:S(2)}) copy-start(bf16[4,128]{1,0:T(4,128)(2,1)} %taps_write_ref.1) | copy-start | bytes 3076
  7.2 75.2 %copy-start.9 = (bf16[4,256]{1,0:T(4,128)(2,1)S(1)}, bf16[4,256]{1,0:T(4,128)(2,1)}, u32[]{:S(2)}) copy-start(bf16[4,256]{1,0:T(4,128)(2,1)} %taps_input_ref.1) | copy-start | bytes 6148
  7.2 75.2 %copy-start.14 = (f32[4]{0:T(128)S(1)}, f32[4]{0:T(128)}, u32[]{:S(2)}) copy-start(f32[4]{0:T(128)} %skip_ref.1) | copy-start | bytes 52
  7.3 75.2 %copy-start.13 = (f32[4]{0:T(128)S(1)}, f32[4]{0:T(128)}, u32[]{:S(2)}) copy-start(f32[4]{0:T(128)} %rate_ref.1) | copy-start | bytes 52
  7.3 75.2 %copy-start.12 = (f32[4]{0:T(128)S(1)}, f32[4]{0:T(128)}, u32[]{:S(2)}) copy-start(f32[4]{0:T(128)} %bias_ref.1) | copy-start | bytes 52
  7.3 75.2 %copy-start.7 = (bf16[2048,4]{0,1:T(4,128)(2,1)S(1)}, bf16[2048,4]{0,1:T(4,128)(2,1)}, u32[]{:S(2)}) copy-start(bf16[2048,4]{0,1:T(4,128)(2,1)} %param.37) | copy-start | bytes 49156
  7.3 75.2 %copy-start.3 = (bf16[2048,128]{1,0:T(8,128)(2,1)S(1)}, bf16[2048,128]{1,0:T(8,128)(2,1)}, u32[]{:S(2)}) copy-start(bf16[2048,128]{1,0:T(8,128)(2,1)} %write_ref.1) | copy-start | bytes 1572868
  7.3 75.2 %copy-start.2 = (bf16[2048,256]{1,0:T(8,128)(2,1)S(1)}, bf16[2048,256]{1,0:T(8,128)(2,1)}, u32[]{:S(2)}) copy-start(bf16[2048,256]{1,0:T(8,128)(2,1)} %input_ref.1) | copy-start | bytes 3145732
  7.3 75.2 %copy-start.1 = (bf16[2048,256]{1,0:T(8,128)(2,1)S(1)}, bf16[2048,256]{1,0:T(8,128)(2,1)}, u32[]{:S(2)}) copy-start(bf16[2048,256]{1,0:T(8,128)(2,1)} %gate_ref.1) | copy-start | bytes 3145732
  7.3 75.2 %copy-start.8 = (bf16[2048]{0:T(1024)(128)(2,1)S(1)}, bf16[2048]{0:T(1024)(128)(2,1)}, u32[]{:S(2)}) copy-start(bf16[2048]{0:T(1024)(128)(2,1)} %gain_ref.1) | copy-start | bytes 12292
  7.3 39.2 %all-gather.5.cloned.1.call-start = ((), (), s32[]{:S(2)}) async-start(), calls=%async_computation.7 | async-start | bytes 2433024 | tf_op jit(solution)/shard_map/all_gather | solution.py:467
  9.6 100.5 %all-gather.7.cloned.1.call-start = ((), (), s32[]{:S(2)}) async-start(), calls=%async_computation.8 | async-start | bytes 8921088 | tf_op jit(solution)/shard_map/all_gather | solution.py:468
  46.5 36.1 %copy-start = (f32[32,4,64,128]{3,2,1,0:T(8,128)S(1)}, f32[32,4,64,128]{3,2,1,0:T(8,128)}, u32[]{:S(2)}) copy-start(f32[32,4,64,128]{3,2,1,0:T(8,128)} %state_ref.1) | copy-start | bytes 12582916
Sparse Core Ops, SparseCore 0:
  10.5 32.0 all-gather.4
  45.2 61.5 all-gather.6

commit v9 on v8

--- a/solution.py
+++ b/solution.py
@@ -14,9 +14,12 @@
 ROWS = 4
 Z, Y, TP = 8, 4, 8
 
-KV_AXES = ("z", "y")
+KV_AXES = ("z", "y_hi", "y_lo")
 TP_AXES = ("x", "core")
-BLOCK_AXES = ("y", "z")
+BLOCK_AXES = ("y_hi", "y_lo", "z")
+PAIR = 2
+ROW_AXES = ("z", "y_hi")
+ROW_BLOCKS = Z * Y // PAIR
 
 norm_eps = 1e-06
 
@@ -159,15 +162,15 @@
     for u in range(TP):
         cols = slice(u * FEATS, (u + 1) * FEATS)
         rows = (first_ref[u].astype(jnp.float32) + mixed[:, cols]).astype(jnp.bfloat16)
-        for z in range(Z):
-            copies_ref[z, :, cols] = rows
+        for n in range(ROW_BLOCKS):
+            copies_ref[n, :, cols] = rows
 
 
 def mixed_copies(first, tiles):
     vmem = pl.BlockSpec(memory_space=pltpu.VMEM)
     return pl.pallas_call(
         mix_kernel,
-        out_shape=pltpu.VMEM((Z, ROWS, D), jnp.bfloat16),
+        out_shape=pltpu.VMEM((ROW_BLOCKS, ROWS, D), jnp.bfloat16),
         in_specs=[vmem, vmem],
         out_specs=vmem,
         compiler_params=pltpu.CompilerParams(vmem_limit_bytes=8 << 20),
@@ -178,10 +181,10 @@
 def second_kernel(
     place_ref, rows_ref, weights_hbm, out_ref, normed_ref, weights_ref, arrived
 ):
-    rows = Z * ROWS
+    rows = ROW_BLOCKS * ROWS
     copies = [
         pltpu.make_async_copy(weights_hbm.at[n], weights_ref.at[n], arrived.at[n])
-        for n in range(Y * TP)
+        for n in range(PAIR * TP)
     ]
     for copy in copies:
         copy.start()
@@ -192,7 +195,7 @@
     for u in range(TP):
         normed_ref[u] = (values[:, u * FEATS : (u + 1) * FEATS] * factor).astype(jnp.bfloat16)
     hidden = []
-    for y in range(Y):
+    for y in range(PAIR):
         both = jnp.zeros((rows, 2 * HIDDEN), jnp.float32)
         for u in range(TP):
             copies[y * TP + u].wait()
@@ -207,20 +210,20 @@
         hidden.append((gate * jax.nn.sigmoid(gate) * lift).astype(jnp.bfloat16))
     for u in range(TP):
         down = values[:, u * FEATS : (u + 1) * FEATS] * own
-        for y in range(Y):
+        for y in range(PAIR):
             down += jnp.dot(
                 hidden[y],
                 weights_ref[y * TP + u, 2 * HIDDEN :],
                 preferred_element_type=jnp.float32,
             )
-        out_ref[:, u] = down.reshape(Z, ROWS, FEATS).astype(jnp.bfloat16)
+        out_ref[:, u] = down.reshape(ROW_BLOCKS, ROWS, FEATS).astype(jnp.bfloat16)
 
 
 def second_partial(place, rows, weights):
     vmem = pl.BlockSpec(memory_space=pltpu.VMEM)
     return pl.pallas_call(
         second_kernel,
-        out_shape=pltpu.VMEM((Z, TP, ROWS, FEATS), jnp.bfloat16),
+        out_shape=pltpu.VMEM((ROW_BLOCKS, TP, ROWS, FEATS), jnp.bfloat16),
         in_specs=[
             pl.BlockSpec(memory_space=pltpu.SMEM),
             vmem,
@@ -228,9 +231,9 @@
         ],
         out_specs=vmem,
         scratch_shapes=[
-            pltpu.VMEM((TP, Z * ROWS, FEATS), jnp.bfloat16),
+            pltpu.VMEM((TP, ROW_BLOCKS * ROWS, FEATS), jnp.bfloat16),
             pltpu.VMEM(weights.shape, jnp.bfloat16),
-            pltpu.SemaphoreType.DMA((Y * TP,)),
+            pltpu.SemaphoreType.DMA((PAIR * TP,)),
         ],
         compiler_params=pltpu.CompilerParams(vmem_limit_bytes=24 << 20),
         name="second_ffn",
@@ -457,7 +460,7 @@
     second_lift,
     second_down,
 ):
-    place = jnp.stack([lax.axis_index(BLOCK_AXES), lax.axis_index("z")]).astype(jnp.int32)
+    place = jnp.stack([lax.axis_index(BLOCK_AXES), lax.axis_index(ROW_AXES)]).astype(jnp.int32)
     share_one, share_two, pieces = weight_shares(
         place,
         residual,
@@ -465,9 +468,10 @@
         (second_gain, second_gate, second_lift, second_down),
     )
     weights_one = lax.all_gather(share_one, TP_AXES)
-    weights_two = lax.all_gather(share_two, ("y", *TP_AXES))
 
     mine = lax.all_to_all(pieces, TP_AXES, 0, 0, tiled=True)
+    share_two, mine = lax.optimization_barrier((share_two, mine))
+    weights_two = lax.all_gather(share_two, ("y_lo", *TP_AXES))
     tiles = sent_to_all(mine, BLOCK_AXES).reshape(Z * Y, TP, ROWS, FEATS)
     share, own = first_partial(place, tiles, weights_one)
     share = lax.all_to_all(share, BLOCK_AXES, 0, 0, tiled=True)
@@ -496,15 +500,15 @@
         proj_output,
     )
 
-    rows = lax.all_to_all(mixed, "z", 0, 0, tiled=True)
+    rows = lax.all_to_all(mixed, ROW_AXES, 0, 0, tiled=True)
     share = second_partial(place, rows, weights_two)
-    share = lax.all_to_all(share.reshape(-1, ROWS, FEATS), ("z", *TP_AXES), 0, 0, tiled=True)
-    residual_out = last_sum(share.reshape(Z, TP, ROWS, FEATS))
+    share = lax.all_to_all(share.reshape(-1, ROWS, FEATS), (*ROW_AXES, *TP_AXES), 0, 0, tiled=True)
+    residual_out = last_sum(share.reshape(ROW_BLOCKS, TP, ROWS, FEATS))
     return (residual_out, state_out)
 
 
 def solution(mesh):
-    mesh = Mesh(mesh.devices.reshape(Z, Y, TP // 2, 2), (*KV_AXES, *TP_AXES))
+    mesh = Mesh(mesh.devices.reshape(Z, Y // PAIR, PAIR, TP // 2, 2), (*KV_AXES, *TP_AXES))
     placed = (
         P(KV_AXES, TP_AXES),
         P(TP_AXES),

time: 142 us -> 150 us (1.056)
  blocking collectives: 107 us -> 118 us
  Pallas kernels: 18.5 us -> 16.3 us
    all_to_all x2, blocking collectives: 28.2 us -> 39.8 us  [the longest x1 23.4 us: per_device(): lax.all_to_all(share.reshape(-1, ROWS, FEATS), (*ROW_AXES, *TP_AXES), 0,...]
    pallas_call x2, Pallas kernels: 6.6 us -> 4.48 us  [the longest x1 4.4 us: second_partial(): pl.pallas_call(second_kernel, out_shape=pltpu.VMEM((ROW_BLOCKS, TP, ROWS,...]
where the time goes in v9:
time: 150 us
  blocking collectives  118 us (79%)
  Pallas kernels  16.3 us (11%)
  between operations  14.3 us (10%)
    all_to_all x1, blocking collectives, sent_to_all(): lax.all_to_all(jnp.broadcast_to(array[None], (length, *array.shape)), axi...  25.6 us
    all_to_all x1, blocking collectives, per_device(): lax.all_to_all(share.reshape(-1, ROWS, FEATS), (*ROW_AXES, *TP_AXES), 0,...  23.4 us
    all_to_all x1, blocking collectives, per_device(): share = lax.all_to_all(share, BLOCK_AXES, 0, 0, tiled=True)  20.8 us
    all_to_all x1, blocking collectives, per_device(): rows = lax.all_to_all(mixed, ROW_AXES, 0, 0, tiled=True)  16.3 us
    all_to_all x1, blocking collectives, per_device(): lax.all_to_all(copies, TP_AXES, 0, 0, tiled=True)  13.2 us
    all_to_all x1, blocking collectives, per_device(): mine = lax.all_to_all(pieces, TP_AXES, 0, 0, tiled=True)  10.2 us
    all_to_all x1, blocking collectives, state_mixer(): tiles = lax.all_to_all(partial_out, TP_AXES, 0, 0, tiled=True)  8.85 us
    pallas_call x1, Pallas kernels, state_mixer(): pl.pallas_call(mixer_kernel, grid=(blocks,), out_shape=[pltpu.VMEM((TP, R...  5.76 us
  transfers between devices with their start and end apart: 2, of which 0 were waited for; matrix products, arithmetic and copies ran while one was open for 0% of the time, Pallas kernels for 6%

profile of v9, /device:TPU:1, one launch (start us, length us, event | category | flops | bytes accessed | tf_op | source)
XLA Modules:
  0.0 149.6 jit_solution(12092800917154041197)
XLA Ops:
  7.2 0.0 copy-start.15
  7.2 0.0 copy-start.6
  7.2 0.0 copy-start.5
  7.2 0.0 copy-start.4
  7.2 0.0 copy-start.11
  7.2 0.0 copy-start.10
  7.2 0.0 copy-start.9
  7.2 0.0 copy-start.14
  7.3 0.0 copy-start.13
  7.3 0.0 copy-start.12
  7.3 0.0 copy-start.7
  7.3 0.0 copy-start.3
  7.3 0.0 copy-start.2
  7.3 0.0 copy-start.1
  7.3 0.0 copy-start.8
  7.3 0.0 all-gather.5.cloned.1.call-start
  7.4 0.1 pad_add_fusion.place_ref
  7.5 2.1 %shares.1 = (bf16[528,256]{1,0:T(8,128)(2,1)}, bf16[528,256]{1,0:T(8,128)(2,1)}, bf16[8,4,256]{2,1,0:T(4,128)(2,1)S(1)}) custom-call(s32[2]{0:T(128)S(1)} %pad_add_fusion.place_ref, bf16[32,256]{1,0:T(8,128)(2,1)} %rows_ref.1, bf16[256]{0:T(256)(128)(2,1)} %refs_0_.1, bf16[176,256]{1,0:T(8,128)(2,1)} %bitcast.22, bf16[176,256]{1,0:T(8,128)(2,1)} %bitcast.23, ...), custom_call_target="tpu_custom_call" | custom-call | tf_op jit(solution)/shard_map/shares/pallas_call | solution.py:66
  9.6 0.0 all-gather.5.cloned.1.call-update
  9.6 0.0 all-gather.7.cloned.1.call-start
  9.7 10.2 %all_to_all.35 = bf16[8,4,256]{2,1,0:T(4,128)(2,1)S(1)} all-to-all(bf16[8,4,256]{2,1,0:T(4,128)(2,1)S(1)} %get-tuple-element.14), channel_id=1, replica_groups=mesh['z'=8,'y_hi'=2,'y_lo'=2,'x'=4,'core'=2] {'x','core'}, dimensions={0} | all-to-all | bytes 32768 | tf_op jit(solution)/shard_map/all_to_all | solution.py:472
  19.9 0.0 all-gather.7.cloned.1.call-update
  19.9 0.2 broadcast_in_dim.2
  20.2 25.6 %all_to_all.36.rows_ref = bf16[32,8,4,256]{3,2,1,0:T(4,128)(2,1)S(1)} all-to-all(bf16[32,8,4,256]{3,2,1,0:T(4,128)(2,1)S(1)} %broadcast_in_dim.2), channel_id=1, replica_groups=mesh['z'=8,'y_hi'=2,'y_lo'=2,'x'=4,'core'=2] {'y_hi','y_lo','z'}, dimensions={0} | all-to-all | bytes 1048576 | tf_op jit(solution)/shard_map/all_to_all | solution.py:31
  45.8 0.0 all-gather.5.cloned.1.call-done
  45.8 0.0 copy-start
  45.8 3.0 %first_ffn.1 = (bf16[32,8,4,256]{3,2,1,0:T(4,128)(2,1)S(1)}, bf16[8,4,256]{2,1,0:T(4,128)(2,1)S(1)}) custom-call(s32[2]{0:T(128)S(1)} %pad_add_fusion.place_ref, bf16[32,8,4,256]{3,2,1,0:T(4,128)(2,1)S(1)} %all_to_all.36.rows_ref, bf16[8,528,256]{2,1,0:T(8,128)(2,1)} %bitcast.21), custom_call_target="tpu_custom_call" | custom-call | tf_op jit(solution)/shard_map/first_ffn/pallas_call | solution.py:115
  48.8 20.8 %all_to_all.37.share_ref = bf16[32,8,4,256]{3,2,1,0:T(4,128)(2,1)S(1)} all-to-all(bf16[32,8,4,256]{3,2,1,0:T(4,128)(2,1)S(1)} %get-tuple-element.18), channel_id=1, replica_groups=mesh['z'=8,'y_hi'=2,'y_lo'=2,'x'=4,'core'=2] {'y_hi','y_lo','z'}, dimensions={0} | all-to-all | bytes 1048576 | tf_op jit(solution)/shard_map/all_to_all | solution.py:477
  69.5 0.2 settle.1
  69.8 13.2 %all_to_all.38.rows_ref = bf16[8,8,4,256]{3,2,1,0:T(4,128)(2,1)S(1)} all-to-all(bf16[8,8,4,256]{3,2,1,0:T(4,128)(2,1)S(1)} %get-tuple-element.20), channel_id=1, replica_groups=mesh['z'=8,'y_hi'=2,'y_lo'=2,'x'=4,'core'=2] {'x','core'}, dimensions={0} | all-to-all | bytes 262144 | tf_op jit(solution)/shard_map/all_to_all | solution.py:482
  83.0 0.0 copy-done.15
  83.0 0.0 copy-done.6
  83.0 0.0 copy-done.5
  83.0 0.0 copy-done.4
  83.0 0.0 copy-done.11
  83.0 0.0 copy-done.10
  83.0 0.0 copy-done.9
  83.0 0.0 copy-done.14
  83.1 0.0 copy-done.13
  83.1 0.0 copy-done.12
  83.1 0.0 copy-done.7
  83.1 0.0 copy-done.3
  83.1 0.0 copy-done.2
  83.1 0.0 copy-done.1
  83.1 0.0 copy-done.8
  83.1 0.0 copy-done
  83.1 5.8 %mixer.1 = (bf16[8,4,2048]{2,1,0:T(4,128)(2,1)S(1)}, f32[32,4,64,128]{3,2,1,0:T(8,128)}) custom-call(bf16[8,8,4,256]{3,2,1,0:T(4,128)(2,1)S(1)} %all_to_all.38.rows_ref, bf16[2048]{0:T(1024)(128)(2,1)S(1)} %copy-done.8, bf16[2048,256]{1,0:T(8,128)(2,1)S(1)} %copy-done.1, bf16[2048,256]{1,0:T(8,128)(2,1)S(1)} %copy-done.2, bf16[2048,128]{1,0:T(8,128)(2,1)S(1)} %copy-done.3, ...), custom_call_target="tpu_custom_call" | custom-call | tf_op jit(solution)/shard_map/mixer/pallas_call | solution.py:405
  88.9 8.9 %all_to_all.39.tiles_ref = bf16[8,4,2048]{2,1,0:T(4,128)(2,1)S(1)} all-to-all(bf16[8,4,2048]{2,1,0:T(4,128)(2,1)S(1)} %get-tuple-element.21), channel_id=1, replica_groups=mesh['z'=8,'y_hi'=2,'y_lo'=2,'x'=4,'core'=2] {'x','core'}, dimensions={0} | all-to-all | bytes 262144 | tf_op jit(solution)/shard_map/all_to_all | solution.py:430
  97.8 0.1 mix.1
  97.8 16.3 %all_to_all.40.rows_ref = bf16[16,4,2048]{2,1,0:T(4,128)(2,1)S(1)} all-to-all(bf16[16,4,2048]{2,1,0:T(4,128)(2,1)S(1)} %mix.1), channel_id=1, replica_groups=mesh['z'=8,'y_hi'=2,'y_lo'=2,'x'=4,'core'=2] {'z','y_hi'}, dimensions={0} | all-to-all | bytes 524288 | tf_op jit(solution)/shard_map/all_to_all | solution.py:503
  114.2 0.0 all-gather.7.cloned.1.call-done
  114.2 4.4 %second_ffn.1 = bf16[16,8,4,256]{3,2,1,0:T(4,128)(2,1)S(1)} custom-call(s32[2]{0:T(128)S(1)} %pad_add_fusion.place_ref, bf16[16,4,2048]{2,1,0:T(4,128)(2,1)S(1)} %all_to_all.40.rows_ref, bf16[16,528,256]{2,1,0:T(8,128)(2,1)} %bitcast.20), custom_call_target="tpu_custom_call" | custom-call | tf_op jit(solution)/shard_map/second_ffn/pallas_call | solution.py:224
  118.6 23.4 %all_to_all.41 = bf16[128,4,256]{2,1,0:T(4,128)(2,1)S(1)} all-to-all(bf16[128,4,256]{2,1,0:T(4,128)(2,1)S(1)} %bitcast.14), channel_id=1, replica_groups=mesh['z'=8,'y_hi'=2,'y_lo'=2,'x'=4,'core'=2] {'z','y_hi','x','core'}, dimensions={0} | all-to-all | bytes 524288 | tf_op jit(solution)/shard_map/all_to_all | solution.py:505
  142.0 0.7 last.1
Async XLA Ops:
  7.2 75.8 %copy-start.15 = (bf16[256]{0:T(256)(128)(2,1)S(1)}, bf16[256]{0:T(256)(128)(2,1)}, u32[]{:S(2)}) copy-start(bf16[256]{0:T(256)(128)(2,1)} %group_ref.1) | copy-start | bytes 1540
  7.2 75.8 %copy-start.6 = (bf16[32,3,128]{2,0,1:T(8,128)(2,1)S(1)}, bf16[32,3,128]{2,0,1:T(8,128)(2,1)}, u32[]{:S(2)}) copy-start(bf16[32,3,128]{2,0,1:T(8,128)(2,1)} %param.46) | copy-start | bytes 73732
  7.2 75.8 %copy-start.5 = (bf16[32,3,128]{2,0,1:T(8,128)(2,1)S(1)}, bf16[32,3,128]{2,0,1:T(8,128)(2,1)}, u32[]{:S(2)}) copy-start(bf16[32,3,128]{2,0,1:T(8,128)(2,1)} %param.45) | copy-start | bytes 73732
  7.2 75.8 %copy-start.4 = (bf16[32,3,256]{2,0,1:T(8,128)(2,1)S(1)}, bf16[32,3,256]{2,0,1:T(8,128)(2,1)}, u32[]{:S(2)}) copy-start(bf16[32,3,256]{2,0,1:T(8,128)(2,1)} %param.44) | copy-start | bytes 147460
  7.2 75.8 %copy-start.11 = (bf16[4,128]{1,0:T(4,128)(2,1)S(1)}, bf16[4,128]{1,0:T(4,128)(2,1)}, u32[]{:S(2)}) copy-start(bf16[4,128]{1,0:T(4,128)(2,1)} %taps_read_ref.1) | copy-start | bytes 3076
  7.2 75.8 %copy-start.10 = (bf16[4,128]{1,0:T(4,128)(2,1)S(1)}, bf16[4,128]{1,0:T(4,128)(2,1)}, u32[]{:S(2)}) copy-start(bf16[4,128]{1,0:T(4,128)(2,1)} %taps_write_ref.1) | copy-start | bytes 3076
  7.2 75.8 %copy-start.9 = (bf16[4,256]{1,0:T(4,128)(2,1)S(1)}, bf16[4,256]{1,0:T(4,128)(2,1)}, u32[]{:S(2)}) copy-start(bf16[4,256]{1,0:T(4,128)(2,1)} %taps_input_ref.1) | copy-start | bytes 6148
  7.2 75.8 %copy-start.14 = (f32[4]{0:T(128)S(1)}, f32[4]{0:T(128)}, u32[]{:S(2)}) copy-start(f32[4]{0:T(128)} %skip_ref.1) | copy-start | bytes 52
  7.3 75.8 %copy-start.13 = (f32[4]{0:T(128)S(1)}, f32[4]{0:T(128)}, u32[]{:S(2)}) copy-start(f32[4]{0:T(128)} %rate_ref.1) | copy-start | bytes 52
  7.3 75.8 %copy-start.12 = (f32[4]{0:T(128)S(1)}, f32[4]{0:T(128)}, u32[]{:S(2)}) copy-start(f32[4]{0:T(128)} %bias_ref.1) | copy-start | bytes 52
  7.3 75.8 %copy-start.7 = (bf16[2048,4]{0,1:T(4,128)(2,1)S(1)}, bf16[2048,4]{0,1:T(4,128)(2,1)}, u32[]{:S(2)}) copy-start(bf16[2048,4]{0,1:T(4,128)(2,1)} %param.37) | copy-start | bytes 49156
  7.3 75.8 %copy-start.3 = (bf16[2048,128]{1,0:T(8,128)(2,1)S(1)}, bf16[2048,128]{1,0:T(8,128)(2,1)}, u32[]{:S(2)}) copy-start(bf16[2048,128]{1,0:T(8,128)(2,1)} %write_ref.1) | copy-start | bytes 1572868
  7.3 75.8 %copy-start.2 = (bf16[2048,256]{1,0:T(8,128)(2,1)S(1)}, bf16[2048,256]{1,0:T(8,128)(2,1)}, u32[]{:S(2)}) copy-start(bf16[2048,256]{1,0:T(8,128)(2,1)} %input_ref.1) | copy-start | bytes 3145732
  7.3 75.8 %copy-start.1 = (bf16[2048,256]{1,0:T(8,128)(2,1)S(1)}, bf16[2048,256]{1,0:T(8,128)(2,1)}, u32[]{:S(2)}) copy-start(bf16[2048,256]{1,0:T(8,128)(2,1)} %gate_ref.1) | copy-start | bytes 3145732
  7.3 75.8 %copy-start.8 = (bf16[2048]{0:T(1024)(128)(2,1)S(1)}, bf16[2048]{0:T(1024)(128)(2,1)}, u32[]{:S(2)}) copy-start(bf16[2048]{0:T(1024)(128)(2,1)} %gain_ref.1) | copy-start | bytes 12292
  7.3 38.5 %all-gather.5.cloned.1.call-start = ((), (), s32[]{:S(2)}) async-start(), calls=%async_computation.7 | async-start | bytes 2433024 | tf_op jit(solution)/shard_map/all_gather | solution.py:470
  9.6 104.6 %all-gather.7.cloned.1.call-start = ((), (), s32[]{:S(2)}) async-start(), calls=%async_computation.8 | async-start | bytes 4595712 | tf_op jit(solution)/shard_map/all_gather | solution.py:474
  45.8 37.3 %copy-start = (f32[32,4,64,128]{3,2,1,0:T(8,128)S(1)}, f32[32,4,64,128]{3,2,1,0:T(8,128)}, u32[]{:S(2)}) copy-start(f32[32,4,64,128]{3,2,1,0:T(8,128)} %state_ref.1) | copy-start | bytes 12582916
Sparse Core Ops, SparseCore 0:
  10.5 32.0 all-gather.4
  44.5 45.3 all-gather.6

commit v10 on v8

--- a/solution.py
+++ b/solution.py
@@ -43,10 +43,10 @@
 
 
 def share_kernel(place_ref, rows_ref, *refs):
-    pieces_ref = refs[-1]
-    pieces_ref[...] = rows_ref[...].astype(jnp.float32).reshape(TP, ROWS, FEATS).astype(
-        jnp.bfloat16
-    )
+    copies_ref = refs[-1]
+    pieces = rows_ref[...].astype(jnp.float32).reshape(TP, ROWS, FEATS).astype(jnp.bfloat16)
+    for n in range(Z * Y):
+        copies_ref[n] = pieces
     for gain, gate, lift, down, out in (refs[0:4] + refs[8:9], refs[4:8] + refs[9:10]):
         gain_f = gain[...].astype(jnp.float32).reshape(1, FEATS)
         out[:HIDDEN] = (gate[...].astype(jnp.float32) * gain_f).astype(jnp.bfloat16)
@@ -62,7 +62,7 @@
     share = jax.ShapeDtypeStruct((3 * HIDDEN, FEATS), jnp.bfloat16)
     return pl.pallas_call(
         share_kernel,
-        out_shape=[share, share, pltpu.VMEM((TP, ROWS, FEATS), jnp.bfloat16)],
+        out_shape=[share, share, pltpu.VMEM((Z * Y, TP, ROWS, FEATS), jnp.bfloat16)],
         compiler_params=pltpu.CompilerParams(vmem_limit_bytes=4 << 20),
         in_specs=[pl.BlockSpec(memory_space=pltpu.SMEM)] + [vmem for _ in operands],
         out_specs=[vmem] * 3,
@@ -180,8 +180,10 @@
 ):
     rows = Z * ROWS
     copies = [
-        pltpu.make_async_copy(weights_hbm.at[n], weights_ref.at[n], arrived.at[n])
-        for n in range(Y * TP)
+        pltpu.make_async_copy(
+            weights_hbm.at[pl.ds(n * 4, 4)], weights_ref.at[pl.ds(n * 4, 4)], arrived.at[n]
+        )
+        for n in range(Y * TP // 4)
     ]
     for copy in copies:
         copy.start()
@@ -194,8 +196,8 @@
     hidden = []
     for y in range(Y):
         both = jnp.zeros((rows, 2 * HIDDEN), jnp.float32)
-        for u in range(TP):
-            copies[y * TP + u].wait()
+        for n in range(TP // 4):
+            copies[y * TP // 4 + n].wait()
         for u in range(TP):
             both += lax.dot_general(
                 normed_ref[u],
@@ -230,7 +232,7 @@
         scratch_shapes=[
             pltpu.VMEM((TP, Z * ROWS, FEATS), jnp.bfloat16),
             pltpu.VMEM(weights.shape, jnp.bfloat16),
-            pltpu.SemaphoreType.DMA((Y * TP,)),
+            pltpu.SemaphoreType.DMA((Y * TP // 4,)),
         ],
         compiler_params=pltpu.CompilerParams(vmem_limit_bytes=24 << 20),
         name="second_ffn",
@@ -467,8 +469,9 @@
     weights_one = lax.all_gather(share_one, TP_AXES)
     weights_two = lax.all_gather(share_two, ("y", *TP_AXES))
 
-    mine = lax.all_to_all(pieces, TP_AXES, 0, 0, tiled=True)
-    tiles = sent_to_all(mine, BLOCK_AXES).reshape(Z * Y, TP, ROWS, FEATS)
+    tiles = lax.all_to_all(
+        pieces.reshape(-1, ROWS, FEATS), (*BLOCK_AXES, *TP_AXES), 0, 0, tiled=True
+    ).reshape(Z * Y, TP, ROWS, FEATS)
     share, own = first_partial(place, tiles, weights_one)
     share = lax.all_to_all(share, BLOCK_AXES, 0, 0, tiled=True)
     first, copies = settled(own, share)

time: 142 us -> 145 us (1.021)
  blocking collectives: 107 us -> 110 us
    all_to_all x1, blocking collectives: 20.8 us -> 22.3 us  [per_device(): share = lax.all_to_all(share, BLOCK_AXES, 0, 0, tiled=True)]
    all_to_all x2 -> x1, blocking collectives: 35.9 us -> 35.9 us  [per_device(): lax.all_to_all(pieces.reshape(-1, ROWS, FEATS), (*BLOCK_AXES, *TP_AXES),...]
where the time goes in v10:
time: 145 us; the launch traced here: 144 us
  blocking collectives  110 us (76%)
  Pallas kernels  18.3 us (13%)
  between operations  14.3 us (10%)
    all_to_all x1, blocking collectives, per_device(): lax.all_to_all(pieces.reshape(-1, ROWS, FEATS), (*BLOCK_AXES, *TP_AXES),...  35.9 us
    all_to_all x1, blocking collectives, per_device(): share = lax.all_to_all(share, BLOCK_AXES, 0, 0, tiled=True)  22.3 us
    all_to_all x1, blocking collectives, per_device(): lax.all_to_all(share.reshape(-1, ROWS, FEATS), ('z', *TP_AXES), 0, 0, til...  17 us
    all_to_all x1, blocking collectives, per_device(): lax.all_to_all(copies, TP_AXES, 0, 0, tiled=True)  12.5 us
    all_to_all x1, blocking collectives, per_device(): rows = lax.all_to_all(mixed, 'z', 0, 0, tiled=True)  11.8 us
    all_to_all x1, blocking collectives, state_mixer(): tiles = lax.all_to_all(partial_out, TP_AXES, 0, 0, tiled=True)  10.3 us
    pallas_call x1, Pallas kernels, second_partial(): pl.pallas_call(second_kernel, out_shape=pltpu.VMEM((Z, TP, ROWS, FEATS),...  6.35 us
    pallas_call x1, Pallas kernels, state_mixer(): pl.pallas_call(mixer_kernel, grid=(blocks,), out_shape=[pltpu.VMEM((TP, R...  5.86 us
  transfers between devices with their start and end apart: 2, of which 0 were waited for; matrix products, arithmetic and copies ran while one was open for 0% of the time, Pallas kernels for 6%

profile of v10, /device:TPU:1, one launch (start us, length us, event | category | flops | bytes accessed | tf_op | source)
XLA Modules:
  0.0 144.5 jit_solution(14262327930030948716)
XLA Ops:
  7.2 0.0 copy-start.15
  7.2 0.0 copy-start.6
  7.2 0.0 copy-start.5
  7.2 0.0 copy-start.4
  7.2 0.0 copy-start.11
  7.2 0.0 copy-start.10
  7.2 0.0 copy-start.9
  7.2 0.0 copy-start.14
  7.2 0.0 copy-start.13
  7.3 0.0 copy-start.12
  7.3 0.0 copy-start.7
  7.3 0.0 copy-start.2
  7.3 0.0 copy-start.1
  7.3 0.0 copy-start.8
  7.3 0.0 all-gather.5.cloned.1.call-start
  7.4 0.1 pad_add_fusion.place_ref
  7.4 2.1 %shares.1 = (bf16[528,256]{1,0:T(8,128)(2,1)}, bf16[528,256]{1,0:T(8,128)(2,1)}, bf16[32,8,4,256]{3,2,1,0:T(4,128)(2,1)S(1)}) custom-call(s32[2]{0:T(128)S(1)} %pad_add_fusion.place_ref, bf16[32,256]{1,0:T(8,128)(2,1)} %rows_ref.1, bf16[256]{0:T(256)(128)(2,1)} %refs_0_.1, bf16[176,256]{1,0:T(8,128)(2,1)} %bitcast.26, bf16[176,256]{1,0:T(8,128)(2,1)} %bitcast.27, ...), custom_call_target="tpu_custom_call" | custom-call | tf_op jit(solution)/shard_map/shares/pallas_call | solution.py:63
  9.6 0.0 all-gather.5.cloned.1.call-update
  9.6 0.0 all-gather.7.cloned.1.call-start
  9.7 0.7 all-gather.7.cloned.1.call-update
  10.4 35.9 %all_to_all.30 = bf16[256,4,256]{2,1,0:T(4,128)(2,1)S(1)} all-to-all(bf16[256,4,256]{2,1,0:T(4,128)(2,1)S(1)} %bitcast.18), channel_id=1, replica_groups=mesh['z'=8,'y'=4,'x'=4,'core'=2] {'y','z','x','core'}, dimensions={0} | all-to-all | bytes 1048576 | tf_op jit(solution)/shard_map/all_to_all | solution.py:472
  46.3 0.0 all-gather.5.cloned.1.call-done
  46.3 0.0 copy-start
  46.3 3.0 %first_ffn.1 = (bf16[32,8,4,256]{3,2,1,0:T(4,128)(2,1)S(1)}, bf16[8,4,256]{2,1,0:T(4,128)(2,1)S(1)}) custom-call(s32[2]{0:T(128)S(1)} %pad_add_fusion.place_ref, bf16[32,8,4,256]{3,2,1,0:T(4,128)(2,1)S(1)} %bitcast.16, bf16[8,528,256]{2,1,0:T(8,128)(2,1)} %bitcast.25), custom_call_target="tpu_custom_call" | custom-call | tf_op jit(solution)/shard_map/first_ffn/pallas_call | solution.py:112
  49.3 22.3 %all_to_all.31.share_ref = bf16[32,8,4,256]{3,2,1,0:T(4,128)(2,1)S(1)} all-to-all(bf16[32,8,4,256]{3,2,1,0:T(4,128)(2,1)S(1)} %get-tuple-element.14), channel_id=1, replica_groups=mesh['z'=8,'y'=4,'x'=4,'core'=2] {'y','z'}, dimensions={0} | all-to-all | bytes 1048576 | tf_op jit(solution)/shard_map/all_to_all | solution.py:476
  71.6 0.2 settle.1
  71.8 12.5 %all_to_all.32.rows_ref = bf16[8,8,4,256]{3,2,1,0:T(4,128)(2,1)S(1)} all-to-all(bf16[8,8,4,256]{3,2,1,0:T(4,128)(2,1)S(1)} %get-tuple-element.16), channel_id=1, replica_groups=mesh['z'=8,'y'=4,'x'=4,'core'=2] {'x','core'}, dimensions={0} | all-to-all | bytes 262144 | tf_op jit(solution)/shard_map/all_to_all | solution.py:481
  84.3 0.0 copy-done.15
  84.3 0.0 copy-done.6
  84.3 0.0 copy-done.5
  84.3 0.0 copy-done.4
  84.3 0.0 copy-done.11
  84.4 0.0 copy-done.10
  84.4 0.0 copy-done.9
  84.4 0.0 copy-done.14
  84.4 0.0 copy-done.13
  84.4 0.0 copy-done.12
  84.4 0.0 copy-done.7
  84.4 0.0 copy-done.2
  84.4 0.0 copy-done.1
  84.4 0.0 copy-done.8
  84.4 0.0 copy-done
  84.5 0.0 copy-start.3
  84.5 1.0 copy-done.3
  85.5 5.9 %mixer.1 = (bf16[8,4,2048]{2,1,0:T(4,128)(2,1)S(1)}, f32[32,4,64,128]{3,2,1,0:T(8,128)}) custom-call(bf16[8,8,4,256]{3,2,1,0:T(4,128)(2,1)S(1)} %all_to_all.32.rows_ref, bf16[2048]{0:T(1024)(128)(2,1)S(1)} %copy-done.8, bf16[2048,256]{1,0:T(8,128)(2,1)S(1)} %copy-done.1, bf16[2048,256]{1,0:T(8,128)(2,1)S(1)} %copy-done.2, bf16[2048,128]{1,0:T(8,128)(2,1)S(1)} %copy-done.3, ...), custom_call_target="tpu_custom_call" | custom-call | tf_op jit(solution)/shard_map/mixer/pallas_call | solution.py:404
  91.4 10.3 %all_to_all.33.tiles_ref = bf16[8,4,2048]{2,1,0:T(4,128)(2,1)S(1)} all-to-all(bf16[8,4,2048]{2,1,0:T(4,128)(2,1)S(1)} %get-tuple-element.17), channel_id=1, replica_groups=mesh['z'=8,'y'=4,'x'=4,'core'=2] {'x','core'}, dimensions={0} | all-to-all | bytes 262144 | tf_op jit(solution)/shard_map/all_to_all | solution.py:429
  101.7 0.1 mix.1
  101.8 11.8 %all_to_all.34.rows_ref = bf16[8,4,2048]{2,1,0:T(4,128)(2,1)S(1)} all-to-all(bf16[8,4,2048]{2,1,0:T(4,128)(2,1)S(1)} %mix.1), channel_id=1, replica_groups=mesh['z'=8,'y'=4,'x'=4,'core'=2] {'z'}, dimensions={0} | all-to-all | bytes 262144 | tf_op jit(solution)/shard_map/all_to_all | solution.py:502
  113.6 0.0 all-gather.7.cloned.1.call-done
  113.6 6.4 %second_ffn.1 = bf16[8,8,4,256]{3,2,1,0:T(4,128)(2,1)S(1)} custom-call(s32[2]{0:T(128)S(1)} %pad_add_fusion.place_ref, bf16[8,4,2048]{2,1,0:T(4,128)(2,1)S(1)} %all_to_all.34.rows_ref, bf16[32,528,256]{2,1,0:T(8,128)(2,1)} %bitcast.24), custom_call_target="tpu_custom_call" | custom-call | tf_op jit(solution)/shard_map/second_ffn/pallas_call | solution.py:223
  120.0 17.0 %all_to_all.35 = bf16[64,4,256]{2,1,0:T(4,128)(2,1)S(1)} all-to-all(bf16[64,4,256]{2,1,0:T(4,128)(2,1)S(1)} %bitcast.17), channel_id=1, replica_groups=mesh['z'=8,'y'=4,'x'=4,'core'=2] {'z','x','core'}, dimensions={0} | all-to-all | bytes 262144 | tf_op jit(solution)/shard_map/all_to_all | solution.py:504
  137.0 0.7 last.1
Async XLA Ops:
  7.2 77.2 %copy-start.15 = (bf16[256]{0:T(256)(128)(2,1)S(1)}, bf16[256]{0:T(256)(128)(2,1)}, u32[]{:S(2)}) copy-start(bf16[256]{0:T(256)(128)(2,1)} %group_ref.1) | copy-start | bytes 1540
  7.2 77.2 %copy-start.6 = (bf16[32,3,128]{2,0,1:T(8,128)(2,1)S(1)}, bf16[32,3,128]{2,0,1:T(8,128)(2,1)}, u32[]{:S(2)}) copy-start(bf16[32,3,128]{2,0,1:T(8,128)(2,1)} %param.46) | copy-start | bytes 73732
  7.2 77.1 %copy-start.5 = (bf16[32,3,128]{2,0,1:T(8,128)(2,1)S(1)}, bf16[32,3,128]{2,0,1:T(8,128)(2,1)}, u32[]{:S(2)}) copy-start(bf16[32,3,128]{2,0,1:T(8,128)(2,1)} %param.45) | copy-start | bytes 73732
  7.2 77.1 %copy-start.4 = (bf16[32,3,256]{2,0,1:T(8,128)(2,1)S(1)}, bf16[32,3,256]{2,0,1:T(8,128)(2,1)}, u32[]{:S(2)}) copy-start(bf16[32,3,256]{2,0,1:T(8,128)(2,1)} %param.44) | copy-start | bytes 147460
  7.2 77.1 %copy-start.11 = (bf16[4,128]{1,0:T(4,128)(2,1)S(1)}, bf16[4,128]{1,0:T(4,128)(2,1)}, u32[]{:S(2)}) copy-start(bf16[4,128]{1,0:T(4,128)(2,1)} %taps_read_ref.1) | copy-start | bytes 3076
  7.2 77.1 %copy-start.10 = (bf16[4,128]{1,0:T(4,128)(2,1)S(1)}, bf16[4,128]{1,0:T(4,128)(2,1)}, u32[]{:S(2)}) copy-start(bf16[4,128]{1,0:T(4,128)(2,1)} %taps_write_ref.1) | copy-start | bytes 3076
  7.2 77.1 %copy-start.9 = (bf16[4,256]{1,0:T(4,128)(2,1)S(1)}, bf16[4,256]{1,0:T(4,128)(2,1)}, u32[]{:S(2)}) copy-start(bf16[4,256]{1,0:T(4,128)(2,1)} %taps_input_ref.1) | copy-start | bytes 6148
  7.2 77.1 %copy-start.14 = (f32[4]{0:T(128)S(1)}, f32[4]{0:T(128)}, u32[]{:S(2)}) copy-start(f32[4]{0:T(128)} %skip_ref.1) | copy-start | bytes 52
  7.2 77.1 %copy-start.13 = (f32[4]{0:T(128)S(1)}, f32[4]{0:T(128)}, u32[]{:S(2)}) copy-start(f32[4]{0:T(128)} %rate_ref.1) | copy-start | bytes 52
  7.3 77.1 %copy-start.12 = (f32[4]{0:T(128)S(1)}, f32[4]{0:T(128)}, u32[]{:S(2)}) copy-start(f32[4]{0:T(128)} %bias_ref.1) | copy-start | bytes 52
  7.3 77.1 %copy-start.7 = (bf16[2048,4]{0,1:T(4,128)(2,1)S(1)}, bf16[2048,4]{0,1:T(4,128)(2,1)}, u32[]{:S(2)}) copy-start(bf16[2048,4]{0,1:T(4,128)(2,1)} %param.37) | copy-start | bytes 49156
  7.3 77.1 %copy-start.2 = (bf16[2048,256]{1,0:T(8,128)(2,1)S(1)}, bf16[2048,256]{1,0:T(8,128)(2,1)}, u32[]{:S(2)}) copy-start(bf16[2048,256]{1,0:T(8,128)(2,1)} %input_ref.1) | copy-start | bytes 3145732
  7.3 77.1 %copy-start.1 = (bf16[2048,256]{1,0:T(8,128)(2,1)S(1)}, bf16[2048,256]{1,0:T(8,128)(2,1)}, u32[]{:S(2)}) copy-start(bf16[2048,256]{1,0:T(8,128)(2,1)} %gate_ref.1) | copy-start | bytes 3145732
  7.3 77.1 %copy-start.8 = (bf16[2048]{0:T(1024)(128)(2,1)S(1)}, bf16[2048]{0:T(1024)(128)(2,1)}, u32[]{:S(2)}) copy-start(bf16[2048]{0:T(1024)(128)(2,1)} %gain_ref.1) | copy-start | bytes 12292
  7.3 39.0 %all-gather.5.cloned.1.call-start = ((), (), s32[]{:S(2)}) async-start(), calls=%async_computation.6 | async-start | bytes 2433024 | tf_op jit(solution)/shard_map/all_gather | solution.py:469
  9.6 104.0 %all-gather.7.cloned.1.call-start = ((), (), s32[]{:S(2)}) async-start(), calls=%async_computation.7 | async-start | bytes 8921088 | tf_op jit(solution)/shard_map/all_gather | solution.py:470
  46.3 38.1 %copy-start = (f32[32,4,64,128]{3,2,1,0:T(8,128)S(1)}, f32[32,4,64,128]{3,2,1,0:T(8,128)}, u32[]{:S(2)}) copy-start(f32[32,4,64,128]{3,2,1,0:T(8,128)} %state_ref.1) | copy-start | bytes 12582916
  84.5 1.0 copy-start.3
Sparse Core Ops, SparseCore 0:
  10.5 35.2 all-gather.4
  48.3 61.5 all-gather.6

commit v11 on v8

--- a/solution.py
+++ b/solution.py
@@ -180,8 +180,10 @@
 ):
     rows = Z * ROWS
     copies = [
-        pltpu.make_async_copy(weights_hbm.at[n], weights_ref.at[n], arrived.at[n])
-        for n in range(Y * TP)
+        pltpu.make_async_copy(
+            weights_hbm.at[pl.ds(n * 4, 4)], weights_ref.at[pl.ds(n * 4, 4)], arrived.at[n]
+        )
+        for n in range(Y * TP // 4)
     ]
     for copy in copies:
         copy.start()
@@ -194,8 +196,8 @@
     hidden = []
     for y in range(Y):
         both = jnp.zeros((rows, 2 * HIDDEN), jnp.float32)
-        for u in range(TP):
-            copies[y * TP + u].wait()
+        for n in range(TP // 4):
+            copies[y * TP // 4 + n].wait()
         for u in range(TP):
             both += lax.dot_general(
                 normed_ref[u],
@@ -230,7 +232,7 @@
         scratch_shapes=[
             pltpu.VMEM((TP, Z * ROWS, FEATS), jnp.bfloat16),
             pltpu.VMEM(weights.shape, jnp.bfloat16),
-            pltpu.SemaphoreType.DMA((Y * TP,)),
+            pltpu.SemaphoreType.DMA((Y * TP // 4,)),
         ],
         compiler_params=pltpu.CompilerParams(vmem_limit_bytes=24 << 20),
         name="second_ffn",
@@ -465,9 +467,10 @@
         (second_gain, second_gate, second_lift, second_down),
     )
     weights_one = lax.all_gather(share_one, TP_AXES)
+
+    mine = lax.all_to_all(pieces, TP_AXES, 0, 0, tiled=True)
+    share_two, mine = lax.optimization_barrier((share_two, mine))
     weights_two = lax.all_gather(share_two, ("y", *TP_AXES))
-
-    mine = lax.all_to_all(pieces, TP_AXES, 0, 0, tiled=True)
     tiles = sent_to_all(mine, BLOCK_AXES).reshape(Z * Y, TP, ROWS, FEATS)
     share, own = first_partial(place, tiles, weights_one)
     share = lax.all_to_all(share, BLOCK_AXES, 0, 0, tiled=True)

time: 142 us -> 141 us (level)
  no operation moved by 1% of the time
where the time goes in v11:
time: 141 us
  blocking collectives  108 us (77%)
  Pallas kernels  18.2 us (13%)
  between operations  14.3 us (10%)
    all_to_all x1, blocking collectives, sent_to_all(): lax.all_to_all(jnp.broadcast_to(array[None], (length, *array.shape)), axi...  25.6 us
    all_to_all x1, blocking collectives, per_device(): share = lax.all_to_all(share, BLOCK_AXES, 0, 0, tiled=True)  20.8 us
    all_to_all x1, blocking collectives, per_device(): lax.all_to_all(share.reshape(-1, ROWS, FEATS), ('z', *TP_AXES), 0, 0, til...  17.2 us
    all_to_all x1, blocking collectives, per_device(): lax.all_to_all(copies, TP_AXES, 0, 0, tiled=True)  12 us
    all_to_all x1, blocking collectives, per_device(): rows = lax.all_to_all(mixed, 'z', 0, 0, tiled=True)  11.4 us
    all_to_all x1, blocking collectives, state_mixer(): tiles = lax.all_to_all(partial_out, TP_AXES, 0, 0, tiled=True)  10.3 us
    all_to_all x1, blocking collectives, per_device(): mine = lax.all_to_all(pieces, TP_AXES, 0, 0, tiled=True)  10.2 us
    pallas_call x1, Pallas kernels, second_partial(): pl.pallas_call(second_kernel, out_shape=pltpu.VMEM((Z, TP, ROWS, FEATS),...  6.35 us
  transfers between devices with their start and end apart: 2, of which 0 were waited for; matrix products, arithmetic and copies ran while one was open for 0% of the time, Pallas kernels for 6%

profile of v11, /device:TPU:1, one launch (start us, length us, event | category | flops | bytes accessed | tf_op | source)
XLA Modules:
  0.0 140.5 jit_solution(17695716401612438821)
XLA Ops:
  7.2 0.0 copy-start.15
  7.2 0.0 copy-start.6
  7.2 0.0 copy-start.5
  7.2 0.0 copy-start.4
  7.2 0.0 copy-start.11
  7.2 0.0 copy-start.10
  7.2 0.0 copy-start.9
  7.2 0.0 copy-start.14
  7.3 0.0 copy-start.13
  7.3 0.0 copy-start.12
  7.3 0.0 copy-start.7
  7.3 0.0 copy-start.3
  7.3 0.0 copy-start.2
  7.3 0.0 copy-start.1
  7.3 0.0 copy-start.8
  7.3 0.0 all-gather.5.cloned.1.call-start
  7.4 0.1 pad_add_fusion.place_ref
  7.4 2.1 %shares.1 = (bf16[528,256]{1,0:T(8,128)(2,1)}, bf16[528,256]{1,0:T(8,128)(2,1)}, bf16[8,4,256]{2,1,0:T(4,128)(2,1)S(1)}) custom-call(s32[2]{0:T(128)S(1)} %pad_add_fusion.place_ref, bf16[32,256]{1,0:T(8,128)(2,1)} %rows_ref.1, bf16[256]{0:T(256)(128)(2,1)} %refs_0_.1, bf16[176,256]{1,0:T(8,128)(2,1)} %bitcast.22, bf16[176,256]{1,0:T(8,128)(2,1)} %bitcast.23, ...), custom_call_target="tpu_custom_call" | custom-call | tf_op jit(solution)/shard_map/shares/pallas_call | solution.py:63
  9.6 0.0 all-gather.5.cloned.1.call-update
  9.6 0.0 all-gather.7.cloned.1.call-start
  9.7 10.2 %all_to_all.35 = bf16[8,4,256]{2,1,0:T(4,128)(2,1)S(1)} all-to-all(bf16[8,4,256]{2,1,0:T(4,128)(2,1)S(1)} %get-tuple-element.14), channel_id=1, replica_groups=mesh['z'=8,'y'=4,'x'=4,'core'=2] {'x','core'}, dimensions={0} | all-to-all | bytes 32768 | tf_op jit(solution)/shard_map/all_to_all | solution.py:471
  19.9 0.0 all-gather.7.cloned.1.call-update
  19.9 0.2 broadcast_in_dim.2
  20.2 25.6 %all_to_all.36.rows_ref = bf16[32,8,4,256]{3,2,1,0:T(4,128)(2,1)S(1)} all-to-all(bf16[32,8,4,256]{3,2,1,0:T(4,128)(2,1)S(1)} %broadcast_in_dim.2), channel_id=1, replica_groups=mesh['z'=8,'y'=4,'x'=4,'core'=2] {'y','z'}, dimensions={0} | all-to-all | bytes 1048576 | tf_op jit(solution)/shard_map/all_to_all | solution.py:28
  45.8 0.0 all-gather.5.cloned.1.call-done
  45.8 0.0 copy-start
  45.8 3.0 %first_ffn.1 = (bf16[32,8,4,256]{3,2,1,0:T(4,128)(2,1)S(1)}, bf16[8,4,256]{2,1,0:T(4,128)(2,1)S(1)}) custom-call(s32[2]{0:T(128)S(1)} %pad_add_fusion.place_ref, bf16[32,8,4,256]{3,2,1,0:T(4,128)(2,1)S(1)} %all_to_all.36.rows_ref, bf16[8,528,256]{2,1,0:T(8,128)(2,1)} %bitcast.21), custom_call_target="tpu_custom_call" | custom-call | tf_op jit(solution)/shard_map/first_ffn/pallas_call | solution.py:112
  48.8 20.8 %all_to_all.37.share_ref = bf16[32,8,4,256]{3,2,1,0:T(4,128)(2,1)S(1)} all-to-all(bf16[32,8,4,256]{3,2,1,0:T(4,128)(2,1)S(1)} %get-tuple-element.18), channel_id=1, replica_groups=mesh['z'=8,'y'=4,'x'=4,'core'=2] {'y','z'}, dimensions={0} | all-to-all | bytes 1048576 | tf_op jit(solution)/shard_map/all_to_all | solution.py:476
  69.5 0.2 settle.1
  69.8 12.0 %all_to_all.38.rows_ref = bf16[8,8,4,256]{3,2,1,0:T(4,128)(2,1)S(1)} all-to-all(bf16[8,8,4,256]{3,2,1,0:T(4,128)(2,1)S(1)} %get-tuple-element.20), channel_id=1, replica_groups=mesh['z'=8,'y'=4,'x'=4,'core'=2] {'x','core'}, dimensions={0} | all-to-all | bytes 262144 | tf_op jit(solution)/shard_map/all_to_all | solution.py:481
  81.8 0.0 copy-done.15
  81.8 0.0 copy-done.6
  81.8 0.0 copy-done.5
  81.8 0.0 copy-done.4
  81.8 0.0 copy-done.11
  81.8 0.0 copy-done.10
  81.8 0.0 copy-done.9
  81.8 0.0 copy-done.14
  81.8 0.0 copy-done.13
  81.8 0.0 copy-done.12
  81.8 0.0 copy-done.7
  81.8 0.0 copy-done.3
  81.9 0.0 copy-done.2
  81.9 0.0 copy-done.1
  81.9 0.0 copy-done.8
  81.9 0.0 copy-done
  81.9 5.8 %mixer.1 = (bf16[8,4,2048]{2,1,0:T(4,128)(2,1)S(1)}, f32[32,4,64,128]{3,2,1,0:T(8,128)}) custom-call(bf16[8,8,4,256]{3,2,1,0:T(4,128)(2,1)S(1)} %all_to_all.38.rows_ref, bf16[2048]{0:T(1024)(128)(2,1)S(1)} %copy-done.8, bf16[2048,256]{1,0:T(8,128)(2,1)S(1)} %copy-done.1, bf16[2048,256]{1,0:T(8,128)(2,1)S(1)} %copy-done.2, bf16[2048,128]{1,0:T(8,128)(2,1)S(1)} %copy-done.3, ...), custom_call_target="tpu_custom_call" | custom-call | tf_op jit(solution)/shard_map/mixer/pallas_call | solution.py:404
  87.7 10.3 %all_to_all.39.tiles_ref = bf16[8,4,2048]{2,1,0:T(4,128)(2,1)S(1)} all-to-all(bf16[8,4,2048]{2,1,0:T(4,128)(2,1)S(1)} %get-tuple-element.21), channel_id=1, replica_groups=mesh['z'=8,'y'=4,'x'=4,'core'=2] {'x','core'}, dimensions={0} | all-to-all | bytes 262144 | tf_op jit(solution)/shard_map/all_to_all | solution.py:429
  98.0 0.1 mix.1
  98.1 11.4 %all_to_all.40.rows_ref = bf16[8,4,2048]{2,1,0:T(4,128)(2,1)S(1)} all-to-all(bf16[8,4,2048]{2,1,0:T(4,128)(2,1)S(1)} %mix.1), channel_id=1, replica_groups=mesh['z'=8,'y'=4,'x'=4,'core'=2] {'z'}, dimensions={0} | all-to-all | bytes 262144 | tf_op jit(solution)/shard_map/all_to_all | solution.py:502
  109.4 0.0 all-gather.7.cloned.1.call-done
  109.4 6.4 %second_ffn.1 = bf16[8,8,4,256]{3,2,1,0:T(4,128)(2,1)S(1)} custom-call(s32[2]{0:T(128)S(1)} %pad_add_fusion.place_ref, bf16[8,4,2048]{2,1,0:T(4,128)(2,1)S(1)} %all_to_all.40.rows_ref, bf16[32,528,256]{2,1,0:T(8,128)(2,1)} %bitcast.20), custom_call_target="tpu_custom_call" | custom-call | tf_op jit(solution)/shard_map/second_ffn/pallas_call | solution.py:223
  115.8 17.2 %all_to_all.41 = bf16[64,4,256]{2,1,0:T(4,128)(2,1)S(1)} all-to-all(bf16[64,4,256]{2,1,0:T(4,128)(2,1)S(1)} %bitcast.14), channel_id=1, replica_groups=mesh['z'=8,'y'=4,'x'=4,'core'=2] {'z','x','core'}, dimensions={0} | all-to-all | bytes 262144 | tf_op jit(solution)/shard_map/all_to_all | solution.py:504
  133.0 0.7 last.1
Async XLA Ops:
  7.2 74.6 %copy-start.15 = (bf16[256]{0:T(256)(128)(2,1)S(1)}, bf16[256]{0:T(256)(128)(2,1)}, u32[]{:S(2)}) copy-start(bf16[256]{0:T(256)(128)(2,1)} %group_ref.1) | copy-start | bytes 1540
  7.2 74.6 %copy-start.6 = (bf16[32,3,128]{2,0,1:T(8,128)(2,1)S(1)}, bf16[32,3,128]{2,0,1:T(8,128)(2,1)}, u32[]{:S(2)}) copy-start(bf16[32,3,128]{2,0,1:T(8,128)(2,1)} %param.46) | copy-start | bytes 73732
  7.2 74.6 %copy-start.5 = (bf16[32,3,128]{2,0,1:T(8,128)(2,1)S(1)}, bf16[32,3,128]{2,0,1:T(8,128)(2,1)}, u32[]{:S(2)}) copy-start(bf16[32,3,128]{2,0,1:T(8,128)(2,1)} %param.45) | copy-start | bytes 73732
  7.2 74.6 %copy-start.4 = (bf16[32,3,256]{2,0,1:T(8,128)(2,1)S(1)}, bf16[32,3,256]{2,0,1:T(8,128)(2,1)}, u32[]{:S(2)}) copy-start(bf16[32,3,256]{2,0,1:T(8,128)(2,1)} %param.44) | copy-start | bytes 147460
  7.2 74.6 %copy-start.11 = (bf16[4,128]{1,0:T(4,128)(2,1)S(1)}, bf16[4,128]{1,0:T(4,128)(2,1)}, u32[]{:S(2)}) copy-start(bf16[4,128]{1,0:T(4,128)(2,1)} %taps_read_ref.1) | copy-start | bytes 3076
  7.2 74.6 %copy-start.10 = (bf16[4,128]{1,0:T(4,128)(2,1)S(1)}, bf16[4,128]{1,0:T(4,128)(2,1)}, u32[]{:S(2)}) copy-start(bf16[4,128]{1,0:T(4,128)(2,1)} %taps_write_ref.1) | copy-start | bytes 3076
  7.2 74.6 %copy-start.9 = (bf16[4,256]{1,0:T(4,128)(2,1)S(1)}, bf16[4,256]{1,0:T(4,128)(2,1)}, u32[]{:S(2)}) copy-start(bf16[4,256]{1,0:T(4,128)(2,1)} %taps_input_ref.1) | copy-start | bytes 6148
  7.2 74.6 %copy-start.14 = (f32[4]{0:T(128)S(1)}, f32[4]{0:T(128)}, u32[]{:S(2)}) copy-start(f32[4]{0:T(128)} %skip_ref.1) | copy-start | bytes 52
  7.3 74.6 %copy-start.13 = (f32[4]{0:T(128)S(1)}, f32[4]{0:T(128)}, u32[]{:S(2)}) copy-start(f32[4]{0:T(128)} %rate_ref.1) | copy-start | bytes 52
  7.3 74.6 %copy-start.12 = (f32[4]{0:T(128)S(1)}, f32[4]{0:T(128)}, u32[]{:S(2)}) copy-start(f32[4]{0:T(128)} %bias_ref.1) | copy-start | bytes 52
  7.3 74.6 %copy-start.7 = (bf16[2048,4]{0,1:T(4,128)(2,1)S(1)}, bf16[2048,4]{0,1:T(4,128)(2,1)}, u32[]{:S(2)}) copy-start(bf16[2048,4]{0,1:T(4,128)(2,1)} %param.37) | copy-start | bytes 49156
  7.3 74.6 %copy-start.3 = (bf16[2048,128]{1,0:T(8,128)(2,1)S(1)}, bf16[2048,128]{1,0:T(8,128)(2,1)}, u32[]{:S(2)}) copy-start(bf16[2048,128]{1,0:T(8,128)(2,1)} %write_ref.1) | copy-start | bytes 1572868
  7.3 74.6 %copy-start.2 = (bf16[2048,256]{1,0:T(8,128)(2,1)S(1)}, bf16[2048,256]{1,0:T(8,128)(2,1)}, u32[]{:S(2)}) copy-start(bf16[2048,256]{1,0:T(8,128)(2,1)} %input_ref.1) | copy-start | bytes 3145732
  7.3 74.6 %copy-start.1 = (bf16[2048,256]{1,0:T(8,128)(2,1)S(1)}, bf16[2048,256]{1,0:T(8,128)(2,1)}, u32[]{:S(2)}) copy-start(bf16[2048,256]{1,0:T(8,128)(2,1)} %gate_ref.1) | copy-start | bytes 3145732
  7.3 74.6 %copy-start.8 = (bf16[2048]{0:T(1024)(128)(2,1)S(1)}, bf16[2048]{0:T(1024)(128)(2,1)}, u32[]{:S(2)}) copy-start(bf16[2048]{0:T(1024)(128)(2,1)} %gain_ref.1) | copy-start | bytes 12292
  7.3 38.5 %all-gather.5.cloned.1.call-start = ((), (), s32[]{:S(2)}) async-start(), calls=%async_computation.7 | async-start | bytes 2433024 | tf_op jit(solution)/shard_map/all_gather | solution.py:469
  9.6 99.8 %all-gather.7.cloned.1.call-start = ((), (), s32[]{:S(2)}) async-start(), calls=%async_computation.8 | async-start | bytes 8921088 | tf_op jit(solution)/shard_map/all_gather | solution.py:473
  45.8 36.1 %copy-start = (f32[32,4,64,128]{3,2,1,0:T(8,128)S(1)}, f32[32,4,64,128]{3,2,1,0:T(8,128)}, u32[]{:S(2)}) copy-start(f32[32,4,64,128]{3,2,1,0:T(8,128)} %state_ref.1) | copy-start | bytes 12582916
Sparse Core Ops, SparseCore 0:
  10.5 32.0 all-gather.4
  45.2 61.4 all-gather.6

commit v12 on v11

--- a/solution.py
+++ b/solution.py
@@ -215,14 +215,14 @@
                 weights_ref[y * TP + u, 2 * HIDDEN :],
                 preferred_element_type=jnp.float32,
             )
-        out_ref[:, u] = down.reshape(Z, ROWS, FEATS).astype(jnp.bfloat16)
+        out_ref[u] = down.reshape(Z, ROWS, FEATS).astype(jnp.bfloat16)
 
 
 def second_partial(place, rows, weights):
     vmem = pl.BlockSpec(memory_space=pltpu.VMEM)
     return pl.pallas_call(
         second_kernel,
-        out_shape=pltpu.VMEM((Z, TP, ROWS, FEATS), jnp.bfloat16),
+        out_shape=pltpu.VMEM((TP, Z, ROWS, FEATS), jnp.bfloat16),
         in_specs=[
             pl.BlockSpec(memory_space=pltpu.SMEM),
             vmem,
@@ -240,7 +240,7 @@
 
 
 def last_kernel(share_ref, out_ref):
-    branch = jnp.sum(share_ref[...].astype(jnp.float32), axis=0)
+    branch = jnp.sum(share_ref[...].astype(jnp.float32), axis=1)
     out_ref[...] = (0.5 * branch).reshape(TP * ROWS, FEATS).astype(jnp.bfloat16)
 
 
@@ -501,8 +501,8 @@
 
     rows = lax.all_to_all(mixed, "z", 0, 0, tiled=True)
     share = second_partial(place, rows, weights_two)
-    share = lax.all_to_all(share.reshape(-1, ROWS, FEATS), ("z", *TP_AXES), 0, 0, tiled=True)
-    residual_out = last_sum(share.reshape(Z, TP, ROWS, FEATS))
+    share = lax.all_to_all(share.reshape(-1, ROWS, FEATS), (*TP_AXES, "z"), 0, 0, tiled=True)
+    residual_out = last_sum(share.reshape(TP, Z, ROWS, FEATS))
     return (residual_out, state_out)
 
 

time: 141 us -> 140 us (level)
  blocking collectives: 108 us -> 106 us
where the time goes in v12:
time: 140 us; the launch traced here: 139 us
  blocking collectives  106 us (76%)
  Pallas kernels  18.2 us (13%)
  between operations  14.3 us (10%)
    all_to_all x1, blocking collectives, sent_to_all(): lax.all_to_all(jnp.broadcast_to(array[None], (length, *array.shape)), axi...  25.6 us
    all_to_all x1, blocking collectives, per_device(): share = lax.all_to_all(share, BLOCK_AXES, 0, 0, tiled=True)  20.8 us
    all_to_all x1, blocking collectives, per_device(): lax.all_to_all(share.reshape(-1, ROWS, FEATS), (*TP_AXES, 'z'), 0, 0, til...  16.1 us
    all_to_all x1, blocking collectives, per_device(): lax.all_to_all(copies, TP_AXES, 0, 0, tiled=True)  12 us
    all_to_all x1, blocking collectives, per_device(): rows = lax.all_to_all(mixed, 'z', 0, 0, tiled=True)  11.4 us
    all_to_all x1, blocking collectives, state_mixer(): tiles = lax.all_to_all(partial_out, TP_AXES, 0, 0, tiled=True)  10.3 us
    all_to_all x1, blocking collectives, per_device(): mine = lax.all_to_all(pieces, TP_AXES, 0, 0, tiled=True)  10.2 us
    pallas_call x1, Pallas kernels, second_partial(): pl.pallas_call(second_kernel, out_shape=pltpu.VMEM((TP, Z, ROWS, FEATS),...  6.35 us
  transfers between devices with their start and end apart: 2, of which 0 were waited for; matrix products, arithmetic and copies ran while one was open for 0% of the time, Pallas kernels for 6%

profile of v12, /device:TPU:1, one launch (start us, length us, event | category | flops | bytes accessed | tf_op | source)
XLA Modules:
  0.0 139.4 jit_solution(18001822098092175382)
XLA Ops:
  7.2 0.0 copy-start.15
  7.2 0.0 copy-start.6
  7.2 0.0 copy-start.5
  7.2 0.0 copy-start.4
  7.2 0.0 copy-start.11
  7.2 0.0 copy-start.10
  7.2 0.0 copy-start.9
  7.2 0.0 copy-start.14
  7.3 0.0 copy-start.13
  7.3 0.0 copy-start.12
  7.3 0.0 copy-start.7
  7.3 0.0 copy-start.3
  7.3 0.0 copy-start.2
  7.3 0.0 copy-start.1
  7.3 0.0 copy-start.8
  7.3 0.0 all-gather.5.cloned.1.call-start
  7.4 0.1 pad_add_fusion.place_ref
  7.4 2.1 %shares.1 = (bf16[528,256]{1,0:T(8,128)(2,1)}, bf16[528,256]{1,0:T(8,128)(2,1)}, bf16[8,4,256]{2,1,0:T(4,128)(2,1)S(1)}) custom-call(s32[2]{0:T(128)S(1)} %pad_add_fusion.place_ref, bf16[32,256]{1,0:T(8,128)(2,1)} %rows_ref.1, bf16[256]{0:T(256)(128)(2,1)} %refs_0_.1, bf16[176,256]{1,0:T(8,128)(2,1)} %bitcast.22, bf16[176,256]{1,0:T(8,128)(2,1)} %bitcast.23, ...), custom_call_target="tpu_custom_call" | custom-call | tf_op jit(solution)/shard_map/shares/pallas_call | solution.py:63
  9.6 0.0 all-gather.5.cloned.1.call-update
  9.6 0.0 all-gather.7.cloned.1.call-start
  9.7 10.2 %all_to_all.35 = bf16[8,4,256]{2,1,0:T(4,128)(2,1)S(1)} all-to-all(bf16[8,4,256]{2,1,0:T(4,128)(2,1)S(1)} %get-tuple-element.14), channel_id=1, replica_groups=mesh['z'=8,'y'=4,'x'=4,'core'=2] {'x','core'}, dimensions={0} | all-to-all | bytes 32768 | tf_op jit(solution)/shard_map/all_to_all | solution.py:471
  19.9 0.0 all-gather.7.cloned.1.call-update
  19.9 0.2 broadcast_in_dim.2
  20.2 25.6 %all_to_all.36.rows_ref = bf16[32,8,4,256]{3,2,1,0:T(4,128)(2,1)S(1)} all-to-all(bf16[32,8,4,256]{3,2,1,0:T(4,128)(2,1)S(1)} %broadcast_in_dim.2), channel_id=1, replica_groups=mesh['z'=8,'y'=4,'x'=4,'core'=2] {'y','z'}, dimensions={0} | all-to-all | bytes 1048576 | tf_op jit(solution)/shard_map/all_to_all | solution.py:28
  45.8 0.0 all-gather.5.cloned.1.call-done
  45.8 0.0 copy-start
  45.8 3.0 %first_ffn.1 = (bf16[32,8,4,256]{3,2,1,0:T(4,128)(2,1)S(1)}, bf16[8,4,256]{2,1,0:T(4,128)(2,1)S(1)}) custom-call(s32[2]{0:T(128)S(1)} %pad_add_fusion.place_ref, bf16[32,8,4,256]{3,2,1,0:T(4,128)(2,1)S(1)} %all_to_all.36.rows_ref, bf16[8,528,256]{2,1,0:T(8,128)(2,1)} %bitcast.21), custom_call_target="tpu_custom_call" | custom-call | tf_op jit(solution)/shard_map/first_ffn/pallas_call | solution.py:112
  48.8 20.8 %all_to_all.37.share_ref = bf16[32,8,4,256]{3,2,1,0:T(4,128)(2,1)S(1)} all-to-all(bf16[32,8,4,256]{3,2,1,0:T(4,128)(2,1)S(1)} %get-tuple-element.18), channel_id=1, replica_groups=mesh['z'=8,'y'=4,'x'=4,'core'=2] {'y','z'}, dimensions={0} | all-to-all | bytes 1048576 | tf_op jit(solution)/shard_map/all_to_all | solution.py:476
  69.5 0.2 settle.1
  69.8 12.0 %all_to_all.38.rows_ref = bf16[8,8,4,256]{3,2,1,0:T(4,128)(2,1)S(1)} all-to-all(bf16[8,8,4,256]{3,2,1,0:T(4,128)(2,1)S(1)} %get-tuple-element.20), channel_id=1, replica_groups=mesh['z'=8,'y'=4,'x'=4,'core'=2] {'x','core'}, dimensions={0} | all-to-all | bytes 262144 | tf_op jit(solution)/shard_map/all_to_all | solution.py:481
  81.8 0.0 copy-done.15
  81.8 0.0 copy-done.6
  81.8 0.0 copy-done.5
  81.8 0.0 copy-done.4
  81.8 0.0 copy-done.11
  81.8 0.0 copy-done.10
  81.8 0.0 copy-done.9
  81.8 0.0 copy-done.14
  81.8 0.0 copy-done.13
  81.8 0.0 copy-done.12
  81.8 0.0 copy-done.7
  81.8 0.0 copy-done.3
  81.9 0.0 copy-done.2
  81.9 0.0 copy-done.1
  81.9 0.0 copy-done.8
  81.9 0.0 copy-done
  81.9 5.8 %mixer.1 = (bf16[8,4,2048]{2,1,0:T(4,128)(2,1)S(1)}, f32[32,4,64,128]{3,2,1,0:T(8,128)}) custom-call(bf16[8,8,4,256]{3,2,1,0:T(4,128)(2,1)S(1)} %all_to_all.38.rows_ref, bf16[2048]{0:T(1024)(128)(2,1)S(1)} %copy-done.8, bf16[2048,256]{1,0:T(8,128)(2,1)S(1)} %copy-done.1, bf16[2048,256]{1,0:T(8,128)(2,1)S(1)} %copy-done.2, bf16[2048,128]{1,0:T(8,128)(2,1)S(1)} %copy-done.3, ...), custom_call_target="tpu_custom_call" | custom-call | tf_op jit(solution)/shard_map/mixer/pallas_call | solution.py:404
  87.7 10.3 %all_to_all.39.tiles_ref = bf16[8,4,2048]{2,1,0:T(4,128)(2,1)S(1)} all-to-all(bf16[8,4,2048]{2,1,0:T(4,128)(2,1)S(1)} %get-tuple-element.21), channel_id=1, replica_groups=mesh['z'=8,'y'=4,'x'=4,'core'=2] {'x','core'}, dimensions={0} | all-to-all | bytes 262144 | tf_op jit(solution)/shard_map/all_to_all | solution.py:429
  98.0 0.1 mix.1
  98.1 11.4 %all_to_all.40.rows_ref = bf16[8,4,2048]{2,1,0:T(4,128)(2,1)S(1)} all-to-all(bf16[8,4,2048]{2,1,0:T(4,128)(2,1)S(1)} %mix.1), channel_id=1, replica_groups=mesh['z'=8,'y'=4,'x'=4,'core'=2] {'z'}, dimensions={0} | all-to-all | bytes 262144 | tf_op jit(solution)/shard_map/all_to_all | solution.py:502
  109.4 0.0 all-gather.7.cloned.1.call-done
  109.4 6.4 %second_ffn.1 = bf16[8,8,4,256]{3,2,1,0:T(4,128)(2,1)S(1)} custom-call(s32[2]{0:T(128)S(1)} %pad_add_fusion.place_ref, bf16[8,4,2048]{2,1,0:T(4,128)(2,1)S(1)} %all_to_all.40.rows_ref, bf16[32,528,256]{2,1,0:T(8,128)(2,1)} %bitcast.20), custom_call_target="tpu_custom_call" | custom-call | tf_op jit(solution)/shard_map/second_ffn/pallas_call | solution.py:223
  115.8 16.1 %all_to_all.41 = bf16[64,4,256]{2,1,0:T(4,128)(2,1)S(1)} all-to-all(bf16[64,4,256]{2,1,0:T(4,128)(2,1)S(1)} %bitcast.14), channel_id=1, replica_groups=mesh['z'=8,'y'=4,'x'=4,'core'=2] {'x','core','z'}, dimensions={0} | all-to-all | bytes 262144 | tf_op jit(solution)/shard_map/all_to_all | solution.py:504
  131.9 0.7 last.1
Async XLA Ops:
  7.2 74.6 %copy-start.15 = (bf16[256]{0:T(256)(128)(2,1)S(1)}, bf16[256]{0:T(256)(128)(2,1)}, u32[]{:S(2)}) copy-start(bf16[256]{0:T(256)(128)(2,1)} %group_ref.1) | copy-start | bytes 1540
  7.2 74.6 %copy-start.6 = (bf16[32,3,128]{2,0,1:T(8,128)(2,1)S(1)}, bf16[32,3,128]{2,0,1:T(8,128)(2,1)}, u32[]{:S(2)}) copy-start(bf16[32,3,128]{2,0,1:T(8,128)(2,1)} %param.46) | copy-start | bytes 73732
  7.2 74.6 %copy-start.5 = (bf16[32,3,128]{2,0,1:T(8,128)(2,1)S(1)}, bf16[32,3,128]{2,0,1:T(8,128)(2,1)}, u32[]{:S(2)}) copy-start(bf16[32,3,128]{2,0,1:T(8,128)(2,1)} %param.45) | copy-start | bytes 73732
  7.2 74.6 %copy-start.4 = (bf16[32,3,256]{2,0,1:T(8,128)(2,1)S(1)}, bf16[32,3,256]{2,0,1:T(8,128)(2,1)}, u32[]{:S(2)}) copy-start(bf16[32,3,256]{2,0,1:T(8,128)(2,1)} %param.44) | copy-start | bytes 147460
  7.2 74.6 %copy-start.11 = (bf16[4,128]{1,0:T(4,128)(2,1)S(1)}, bf16[4,128]{1,0:T(4,128)(2,1)}, u32[]{:S(2)}) copy-start(bf16[4,128]{1,0:T(4,128)(2,1)} %taps_read_ref.1) | copy-start | bytes 3076
  7.2 74.6 %copy-start.10 = (bf16[4,128]{1,0:T(4,128)(2,1)S(1)}, bf16[4,128]{1,0:T(4,128)(2,1)}, u32[]{:S(2)}) copy-start(bf16[4,128]{1,0:T(4,128)(2,1)} %taps_write_ref.1) | copy-start | bytes 3076
  7.2 74.6 %copy-start.9 = (bf16[4,256]{1,0:T(4,128)(2,1)S(1)}, bf16[4,256]{1,0:T(4,128)(2,1)}, u32[]{:S(2)}) copy-start(bf16[4,256]{1,0:T(4,128)(2,1)} %taps_input_ref.1) | copy-start | bytes 6148
  7.2 74.6 %copy-start.14 = (f32[4]{0:T(128)S(1)}, f32[4]{0:T(128)}, u32[]{:S(2)}) copy-start(f32[4]{0:T(128)} %skip_ref.1) | copy-start | bytes 52
  7.3 74.6 %copy-start.13 = (f32[4]{0:T(128)S(1)}, f32[4]{0:T(128)}, u32[]{:S(2)}) copy-start(f32[4]{0:T(128)} %rate_ref.1) | copy-start | bytes 52
  7.3 74.6 %copy-start.12 = (f32[4]{0:T(128)S(1)}, f32[4]{0:T(128)}, u32[]{:S(2)}) copy-start(f32[4]{0:T(128)} %bias_ref.1) | copy-start | bytes 52
  7.3 74.6 %copy-start.7 = (bf16[2048,4]{0,1:T(4,128)(2,1)S(1)}, bf16[2048,4]{0,1:T(4,128)(2,1)}, u32[]{:S(2)}) copy-start(bf16[2048,4]{0,1:T(4,128)(2,1)} %param.37) | copy-start | bytes 49156
  7.3 74.6 %copy-start.3 = (bf16[2048,128]{1,0:T(8,128)(2,1)S(1)}, bf16[2048,128]{1,0:T(8,128)(2,1)}, u32[]{:S(2)}) copy-start(bf16[2048,128]{1,0:T(8,128)(2,1)} %write_ref.1) | copy-start | bytes 1572868
  7.3 74.6 %copy-start.2 = (bf16[2048,256]{1,0:T(8,128)(2,1)S(1)}, bf16[2048,256]{1,0:T(8,128)(2,1)}, u32[]{:S(2)}) copy-start(bf16[2048,256]{1,0:T(8,128)(2,1)} %input_ref.1) | copy-start | bytes 3145732
  7.3 74.6 %copy-start.1 = (bf16[2048,256]{1,0:T(8,128)(2,1)S(1)}, bf16[2048,256]{1,0:T(8,128)(2,1)}, u32[]{:S(2)}) copy-start(bf16[2048,256]{1,0:T(8,128)(2,1)} %gate_ref.1) | copy-start | bytes 3145732
  7.3 74.6 %copy-start.8 = (bf16[2048]{0:T(1024)(128)(2,1)S(1)}, bf16[2048]{0:T(1024)(128)(2,1)}, u32[]{:S(2)}) copy-start(bf16[2048]{0:T(1024)(128)(2,1)} %gain_ref.1) | copy-start | bytes 12292
  7.3 38.5 %all-gather.5.cloned.1.call-start = ((), (), s32[]{:S(2)}) async-start(), calls=%async_computation.7 | async-start | bytes 2433024 | tf_op jit(solution)/shard_map/all_gather | solution.py:469
  9.6 99.8 %all-gather.7.cloned.1.call-start = ((), (), s32[]{:S(2)}) async-start(), calls=%async_computation.8 | async-start | bytes 8921088 | tf_op jit(solution)/shard_map/all_gather | solution.py:473
  45.8 36.1 %copy-start = (f32[32,4,64,128]{3,2,1,0:T(8,128)S(1)}, f32[32,4,64,128]{3,2,1,0:T(8,128)}, u32[]{:S(2)}) copy-start(f32[32,4,64,128]{3,2,1,0:T(8,128)} %state_ref.1) | copy-start | bytes 12582916
Sparse Core Ops, SparseCore 0:
  10.5 32.0 all-gather.4
  45.2 61.4 all-gather.6
